TPU v7x, 128 devices: a whole 4x4x4 slice. The times are simulated.
128 devices in a mesh: sp: 64 (over z, y, x), tp: 2 (over core).
Axes of the slice: x: 4, y: 4, z: 4, core: 2. Of those that a mesh axis runs over, the one named last changes fastest.
Arguments:
- glu_value: bfloat16 [16384, 1024], P('sp', 'tp'), may hold values from -12 to 12
- glu_gate: bfloat16 [16384, 1024], P('sp', 'tp'), may hold values from -8 to 8
- conv_kernel: bfloat16 [31, 1024], P(None, 'tp'), may hold values from -1 to 1
- conv_bias: float32 [1024], P('tp'), may hold values from -1.5 to 1.5
- group_gain: float32 [1024], P('tp'), may hold values from 0.1 to 1.9
- group_shift: float32 [1024], P('tp'), may hold values from -2.5 to 2.5
- out_weight: bfloat16 [1024, 2048], replicated, may hold values from -0.1875 to 0.1875
- residual: bfloat16 [16384, 2048], P(('sp', 'tp')), may hold values from -12 to 12
- ffn_gain: float32 [2048], replicated, may hold values from 0.1 to 1.9
- expert_pick: int32 [16384, 2], P(('sp', 'tp')), may hold values from 0 to 127, as said below
- pair_logits: float32 [16384, 2], P(('sp', 'tp')), may hold values from -1.2 to 1.2
- group_prob: float32 [16384], P(('sp', 'tp')), may hold values from 0.5 to 1
- gate_weight: bfloat16 [128, 2048, 512], P(('sp', 'tp')), may hold values from -0.125 to 0.125
- up_weight: bfloat16 [128, 2048, 512], P(('sp', 'tp')), may hold values from -0.125 to 0.125
- down_weight: bfloat16 [128, 512, 2048], P(('sp', 'tp')), may hold values from -0.75 to 0.75
Outputs:
- result: bfloat16 [16384, 2048], P(('sp', 'tp'))
Inputs may be any that keep to these rules, and one draw needn't show every extreme that they name: `expert_pick`: both picks of a token are different experts of the same group of 32 consecutive experts. Among the 128 tokens of one device (aligned blocks of rows) no expert is picked more than 4 times, and in every such block some expert is picked exactly 4 times.
All inputs are finite; a program needn't handle non-finite values.
Results may differ from a plain program's by a relative error of at most 0.014.
Values may be sent and summed in bfloat16 or wider, within the bound.
No kernel may reach another device: no remote copies, remote signals or barrier semaphores. Data moves between devices by JAX's collectives and lax.ppermute only.
A program may use at most 64 MiB of HBM per device.

v0:
```python
import jax
import jax.numpy as jnp
from jax import lax
from jax.sharding import PartitionSpec as P

CONV_GROUPS = 8


EPS = 1e-06


def from_behind(value, axis, by):
    peers = lax.axis_size(axis)
    pairs = [(i, i + by) for i in range(peers) if 0 <= i + by < peers]
    return lax.ppermute(value, axis, pairs)


def local(
    glu_value,
    glu_gate,
    conv_kernel,
    conv_bias,
    group_gain,
    group_shift,
    out_weight,
    residual,
    ffn_gain,
    expert_pick,
    pair_logits,
    group_prob,
    gate_weight,
    up_weight,
    down_weight,
):
    glued_rows = (
        glu_value.astype(jnp.float32) * jax.nn.sigmoid(glu_gate.astype(jnp.float32))
    ).astype(jnp.bfloat16)
    reach_rows = conv_kernel.shape[0] - 1
    length = glued_rows.shape[0]
    earlier = from_behind(glued_rows[length - reach_rows :], "sp", 1)
    extended = jnp.concatenate([earlier, glued_rows], axis=0).astype(jnp.float32)
    kernel = conv_kernel.astype(jnp.float32)
    summed = jnp.zeros(glued_rows.shape, jnp.float32) + conv_bias
    for offset in range(reach_rows + 1):
        summed = summed + kernel[offset] * extended[offset : offset + length]
    groups_here = CONV_GROUPS // lax.axis_size("tp")
    grouped = summed.reshape(length, groups_here, -1)
    centre = jnp.mean(grouped, axis=-1, keepdims=True)
    variance = jnp.mean(jnp.square(grouped - centre), axis=-1, keepdims=True)
    leveled = ((grouped - centre) * lax.rsqrt(variance + EPS)).reshape(length, -1)
    mixed_rows = jax.nn.silu(leveled * group_gain + group_shift).astype(jnp.bfloat16)
    local_rows = residual.shape[0]
    regrouped = lax.all_to_all(mixed_rows, "tp", split_axis=0, concat_axis=1, tiled=True)
    projected = jnp.dot(regrouped, out_weight, preferred_element_type=jnp.float32)
    hidden = (residual.astype(jnp.float32) + projected).astype(jnp.bfloat16)
    hidden_full = hidden.astype(jnp.float32)
    scale_rows = lax.rsqrt(jnp.mean(hidden_full * hidden_full, axis=-1, keepdims=True) + EPS)
    normed = (hidden_full * scale_rows * ffn_gain).astype(jnp.bfloat16)
    experts_all = lax.axis_size("sp") * lax.axis_size("tp")
    capacity = 4 * local_rows // experts_all
    picks = expert_pick.shape[1]
    model_width = normed.shape[1]
    slot_experts = expert_pick.reshape(-1)
    onehot = (slot_experts[:, None] == jnp.arange(experts_all, dtype=jnp.int32)[None, :]).astype(
        jnp.int32
    )
    before = jnp.cumsum(onehot, axis=0) - onehot
    slot_rank = jnp.sum(before * onehot, axis=1)
    slot_place = slot_experts * capacity + slot_rank
    doubled = jnp.repeat(normed, picks, axis=0)
    outgoing = (
        jnp.zeros((experts_all * capacity, model_width), jnp.bfloat16).at[slot_place].set(doubled)
    )
    outgoing = outgoing.reshape(experts_all, capacity, model_width)
    arrived = lax.all_to_all(outgoing, ("sp", "tp"), split_axis=0, concat_axis=0, tiled=True)
    senders, slot_count, width_here = arrived.shape
    flat_rows = arrived.reshape(senders * slot_count, width_here)
    gate_out = jnp.dot(flat_rows, gate_weight[0], preferred_element_type=jnp.float32)
    up_out = jnp.dot(flat_rows, up_weight[0], preferred_element_type=jnp.float32)
    active = (jax.nn.silu(gate_out) * up_out).astype(jnp.bfloat16)
    answer = jnp.dot(active, down_weight[0], preferred_element_type=jnp.float32).astype(
        jnp.bfloat16
    )
    returned = lax.all_to_all(
        answer.reshape(senders, slot_count, width_here),
        ("sp", "tp"),
        split_axis=0,
        concat_axis=0,
        tiled=True,
    )
    flat_returned = returned.reshape(experts_all * capacity, model_width)
    picked = flat_returned[slot_place].reshape(local_rows, picks, model_width)
    first_share = group_prob * jax.nn.sigmoid(pair_logits[:, 0] - pair_logits[:, 1])
    second_share = group_prob * jax.nn.sigmoid(pair_logits[:, 1] - pair_logits[:, 0])
    combined = hidden_full + first_share[:, None] * picked[:, 0].astype(jnp.float32)
    combined = combined + second_share[:, None] * picked[:, 1].astype(jnp.float32)
    return combined.astype(jnp.bfloat16)


def solution(mesh):
    in_specs = (
        P("sp", "tp"),
        P("sp", "tp"),
        P(None, "tp"),
        P("tp"),
        P("tp"),
        P("tp"),
        P(),
        P(("sp", "tp"), None),
        P(),
        P(("sp", "tp"), None),
        P(("sp", "tp"), None),
        P(("sp", "tp")),
        P(("sp", "tp"), None, None),
        P(("sp", "tp"), None, None),
        P(("sp", "tp"), None, None),
    )
    out_specs = P(("sp", "tp"), None)
    return jax.shard_map(local, mesh=mesh, in_specs=in_specs, out_specs=out_specs, check_vma=False)
```

profile of v0, /device:TPU:1, one launch (start us, length us, event | category | flops | bytes accessed | tf_op | source)
XLA Modules:
  0.0 145.9 jit_solution(6658203360386712343)
XLA Ops:
  0.0 0.0 copy-start
  0.0 0.0 copy-start.5
  0.0 1.3 multiply_convert_fusion.2
  1.4 3.9 %collective-permute-start = (bf16[30,512]{1,0:T(8,128)(2,1)S(1)}, bf16[30,512]{1,0:T(8,128)(2,1)S(1)}, u32[]{:S(2)}, u32[]{:S(2)}) collective-permute-start(bf16[30,512]{1,0:T(8,128)(2,1)S(1)} %slice.281), channel_id=1, source_target_pairs={{0,2},{2,4},{4,6},{6,8},{8,10},{10,12},{12,14},{14,16},{16,18},{18... | collective-permute-start | bytes 92168 | tf_op jit(solution)/shard_map/ppermute | solution.py:15
  5.3 1.0 fusion.61
  6.4 1.0 fusion.62
  7.3 0.8 copy.25
  8.1 0.1 eq.29
  8.3 0.1 eq.25
  8.4 0.7 broadcast_multiply_fusion.1
  9.1 0.1 copy.27
  9.2 0.2 fusion.54
  9.5 0.1 copy.24
  9.6 0.1 mul.507
  9.8 0.2 fusion.56
  10.0 0.0 collective-permute-done
  10.0 0.1 maximum_convert_fusion
  10.1 0.0 copy-done.5
  10.1 2.8 %fusion.22 = f32[256,512]{1,0:T(8,128)} fusion(f32[286,512]{1,0:T(8,128)S(1)} %maximum_convert_fusion, f32[512]{0:T(512)S(1)} %bitcast.165, f32[512]{0:T(512)S(1)} %bitcast.163, f32[512]{0:T(512)S(1)} %bitcast.161, f32[512]{0:T(512)S(1)} %bitcast.159, f32[512]{0:T(512)S(1)} %bitcast.157, f32[512]{0:T(512)S(1)} %bitcast.155, f32[512]{0:T(512)S(1)} %bitcast.153, ...), kind=kLoop, calls=%fused_computation.27 | loop fusion | flops 8126464 | bytes 16842752 | tf_op jit(solution)/shard_map/add | solution.py:45
  12.9 0.0 copy-start.6
  12.9 0.0 copy-start.7
  12.9 1.2 reshape.113
  14.1 0.3 reduce_sum.38
  14.5 0.6 multiply_reduce_fusion.1
  15.2 0.3 mul.497
  15.5 0.3 sub.28
  15.8 0.0 copy-done.6
  15.8 0.0 copy-done.7
  15.8 0.0 copy-start.3
  15.9 2.3 %multiply_convert_fusion.1 = bf16[256,512]{1,0:T(8,128)(2,1)S(1)} fusion(f32[32,8,4,128]{3,2,1,0:T(4,128)S(1)} %bitcast.98, f32[32,8,4,128]{3,2,1,0:T(4,128)S(1)} %bitcast.99, f32[512]{0:T(512)S(1)} %copy-done.6, f32[512]{0:T(512)S(1)} %copy-done.7, f32[286,512]{1,0:T(8,128)S(1)} %maximum_convert_fusion, f32[512]{0:T(512)S(1)} %bitcast.166, ...), kind=kLoop, calls=%fused_computation.91 | loop fusion | flops 9306112 | bytes 17633280 | tf_op jit(solution)/shard_map/convert_element_type | solution.py:51
  18.2 4.5 %all_to_all.29 = bf16[2,128,512]{2,1,0:T(8,128)(2,1)S(1)} all-to-all(bf16[2,128,512]{2,1,0:T(8,128)(2,1)S(1)} %bitcast.100), channel_id=1, replica_groups=mesh['sp'=64,'tp'=2] {'tp'}, dimensions={0} | all-to-all | bytes 524288 | tf_op jit(solution)/shard_map/all_to_all | solution.py:53
  22.7 0.2 copy.23
  22.9 0.0 copy-done.3
  22.9 0.0 copy-start.4
  22.9 3.0 %multiply_reduce_fusion = (f32[128]{0:T(128)S(1)}, f32[128,2048]{1,0:T(8,128)S(1)}) fusion(bf16[128,1024]{0,1:T(8,128)(2,1)S(1)} %bitcast.101, bf16[1024,2048]{1,0:T(8,128)(2,1)} %param.21, bf16[128,2048]{1,0:T(8,128)(2,1)S(1)} %copy-done.3), kind=kOutput, calls=%fused_computation.19 | convolution fusion | flops 538443648 | bytes 6029824 | tf_op jit(solution)/shard_map/dot_general | solution.py:54
  25.9 0.0 copy-start.1
  25.9 1.0 copy-done.1
  26.9 0.0 copy-done.4
  26.9 0.2 multiply_convert_fusion
  27.0 0.6 broadcast_in_dim.5
  27.7 1.2 reshape.139
  28.9 4.4 %scatter_custom_fusion = bf16[512,2048]{1,0:T(8,128)(2,1)} fusion(s32[256]{0:T(256)S(1)} %bitcast.169, bf16[256,2048]{1,0:T(8,128)(2,1)} %reshape.139, bf16[]{:T(256)} %constant.8.clone.1), kind=kCustom, calls=%fused_computation.20 | custom fusion | bytes 2097664 | tf_op jit(solution)/shard_map/scatter | solution.py:72
  33.4 4.1 %reshape.116 = bf16[128,4,2048]{2,1,0:T(4,128)(2,1)} reshape(bf16[512,2048]{1,0:T(8,128)(2,1)} %scatter_custom_fusion) | data formatting | bytes 4194304 | tf_op jit(solution)/shard_map/reshape | solution.py:74
  37.5 40.6 %all_to_all.30 = bf16[128,4,2048]{2,1,0:T(4,128)(2,1)} all-to-all(bf16[128,4,2048]{2,1,0:T(4,128)(2,1)} %reshape.116), channel_id=1, replica_groups=mesh['sp'=64,'tp'=2] {'sp','tp'}, dimensions={0} | all-to-all | bytes 4194304 | tf_op jit(solution)/shard_map/all_to_all | solution.py:75
  78.1 4.0 %reshape.117 = bf16[512,2048]{1,0:T(8,128)(2,1)} reshape(bf16[128,4,2048]{2,1,0:T(4,128)(2,1)} %all_to_all.30) | data formatting | bytes 4194304 | tf_op jit(solution)/shard_map/reshape | solution.py:77
  82.1 3.5 %fusion.5 = f32[512,512]{1,0:T(8,128)S(1)} fusion(bf16[512,2048]{1,0:T(8,128)(2,1)} %reshape.117, bf16[1,2048,512]{2,1,0:T(8,128)(2,1)} %param.27), kind=kOutput, calls=%fused_computation.9 | convolution fusion | flops 1073741824 | bytes 5242880 | tf_op jit(solution)/shard_map/dot_general | solution.py:78
  85.5 0.0 copy-done
  85.6 6.0 %convolution_convert_fusion = bf16[512,2048]{1,0:T(8,128)(2,1)} fusion(bf16[1,512,2048]{2,1,0:T(8,128)(2,1)S(1)} %copy-done, bf16[512,2048]{1,0:T(8,128)(2,1)} %reshape.117, bf16[1,2048,512]{2,1,0:T(8,128)(2,1)} %param.28, f32[512,512]{1,0:T(8,128)S(1)} %fusion.5), kind=kOutput, calls=%fused_computation.2 | convolution fusion | flops 2150105088 | bytes 9437184 | tf_op jit(solution)/shard_map/dot_general | solution.py:81
  91.6 4.1 %reshape.118 = bf16[128,4,2048]{2,1,0:T(4,128)(2,1)} reshape(bf16[512,2048]{1,0:T(8,128)(2,1)} %convolution_convert_fusion) | data formatting | bytes 4194304 | tf_op jit(solution)/shard_map/reshape | solution.py:85
  95.7 0.0 copy-start.8
  95.7 0.0 copy-start.9
  95.7 5.6 %all-to-all-start.2 = ((bf16[128,4,2048]{2,1,0:T(4,128)(2,1)}), bf16[128,4,2048]{2,1,0:T(4,128)(2,1)}, u32[]{:S(2)}, u32[]{:S(2)}) async-start(bf16[128,4,2048]{2,1,0:T(4,128)(2,1)} %reshape.118), calls=%async_computation.2 | async-start | bytes 4194304 | tf_op jit(solution)/shard_map/all_to_all | solution.py:84
  101.3 0.0 copy-done.8
  101.3 0.0 copy-done.9
  101.4 30.2 %all-to-all-done.2 = bf16[128,4,2048]{2,1,0:T(4,128)(2,1)} async-done(((bf16[128,4,2048]{2,1,0:T(4,128)(2,1)}), bf16[128,4,2048]{2,1,0:T(4,128)(2,1)}, u32[]{:S(2)}, u32[]{:S(2)}) %all-to-all-start.2) | async-done | bytes 2097184 | tf_op jit(solution)/shard_map/all_to_all | solution.py:84
  131.5 4.0 %reshape.119 = bf16[512,2048]{1,0:T(8,128)(2,1)} reshape(bf16[128,4,2048]{2,1,0:T(4,128)(2,1)} %all-to-all-done.2) | data formatting | bytes 4194304 | tf_op jit(solution)/shard_map/reshape | solution.py:91
  135.5 5.2 %gather_fusion = bf16[256,2048]{1,0:T(8,128)(2,1)} fusion(bf16[512,2048]{1,0:T(8,128)(2,1)} %reshape.119, s32[1024]{0:T(1024)S(1)} %pad_clamp_fusion), kind=kCustom, calls=%fused_computation | custom fusion | bytes 2098176 | tf_op jit(solution)/shard_map/gather | solution.py:92
  140.7 1.7 %reshape.120 = bf16[128,2,2048]{2,1,0:T(2,128)(2,1)S(1)} reshape(bf16[256,2048]{1,0:T(8,128)(2,1)} %gather_fusion) | data formatting | bytes 2097152 | tf_op jit(solution)/shard_map/reshape | solution.py:92
  142.5 0.0 copy-start.2
  142.5 1.5 %fusion.60 = (bf16[128,1,2048]{2,1,0:T(2,128)(2,1)S(1)}, bf16[128,1,2048]{2,1,0:T(2,128)(2,1)S(1)}) fusion(bf16[128,2,2048]{2,1,0:T(2,128)(2,1)S(1)} %reshape.120), kind=kLoop, calls=%fused_computation.114 | loop fusion | bytes 2097152 | tf_op jit(solution)/shard_map/slice | solution.py:95
  144.0 0.0 copy-done.2
  144.0 1.9 %fusion.14 = bf16[128,2048]{1,0:T(8,128)(2,1)} fusion(f32[128,2048]{1,0:T(8,128)S(1)} %copy-done.2, bf16[128,1,2048]{2,1,0:T(2,128)(2,1)S(1)} %get-tuple-element.6, bf16[128,1,2048]{2,1,0:T(2,128)(2,1)S(1)} %get-tuple-element.5, f32[128]{0:T(128)S(1)} %get-tuple-element.39, f32[128]{0:T(128)S(1)} %get-tuple-element.38), kind=kLoop, calls=%fused_computation.15 | loop fusion | flops 1835008 | bytes 2622464 | tf_op jit(solution)/shard_map/convert_element_type | solution.py:97
  (13 shorter events, 0.2 us)
Async XLA Ops:
  0.0 85.5 %copy-start = (bf16[1,512,2048]{2,1,0:T(8,128)(2,1)S(1)}, bf16[1,512,2048]{2,1,0:T(8,128)(2,1)}, u32[]{:S(2)}) copy-start(bf16[1,512,2048]{2,1,0:T(8,128)(2,1)} %param.29) | copy-start | bytes 6291460
  0.0 10.1 %copy-start.5 = (f32[512]{0:T(512)S(1)}, f32[512]{0:T(512)}, u32[]{:S(2)}) copy-start(f32[512]{0:T(512)} %param.18) | copy-start | bytes 6148
  1.4 8.6 %collective-permute-start = (bf16[30,512]{1,0:T(8,128)(2,1)S(1)}, bf16[30,512]{1,0:T(8,128)(2,1)S(1)}, u32[]{:S(2)}, u32[]{:S(2)}) collective-permute-start(bf16[30,512]{1,0:T(8,128)(2,1)S(1)} %slice.281), channel_id=1, source_target_pairs={{0,2},{2,4},{4,6},{6,8},{8,10},{10,12},{12,14},{14,16},{16,18},{18... | collective-permute-start | bytes 92168 | tf_op jit(solution)/shard_map/ppermute | solution.py:15
  12.9 3.0 %copy-start.6 = (f32[512]{0:T(512)S(1)}, f32[512]{0:T(512)}, u32[]{:S(2)}) copy-start(f32[512]{0:T(512)} %param.20) | copy-start | bytes 6148
  12.9 3.0 %copy-start.7 = (f32[512]{0:T(512)S(1)}, f32[512]{0:T(512)}, u32[]{:S(2)}) copy-start(f32[512]{0:T(512)} %param.19) | copy-start | bytes 6148
  15.8 7.0 %copy-start.3 = (bf16[128,2048]{1,0:T(8,128)(2,1)S(1)}, bf16[128,2048]{1,0:T(8,128)(2,1)}, u32[]{:S(2)}) copy-start(bf16[128,2048]{1,0:T(8,128)(2,1)} %param.22) | copy-start | bytes 1572868
  22.9 4.0 %copy-start.4 = (f32[2048]{0:T(1024)S(1)}, f32[2048]{0:T(1024)}, u32[]{:S(2)}) copy-start(f32[2048]{0:T(1024)} %param.23) | copy-start | bytes 24580
  25.9 1.0 copy-start.1
  95.7 5.6 %copy-start.8 = (f32[128,2]{0,1:T(2,128)S(1)}, f32[128,2]{0,1:T(2,128)}, u32[]{:S(2)}) copy-start(f32[128,2]{0,1:T(2,128)} %param.25) | copy-start | bytes 3076
  95.7 5.6 %copy-start.9 = (f32[128]{0:T(128)S(1)}, f32[128]{0:T(128)}, u32[]{:S(2)}) copy-start(f32[128]{0:T(128)} %param.26) | copy-start | bytes 1540
  95.7 35.8 %all-to-all-start.2 = ((bf16[128,4,2048]{2,1,0:T(4,128)(2,1)}), bf16[128,4,2048]{2,1,0:T(4,128)(2,1)}, u32[]{:S(2)}, u32[]{:S(2)}) async-start(bf16[128,4,2048]{2,1,0:T(4,128)(2,1)} %reshape.118), calls=%async_computation.2 | async-start | bytes 4194304 | tf_op jit(solution)/shard_map/all_to_all | solution.py:84
  142.5 1.5 %copy-start.2 = (f32[128,2048]{1,0:T(8,128)S(1)}, f32[128,2048]{1,0:T(8,128)}, u32[]{:S(2)}) copy-start(f32[128,2048]{1,0:T(8,128)} %copy-done.1) | copy-start | bytes 3145732
where the time goes:
time: 147 us; the launch traced here: 146 us
  blocking collectives  45.2 us (31%)
  local copies, waits for them, and re-layouts  37.5 us (26%)
  waiting for transfers between devices  30.2 us (21%)
  matrix products  12.5 us (9%)
  other arithmetic  10.7 us (7%)
  starting transfers between devices  9.52 us (6%)
    all_to_all x1, blocking collectives, local(): lax.all_to_all(outgoing, ('sp', 'tp'), split_axis=0, concat_axis=0, tiled...  40.6 us
    all_to_all x1, waiting for transfers between devices, local(): lax.all_to_all(answer.reshape(senders, slot_count, width_here), ('sp', 't...  30.2 us
    dot_general x1, matrix products, local(): jnp.dot(active, down_weight[0], preferred_element_type=jnp.float32)  6.02 us
    all_to_all x1, starting transfers between devices, local(): lax.all_to_all(answer.reshape(senders, slot_count, width_here), ('sp', 't...  5.59 us
    gather x1, local copies, waits for them, and re-layouts, local(): picked = flat_returned[slot_place].reshape(local_rows, picks, model_width)  5.21 us
    all_to_all x1, blocking collectives, local(): lax.all_to_all(mixed_rows, 'tp', split_axis=0, concat_axis=1, tiled=True)  4.54 us
    scatter x1, local copies, waits for them, and re-layouts, local(): jnp.zeros((experts_all * capacity, model_width), jnp.bfloat16)  4.43 us
    reshape x1, local copies, waits for them, and re-layouts, local(): outgoing = outgoing.reshape(experts_all, capacity, model_width)  4.12 us
  transfers between devices with their start and end apart: 2, of which 1 were waited for; matrix products, arithmetic and copies ran while one was open for 3% of the time, Pallas kernels for 0%

commit v1 on v0

v1 whole, which is shorter than its diff:
```python
import functools
import jax
import jax.numpy as jnp
from jax import lax
from jax.experimental import pallas as pl
from jax.experimental.pallas import tpu as pltpu
from jax.sharding import PartitionSpec as P

EPS = 1e-06
F32 = jnp.float32
BF16 = jnp.bfloat16
HALO = 32
PARTS = 4
LANE = 128
MIB = 1024 * 1024


def iota(shape, axis):
    return lax.broadcasted_iota(jnp.int32, shape, axis)


def onehot(cond):
    return jnp.where(cond, 1.0, 0.0).astype(BF16)


def call(body, out_shape, scratch=(), limit=16, smem=(), n_in=0, flops=0, moved=0, name=None):
    spec = [
        pl.BlockSpec(memory_space=pltpu.SMEM if i in smem else pltpu.VMEM) for i in range(n_in)
    ]
    multi = isinstance(out_shape, (tuple, list))
    outs = [pl.BlockSpec(memory_space=pltpu.VMEM) for _ in out_shape] if multi else pl.BlockSpec(
        memory_space=pltpu.VMEM
    )
    return pl.pallas_call(
        body,
        out_shape=out_shape,
        in_specs=spec,
        out_specs=outs,
        scratch_shapes=list(scratch),
        compiler_params=pltpu.CompilerParams(vmem_limit_bytes=limit * MIB),
        cost_estimate=pl.CostEstimate(flops=flops, bytes_accessed=moved, transcendentals=0),
        name=name,
    )


def route_body(pick, logits, prob, place, cols):
    e_iota = iota((LANE, LANE), 0)
    n_iota = iota((LANE, LANE), 1)
    picks = [pick[k : k + 1, :] for k in range(2)]
    hits = [(e_iota == p).astype(F32) for p in picks]
    both = (hits[0] + hits[1]).astype(BF16)
    before = jnp.dot(both, onehot(e_iota < n_iota), preferred_element_type=F32)
    spots = []
    for k in range(2):
        rank = jnp.sum(before * hits[k], axis=0, keepdims=True)
        spots.append(4 * picks[k] + rank.astype(jnp.int32))
        place[k : k + 1, :] = spots[k]
    first = prob[...] * jax.nn.sigmoid(logits[0:1, :] - logits[1:2, :])
    second = prob[...] * jax.nn.sigmoid(logits[1:2, :] - logits[0:1, :])
    rows = [spots[0].astype(F32), spots[1].astype(F32), first, second]
    table = jnp.zeros((LANE, LANE), F32)
    for i, row in enumerate(rows):
        table = jnp.where(e_iota == i, row, table)
    cols[...] = table.T


def conv_body(me, value, gate, halo, kernel, bias, gain, shift, mine, theirs, ext, taps, mixed):
    n_taps, width = kernel.shape
    length = value.shape[0]
    blocks = width // LANE
    for b in range(blocks):
        lanes = slice(b * LANE, (b + 1) * LANE)
        ext[b, 0:HALO, :] = halo[:, lanes].astype(F32)
        taps[b, 0:n_taps, :] = kernel[:, lanes].astype(F32)
        glued = value[:, lanes].astype(F32) * jax.nn.sigmoid(gate[:, lanes].astype(F32))
        ext[b, HALO : HALO + length, :] = glued.astype(BF16).astype(F32)
    first = HALO - (n_taps - 1)
    chunk = 32

    def block(b, carry):
        lanes = pl.ds(pl.multiple_of(b * LANE, LANE), LANE)
        g, s, c0 = gain[:, lanes], shift[:, lanes], bias[:, lanes]
        for r in range(0, length, chunk):
            acc = jnp.broadcast_to(c0, (chunk, LANE))
            for j in range(n_taps):
                at = r + first + j
                acc = acc + taps[b, j : j + 1, :] * ext[b, at : at + chunk, :]
            centre = jnp.mean(acc, axis=-1, keepdims=True)
            away = acc - centre
            variance = jnp.mean(away * away, axis=-1, keepdims=True)
            v = away * lax.rsqrt(variance + EPS) * g + s
            mixed[r : r + chunk, lanes] = (v / (1.0 + jnp.exp(-v))).astype(BF16)
        return carry

    lax.fori_loop(0, blocks, block, 0)
    half = length // 2
    mine[...] = mixed[pl.ds(pl.multiple_of(me[0] * half, half), half), :]
    theirs[...] = mixed[pl.ds(pl.multiple_of((1 - me[0]) * half, half), half), :]


def slots(stacked, place, out, part):
    tokens = place.shape[1]
    quarter = iota((LANE, tokens), 0) // 2 % PARTS
    for b in range(out.shape[0] // LANE):
        row = iota((LANE, tokens), 0) + b * LANE
        code = row // (2 * PARTS) * 4 + 2 * part + row % 2
        hit = jnp.logical_or(code == place[0:1, :], code == place[1:2, :])
        lhs = jnp.concatenate(
            [onehot(jnp.logical_and(hit, quarter == q)) for q in range(PARTS)], axis=1
        )
        out[b * LANE : (b + 1) * LANE, :] = jnp.dot(
            lhs, stacked[...], preferred_element_type=F32
        ).astype(BF16)


def project_body(me, mine, other, weight, residual, gain, place, hidden, stacked, out):
    half = mine.shape[1]
    width = residual.shape[1]
    tokens = mine.shape[0]
    step = width // PARTS
    here = pl.ds(pl.multiple_of(me[0] * half, half), half)
    there = pl.ds(pl.multiple_of((1 - me[0]) * half, half), half)
    total = jnp.zeros((tokens, 1), F32)
    for q in range(PARTS):
        lanes = slice(q * step, (q + 1) * step)
        acc = jnp.dot(mine[...], weight[here, lanes], preferred_element_type=F32)
        acc = acc + jnp.dot(other[...], weight[there, lanes], preferred_element_type=F32)
        full = (acc + residual[:, lanes].astype(F32)).astype(BF16)
        hidden[:, lanes] = full
        wide = full.astype(F32)
        total = total + jnp.sum(wide * wide, axis=-1, keepdims=True)
    scale = lax.rsqrt(total / width + EPS)
    for q in range(PARTS):
        lanes = slice(q * step, (q + 1) * step)
        stacked[q * tokens : (q + 1) * tokens, :] = (
            hidden[:, lanes].astype(F32) * scale * gain[:, lanes]
        ).astype(BF16)
    slots(stacked, place, out, 0)


def second_body(stacked, place, out):
    slots(stacked, place, out, 1)


def perm(back):
    i, j = iota((LANE, LANE), 0), iota((LANE, LANE), 1)
    if back:
        i, j = j, i
    rows = LANE // PARTS
    return onehot(j == (i % rows) // 2 * (2 * PARTS) + i // rows * 2 + i % 2)


def unpack(message, flat):
    p = perm(False)
    rows = LANE // PARTS
    step = message.shape[1]
    for b in range(message.shape[0] // LANE):
        y = jnp.dot(p, message[b * LANE : (b + 1) * LANE, :], preferred_element_type=F32).astype(BF16)
        for q in range(PARTS):
            flat[b * rows : (b + 1) * rows, q * step : (q + 1) * step] = y[q * rows : (q + 1) * rows]


def expert_body(message, gate, up, down, out, flat, answer):
    unpack(message, flat)
    x = flat[...]
    g = jnp.dot(x, gate[...], preferred_element_type=F32)
    u = jnp.dot(x, up[...], preferred_element_type=F32)
    active = (g / (1.0 + jnp.exp(-g)) * u).astype(BF16)
    answer[...] = jnp.dot(active, down[...], preferred_element_type=F32).astype(BF16)
    p = perm(True)
    rows = LANE // PARTS
    step = out.shape[1]
    for b in range(out.shape[0] // LANE):
        z = jnp.concatenate(
            [answer[b * rows : (b + 1) * rows, q * step : (q + 1) * step] for q in range(PARTS)], axis=0
        )
        out[b * LANE : (b + 1) * LANE, :] = jnp.dot(p, z, preferred_element_type=F32).astype(BF16)


def combine_body(part, message, cols, base, out, flat):
    unpack(message, flat)
    rows = flat.shape[0]
    tokens, width = out.shape
    step = width // PARTS
    slot = iota((tokens, rows), 1)
    code = (slot // 2 * 4 + 2 * part + slot % 2).astype(F32)
    picked = [onehot(cols[:, k : k + 1] == code) for k in range(2)]
    for q in range(PARTS):
        lanes = slice(q * step, (q + 1) * step)
        acc = base[:, lanes].astype(F32)
        for k in range(2):
            acc = acc + cols[:, 2 + k : 3 + k] * jnp.dot(
                picked[k], flat[:, lanes], preferred_element_type=F32
            )
        out[:, lanes] = acc.astype(out.dtype)


def local(
    glu_value,
    glu_gate,
    conv_kernel,
    conv_bias,
    group_gain,
    group_shift,
    out_weight,
    residual,
    ffn_gain,
    expert_pick,
    pair_logits,
    group_prob,
    gate_weight,
    up_weight,
    down_weight,
):
    shape = jax.ShapeDtypeStruct
    length, width = glu_value.shape
    tokens, model = residual.shape
    experts = lax.axis_size("sp") * lax.axis_size("tp")
    peers = lax.axis_size("sp")
    me = lax.axis_index("tp").astype(jnp.int32).reshape(1)

    tail = (
        glu_value[length - HALO :].astype(F32) * jax.nn.sigmoid(glu_gate[length - HALO :].astype(F32))
    ).astype(BF16)
    halo = lax.ppermute(tail, "sp", [(i, i + 1) for i in range(peers - 1)])

    place, cols = call(
        route_body,
        (shape((2, tokens), jnp.int32), shape((tokens, LANE), F32)),
        n_in=3,
        limit=4,
        flops=4_000_000,
        name="route",
    )(expert_pick.T, pair_logits.T, group_prob.reshape(1, tokens))

    mine, theirs = call(
        conv_body,
        (shape((length // 2, width), BF16), shape((length // 2, width), BF16)),
        scratch=(
            pltpu.VMEM((width // LANE, HALO + length, LANE), F32),
            pltpu.VMEM((width // LANE, 32, LANE), F32),
            pltpu.VMEM((length, width), BF16),
        ),
        smem=(0,),
        n_in=8,
        limit=8,
        flops=8_000_000,
        name="conv",
    )(
        me,
        glu_value,
        glu_gate,
        halo,
        conv_kernel,
        conv_bias.reshape(1, width),
        group_gain.reshape(1, width),
        group_shift.reshape(1, width),
    )
    other = lax.ppermute(theirs, "tp", [(0, 1), (1, 0)])

    step = model // PARTS
    rows = experts * 2 * PARTS
    message = shape((rows, step), BF16)
    hidden, stacked, send0 = call(
        project_body,
        (shape((tokens, model), BF16), shape((PARTS * tokens, step), BF16), message),
        smem=(0,),
        n_in=7,
        limit=16,
        flops=1_000_000_000,
        name="project",
    )(me, mine, other, out_weight, residual, ffn_gain.reshape(1, model), place)
    send1 = call(second_body, message, n_in=2, limit=8, flops=500_000_000, name="second")(stacked, place)

    def exchange(x):
        x = x.reshape(experts, 2 * PARTS, step)
        return lax.all_to_all(x, ("sp", "tp"), 0, 0, tiled=True).reshape(rows, step)

    expert = call(
        expert_body,
        message,
        scratch=(pltpu.VMEM((2 * experts, model), BF16), pltpu.VMEM((2 * experts, model), BF16)),
        n_in=4,
        limit=20,
        flops=2_000_000_000,
        name="expert",
    )

    def combine(part, dtype):
        return call(
            functools.partial(combine_body, part),
            shape((tokens, model), dtype),
            scratch=(pltpu.VMEM((2 * experts, model), BF16),),
            n_in=3,
            limit=12,
            flops=1_000_000_000,
            name=f"combine{part}",
        )

    with jax.named_scope("out0"):
        got0 = exchange(send0)
    with jax.named_scope("out1"):
        got1 = exchange(send1)
    done0 = expert(got0, gate_weight[0], up_weight[0], down_weight[0])
    with jax.named_scope("back0"):
        back0 = exchange(done0)
    done1 = expert(got1, gate_weight[0], up_weight[0], down_weight[0])
    with jax.named_scope("back1"):
        back1 = exchange(done1)
    acc = combine(0, F32)(back0, cols, hidden)
    return combine(1, BF16)(back1, cols, acc)


def solution(mesh):
    in_specs = (
        P("sp", "tp"),
        P("sp", "tp"),
        P(None, "tp"),
        P("tp"),
        P("tp"),
        P("tp"),
        P(),
        P(("sp", "tp"), None),
        P(),
        P(("sp", "tp"), None),
        P(("sp", "tp"), None),
        P(("sp", "tp")),
        P(("sp", "tp"), None, None),
        P(("sp", "tp"), None, None),
        P(("sp", "tp"), None, None),
    )
    out_specs = P(("sp", "tp"), None)
    return jax.shard_map(local, mesh=mesh, in_specs=in_specs, out_specs=out_specs, check_vma=False)
```

time: 147 us -> 129 us (0.88)
  blocking collectives: 45.2 us -> 0 us
  waiting for transfers between devices: 30.2 us -> 58.5 us
  starting transfers between devices: 9.52 us -> 30.8 us
  Pallas kernels: 0 us -> 15.3 us
  local copies, waits for them, and re-layouts: 37.5 us -> 22.7 us
  matrix products: 12.5 us -> 0 us
  other arithmetic: 10.7 us -> 0.8 us
    all_to_all x2 -> x0, blocking collectives: 45.2 us -> none  [the longest x1 40.6 us: local(): lax.all_to_all(outgoing, ('sp', 'tp'), split_axis=0, concat_axis=0, tiled...]
    all_to_all x1 -> x4, waiting for transfers between devices: 30.2 us -> 57.5 us  [exchange(): return lax.all_to_all(x, ('sp', 'tp'), 0, 0, tiled=True).reshape(rows, step)]
    unnamed x22 -> x46, local copies, waits for them, and re-layouts: 1.8 us -> 22.7 us
    reshape x7 -> x0, local copies, waits for them, and re-layouts: 20.4 us -> none  [the longest x1 4.12 us: local(): outgoing = outgoing.reshape(experts_all, capacity, model_width)]
    all_to_all x1 -> x4, starting transfers between devices: 5.59 us -> 25.2 us  [exchange(): return lax.all_to_all(x, ('sp', 'tp'), 0, 0, tiled=True).reshape(rows, step)]
    pallas_call x0 -> x8, Pallas kernels: none -> 15.3 us  [the longest x1 4.7 us: local(): done1 = expert(got1, gate_weight[0], up_weight[0], down_weight[0])]
    dot_general x3 -> x0, matrix products: 12.5 us -> none  [the longest x1 6.02 us: local(): jnp.dot(active, down_weight[0], preferred_element_type=jnp.float32)]
    gather x1 -> x0, local copies, waits for them, and re-layouts: 5.21 us -> none  [local(): picked = flat_returned[slot_place].reshape(local_rows, picks, model_width)]
  transfers between devices with their start and end apart: 2 -> 6, of which waited for: 1 -> 5; matrix products, arithmetic and copies ran while one was open for 3% -> 0% of each run, Pallas kernels for 0% -> 7%
where the time goes in v1:
time: 129 us; the launch traced here: 128 us
  waiting for transfers between devices  58.5 us (45%)
  starting transfers between devices  30.8 us (24%)
  local copies, waits for them, and re-layouts  22.7 us (18%)
  Pallas kernels  15.3 us (12%)
    all_to_all x4, waiting for transfers between devices, exchange(): return lax.all_to_all(x, ('sp', 'tp'), 0, 0, tiled=True).reshape(rows, step)  57.5 us
    all_to_all x4, starting transfers between devices, exchange(): return lax.all_to_all(x, ('sp', 'tp'), 0, 0, tiled=True).reshape(rows, step)  25.2 us
    unnamed x46, local copies, waits for them, and re-layouts  22.7 us
    pallas_call x1, Pallas kernels, local(): done1 = expert(got1, gate_weight[0], up_weight[0], down_weight[0])  4.7 us
    ppermute x1, starting transfers between devices, local(): halo = lax.ppermute(tail, 'sp', [(i, i + 1) for i in range(peers - 1)])  3.93 us
    pallas_call x1, Pallas kernels, local(): call(project_body, (shape((tokens, model), BF16), shape((PARTS * tokens,...  2.62 us
  transfers between devices with their start and end apart: 6, of which 5 were waited for; matrix products, arithmetic and copies ran while one was open for 0% of the time, Pallas kernels for 7%

profile of v1, /device:TPU:1, one launch (start us, length us, event | category | flops | bytes accessed | tf_op | source)
XLA Modules:
  0.0 128.3 jit_solution(10020503343457779148)
XLA Ops:
  0.0 0.8 multiply_convert_fusion
  0.8 3.9 %collective-permute-start = (bf16[32,512]{1,0:T(8,128)(2,1)S(1)}, bf16[32,512]{1,0:T(8,128)(2,1)S(1)}, u32[]{:S(2)}, u32[]{:S(2)}) collective-permute-start(bf16[32,512]{1,0:T(8,128)(2,1)S(1)} %multiply_convert_fusion), channel_id=1, source_target_pairs={{0,2},{2,4},{4,6},{6,8},{8,10},{10,12},{12,14},{14,16},{16,18},{18... | collective-permute-start | bytes 98312 | tf_op jit(solution)/shard_map/ppermute | solution.py:225
  4.8 1.0 collective-permute-done.halo
  5.8 0.0 copy-start.9
  5.8 0.9 copy-done.9
  6.7 0.0 copy-start.10
  6.7 0.9 copy-done.10
  7.7 0.0 copy-start.11
  7.7 0.8 copy-done.11
  8.4 0.0 copy-start.13
  8.4 0.7 copy-done.13
  9.1 0.0 copy-start.14
  9.1 0.7 copy-done.14
  9.8 0.0 copy-start.15
  9.8 0.7 copy-done.15
  10.5 2.0 %conv.1 = (bf16[128,512]{1,0:T(8,128)(2,1)S(1)}, bf16[128,512]{1,0:T(8,128)(2,1)S(1)}) custom-call(s32[1]{0:T(128)} %bitcast.me, bf16[256,512]{1,0:T(8,128)(2,1)S(1)} %copy-done.9, bf16[256,512]{1,0:T(8,128)(2,1)S(1)} %copy-done.10, bf16[32,512]{1,0:T(8,128)(2,1)S(1)} %collective-permute-done.halo, bf16[31,512]{1,0:T(8,128)(2,1)S(1)} %copy-done.11, ...), custom_call_target="tpu_custom_call" | custom-call | flops 8000000 | tf_op jit(solution)/shard_map/conv/pallas_call | solution.py:236
  12.4 1.6 %collective-permute-start.1 = (bf16[128,512]{1,0:T(8,128)(2,1)S(1)}, bf16[128,512]{1,0:T(8,128)(2,1)S(1)}, u32[]{:S(2)}, u32[]{:S(2)}) collective-permute-start(bf16[128,512]{1,0:T(8,128)(2,1)S(1)} %get-tuple-element.13), channel_id=1, source_target_pairs={{0,1},{1,0},{2,3},{3,2},{4,5},{5,4},{6,7},{7,6},{8,9},{9,8},{10,11... | collective-permute-start | bytes 393224 | tf_op jit(solution)/shard_map/ppermute | solution.py:259
  14.1 0.0 copy-start.20
  14.1 0.7 copy-done.20
  14.7 0.0 copy-start.21
  14.7 0.7 copy-done.21
  15.4 0.0 copy-start.22
  15.4 0.7 copy-done.22
  16.1 0.3 route.1
  16.3 0.0 collective-permute-done.1.other
  16.3 0.0 copy-start.5
  16.4 2.2 %copy-done.5 = bf16[1024,2048]{1,0:T(8,128)(2,1)S(1)} copy-done((bf16[1024,2048]{1,0:T(8,128)(2,1)S(1)}, bf16[1024,2048]{1,0:T(8,128)(2,1)}, u32[]{:S(2)}) %copy-start.5) | copy-done | bytes 4194328
  18.5 0.0 copy-start.8
  18.5 1.0 copy-done.8
  19.6 0.0 copy-start.12
  19.6 0.7 copy-done.12
  20.3 2.6 %project.1 = (bf16[128,2048]{1,0:T(8,128)(2,1)S(1)}, bf16[512,512]{1,0:T(8,128)(2,1)S(1)}, bf16[1024,512]{1,0:T(8,128)(2,1)}) custom-call(s32[1]{0:T(128)} %bitcast.me, bf16[128,512]{1,0:T(8,128)(2,1)S(1)} %get-tuple-element.12.mine, bf16[128,512]{1,0:T(8,128)(2,1)S(1)} %collective-permute-done.1.other, bf16[1024,2048]{1,0:T(8,128)(2,1)S(1)} %copy-done.5, ...), custom_call_target="tpu_custom_call" | custom-call | flops 1000000000 | tf_op jit(solution)/shard_map/project/pallas_call | solution.py:264
  22.9 0.0 copy-start.16
  22.9 0.8 copy-done.16
  23.7 0.8 copy-done.18
  24.5 10.9 %all-to-all-start.2 = ((bf16[128,8,512]{2,1,0:T(8,128)(2,1)}), bf16[128,8,512]{2,1,0:T(8,128)(2,1)S(1)}, u32[]{:S(2)}, u32[]{:S(2)}) async-start(bf16[128,8,512]{2,1,0:T(8,128)(2,1)} %bitcast.15), calls=%async_computation.2 | async-start | bytes 2097152 | tf_op jit(solution)/shard_map/out0/all_to_all | solution.py:277
  35.4 0.0 copy-start
  35.4 0.0 copy-start.19
  35.4 1.2 copy-done.19
  36.6 0.7 second.1
  37.3 0.0 copy-start.7
  37.4 1.0 copy-done.7
  38.3 16.3 %all-to-all-done.2 = bf16[128,8,512]{2,1,0:T(8,128)(2,1)S(1)} async-done(((bf16[128,8,512]{2,1,0:T(8,128)(2,1)}), bf16[128,8,512]{2,1,0:T(8,128)(2,1)S(1)}, u32[]{:S(2)}, u32[]{:S(2)}) %all-to-all-start.2) | async-done | bytes 1048608 | tf_op jit(solution)/shard_map/out0/all_to_all | solution.py:277
  54.6 5.4 %all-to-all-start = ((bf16[128,8,512]{2,1,0:T(8,128)(2,1)}), bf16[128,8,512]{2,1,0:T(8,128)(2,1)}, u32[]{:S(2)}, u32[]{:S(2)}) async-start(bf16[128,8,512]{2,1,0:T(8,128)(2,1)} %bitcast.29), calls=%async_computation | async-start | bytes 2097152 | tf_op jit(solution)/shard_map/out1/all_to_all | solution.py:277
  60.1 0.0 copy-done
  60.1 0.0 copy-start.1
  60.1 1.6 %copy-done.1 = bf16[1,2048,512]{2,1,0:T(8,128)(2,1)S(1)} copy-done((bf16[1,2048,512]{2,1,0:T(8,128)(2,1)S(1)}, bf16[1,2048,512]{2,1,0:T(8,128)(2,1)}, u32[]{:S(2)}) %copy-start.1) | copy-done | bytes 2097176
  61.7 1.6 %copy-done.3 = bf16[1,512,2048]{2,1,0:T(8,128)(2,1)S(1)} copy-done((bf16[1,512,2048]{2,1,0:T(8,128)(2,1)S(1)}, bf16[1,512,2048]{2,1,0:T(8,128)(2,1)}, u32[]{:S(2)}) %copy-start.3) | copy-done | bytes 2097176
  63.3 2.5 %expert.3 = bf16[1024,512]{1,0:T(8,128)(2,1)S(1)} custom-call(bf16[1024,512]{1,0:T(8,128)(2,1)S(1)} %bitcast.25, bf16[2048,512]{1,0:T(8,128)(2,1)S(1)} %bitcast.19, bf16[2048,512]{1,0:T(8,128)(2,1)S(1)} %bitcast.21, bf16[512,2048]{1,0:T(8,128)(2,1)S(1)} %bitcast.23), custom_call_target="tpu_custom_call" | custom-call | flops 2000000000 | tf_op jit(solution)/shard_map/expert/pallas_call | solution.py:304
  65.8 0.0 copy-start.6
  65.8 1.0 copy-done.6
  66.8 12.3 %all-to-all-done = bf16[128,8,512]{2,1,0:T(8,128)(2,1)} async-done(((bf16[128,8,512]{2,1,0:T(8,128)(2,1)}), bf16[128,8,512]{2,1,0:T(8,128)(2,1)}, u32[]{:S(2)}, u32[]{:S(2)}) %all-to-all-start) | async-done | bytes 1048608 | tf_op jit(solution)/shard_map/out1/all_to_all | solution.py:277
  79.1 4.4 %all-to-all-start.3 = ((bf16[128,8,512]{2,1,0:T(8,128)(2,1)}), bf16[128,8,512]{2,1,0:T(8,128)(2,1)S(1)}, u32[]{:S(2)}, u32[]{:S(2)}) async-start(bf16[128,8,512]{2,1,0:T(8,128)(2,1)} %bitcast.26), calls=%async_computation.3 | async-start | bytes 2097152 | tf_op jit(solution)/shard_map/back0/all_to_all | solution.py:277
  83.5 0.0 copy-start.2
  83.6 1.6 %copy-done.2 = bf16[1,2048,512]{2,1,0:T(8,128)(2,1)S(1)} copy-done((bf16[1,2048,512]{2,1,0:T(8,128)(2,1)S(1)}, bf16[1,2048,512]{2,1,0:T(8,128)(2,1)}, u32[]{:S(2)}) %copy-start.2) | copy-done | bytes 2097176
  85.1 1.6 %copy-done.4 = bf16[1,512,2048]{2,1,0:T(8,128)(2,1)S(1)} copy-done((bf16[1,512,2048]{2,1,0:T(8,128)(2,1)S(1)}, bf16[1,512,2048]{2,1,0:T(8,128)(2,1)}, u32[]{:S(2)}) %copy-start.4) | copy-done | bytes 2097176
  86.7 4.7 %expert.2 = bf16[1024,512]{1,0:T(8,128)(2,1)} custom-call(bf16[1024,512]{1,0:T(8,128)(2,1)} %bitcast.9.message, bf16[2048,512]{1,0:T(8,128)(2,1)S(1)} %bitcast.20, bf16[2048,512]{1,0:T(8,128)(2,1)S(1)} %bitcast.22, bf16[512,2048]{1,0:T(8,128)(2,1)S(1)} %bitcast.24), custom_call_target="tpu_custom_call" | custom-call | flops 2000000000 | tf_op jit(solution)/shard_map/expert/pallas_call | solution.py:307
  91.4 11.4 %all-to-all-done.3 = bf16[128,8,512]{2,1,0:T(8,128)(2,1)S(1)} async-done(((bf16[128,8,512]{2,1,0:T(8,128)(2,1)}), bf16[128,8,512]{2,1,0:T(8,128)(2,1)S(1)}, u32[]{:S(2)}, u32[]{:S(2)}) %all-to-all-start.3) | async-done | bytes 1048608 | tf_op jit(solution)/shard_map/back0/all_to_all | solution.py:277
  102.9 4.4 %all-to-all-start.1 = ((bf16[128,8,512]{2,1,0:T(8,128)(2,1)}), bf16[128,8,512]{2,1,0:T(8,128)(2,1)S(1)}, u32[]{:S(2)}, u32[]{:S(2)}) async-start(bf16[128,8,512]{2,1,0:T(8,128)(2,1)} %bitcast.13), calls=%async_computation.1 | async-start | bytes 2097152 | tf_op jit(solution)/shard_map/back1/all_to_all | solution.py:277
  107.3 0.0 copy-start.17
  107.3 1.0 copy-done.17
  108.3 0.8 combine0.1.base
  109.2 17.4 %all-to-all-done.1 = bf16[128,8,512]{2,1,0:T(8,128)(2,1)S(1)} async-done(((bf16[128,8,512]{2,1,0:T(8,128)(2,1)}), bf16[128,8,512]{2,1,0:T(8,128)(2,1)S(1)}, u32[]{:S(2)}, u32[]{:S(2)}) %all-to-all-start.1) | async-done | bytes 1048608 | tf_op jit(solution)/shard_map/back1/all_to_all | solution.py:277
  126.6 1.6 %combine1.1 = bf16[128,2048]{1,0:T(8,128)(2,1)} custom-call(bf16[1024,512]{1,0:T(8,128)(2,1)S(1)} %bitcast.28, f32[128,128]{1,0:T(8,128)S(1)} %get-tuple-element.16.cols, f32[128,2048]{1,0:T(8,128)S(1)} %combine0.1.base), custom_call_target="tpu_custom_call" | custom-call | flops 1000000000 | tf_op jit(solution)/shard_map/combine1/pallas_call | solution.py:311
  (3 shorter events, 0.0 us)
Async XLA Ops:
  0.8 4.9 %collective-permute-start = (bf16[32,512]{1,0:T(8,128)(2,1)S(1)}, bf16[32,512]{1,0:T(8,128)(2,1)S(1)}, u32[]{:S(2)}, u32[]{:S(2)}) collective-permute-start(bf16[32,512]{1,0:T(8,128)(2,1)S(1)} %multiply_convert_fusion), channel_id=1, source_target_pairs={{0,2},{2,4},{4,6},{6,8},{8,10},{10,12},{12,14},{14,16},{16,18},{18... | collective-permute-start | bytes 98312 | tf_op jit(solution)/shard_map/ppermute | solution.py:225
  5.8 0.9 copy-start.9
  6.7 0.9 copy-start.10
  7.7 0.8 copy-start.11
  8.4 0.7 copy-start.13
  9.1 0.7 copy-start.14
  9.8 0.7 copy-start.15
  12.4 3.9 %collective-permute-start.1 = (bf16[128,512]{1,0:T(8,128)(2,1)S(1)}, bf16[128,512]{1,0:T(8,128)(2,1)S(1)}, u32[]{:S(2)}, u32[]{:S(2)}) collective-permute-start(bf16[128,512]{1,0:T(8,128)(2,1)S(1)} %get-tuple-element.13), channel_id=1, source_target_pairs={{0,1},{1,0},{2,3},{3,2},{4,5},{5,4},{6,7},{7,6},{8,9},{9,8},{10,11... | collective-permute-start | bytes 393224 | tf_op jit(solution)/shard_map/ppermute | solution.py:259
  14.1 0.7 copy-start.20
  14.7 0.7 copy-start.21
  15.4 0.7 copy-start.22
  16.3 2.2 %copy-start.5 = (bf16[1024,2048]{1,0:T(8,128)(2,1)S(1)}, bf16[1024,2048]{1,0:T(8,128)(2,1)}, u32[]{:S(2)}) copy-start(bf16[1024,2048]{1,0:T(8,128)(2,1)} %weight.1) | copy-start | bytes 12582916
  18.5 1.0 copy-start.8
  19.6 0.7 copy-start.12
  22.9 0.8 copy-start.16
  23.7 0.8 copy-start.18
  24.5 30.2 %all-to-all-start.2 = ((bf16[128,8,512]{2,1,0:T(8,128)(2,1)}), bf16[128,8,512]{2,1,0:T(8,128)(2,1)S(1)}, u32[]{:S(2)}, u32[]{:S(2)}) async-start(bf16[128,8,512]{2,1,0:T(8,128)(2,1)} %bitcast.15), calls=%async_computation.2 | async-start | bytes 2097152 | tf_op jit(solution)/shard_map/out0/all_to_all | solution.py:277
  35.4 24.7 %copy-start = (bf16[1,2048,512]{2,1,0:T(8,128)(2,1)S(1)}, bf16[1,2048,512]{2,1,0:T(8,128)(2,1)}, u32[]{:S(2)}) copy-start(bf16[1,2048,512]{2,1,0:T(8,128)(2,1)} %param.27) | copy-start | bytes 6291460
  35.4 1.2 copy-start.19
  37.3 1.0 copy-start.7
  54.6 24.5 %all-to-all-start = ((bf16[128,8,512]{2,1,0:T(8,128)(2,1)}), bf16[128,8,512]{2,1,0:T(8,128)(2,1)}, u32[]{:S(2)}, u32[]{:S(2)}) async-start(bf16[128,8,512]{2,1,0:T(8,128)(2,1)} %bitcast.29), calls=%async_computation | async-start | bytes 2097152 | tf_op jit(solution)/shard_map/out1/all_to_all | solution.py:277
  60.1 1.6 %copy-start.1 = (bf16[1,2048,512]{2,1,0:T(8,128)(2,1)S(1)}, bf16[1,2048,512]{2,1,0:T(8,128)(2,1)}, u32[]{:S(2)}) copy-start(bf16[1,2048,512]{2,1,0:T(8,128)(2,1)} %param.28) | copy-start | bytes 6291460
  61.7 1.6 %copy-start.3 = (bf16[1,512,2048]{2,1,0:T(8,128)(2,1)S(1)}, bf16[1,512,2048]{2,1,0:T(8,128)(2,1)}, u32[]{:S(2)}) copy-start(bf16[1,512,2048]{2,1,0:T(8,128)(2,1)} %param.29) | copy-start | bytes 6291460
  65.8 1.0 copy-start.6
  79.1 23.8 %all-to-all-start.3 = ((bf16[128,8,512]{2,1,0:T(8,128)(2,1)}), bf16[128,8,512]{2,1,0:T(8,128)(2,1)S(1)}, u32[]{:S(2)}, u32[]{:S(2)}) async-start(bf16[128,8,512]{2,1,0:T(8,128)(2,1)} %bitcast.26), calls=%async_computation.3 | async-start | bytes 2097152 | tf_op jit(solution)/shard_map/back0/all_to_all | solution.py:277
  83.5 1.6 %copy-start.2 = (bf16[1,2048,512]{2,1,0:T(8,128)(2,1)S(1)}, bf16[1,2048,512]{2,1,0:T(8,128)(2,1)}, u32[]{:S(2)}) copy-start(bf16[1,2048,512]{2,1,0:T(8,128)(2,1)} %param.28) | copy-start | bytes 6291460
  85.1 1.6 %copy-start.4 = (bf16[1,512,2048]{2,1,0:T(8,128)(2,1)S(1)}, bf16[1,512,2048]{2,1,0:T(8,128)(2,1)}, u32[]{:S(2)}) copy-start(bf16[1,512,2048]{2,1,0:T(8,128)(2,1)} %param.29) | copy-start | bytes 6291460
  102.9 23.8 %all-to-all-start.1 = ((bf16[128,8,512]{2,1,0:T(8,128)(2,1)}), bf16[128,8,512]{2,1,0:T(8,128)(2,1)S(1)}, u32[]{:S(2)}, u32[]{:S(2)}) async-start(bf16[128,8,512]{2,1,0:T(8,128)(2,1)} %bitcast.13), calls=%async_computation.1 | async-start | bytes 2097152 | tf_op jit(solution)/shard_map/back1/all_to_all | solution.py:277
  107.3 1.0 copy-start.17

commit v2 on v1

v2 whole, which is shorter than its diff:
```python
import functools
import jax
import jax.numpy as jnp
from jax import lax
from jax.experimental import pallas as pl
from jax.experimental.pallas import tpu as pltpu
from jax.sharding import PartitionSpec as P

EPS = 1e-06
F32 = jnp.float32
BF16 = jnp.bfloat16
HALO = 32
PARTS = 2
RANKS = 4
LANE = 128
MIB = 1024 * 1024


def iota(shape, axis):
    return lax.broadcasted_iota(jnp.int32, shape, axis)


def onehot(cond):
    return jnp.where(cond, 1.0, 0.0).astype(BF16)


def call(body, out_shape, scratch=(), limit=16, smem=(), hbm=(), n_in=0, out_hbm=(), flops=0, name=None):
    kind = {**dict.fromkeys(smem, pltpu.SMEM), **dict.fromkeys(hbm, pltpu.HBM)}
    n_out = len(out_shape)
    run = pl.pallas_call(
        body,
        out_shape=out_shape,
        in_specs=[pl.BlockSpec(memory_space=kind.get(i, pltpu.VMEM)) for i in range(n_in)],
        out_specs=[
            pl.BlockSpec(memory_space=pltpu.HBM if i in out_hbm else pltpu.VMEM) for i in range(n_out)
        ],
        scratch_shapes=list(scratch),
        compiler_params=pltpu.CompilerParams(vmem_limit_bytes=limit * MIB),
        cost_estimate=pl.CostEstimate(flops=flops, bytes_accessed=0, transcendentals=0),
        name=name,
    )
    return lambda *args: run(
        *(pltpu.with_memory_space_constraint(a, pltpu.HBM) if i in hbm else a for i, a in enumerate(args))
    )


def fetch(sources, targets, sems):
    copies = [
        pltpu.make_async_copy(source, target, sems.at[i])
        for i, (source, target) in enumerate(zip(sources, targets, strict=True))
    ]
    for copy in copies:
        copy.start()
    return copies


def route_body(pick_in, logits_in, prob_in, place, cols, pick, logits, prob, sems):
    for copy in fetch((pick_in, logits_in, prob_in), (pick, logits, prob), sems):
        copy.wait()
    e_iota = iota((LANE, LANE), 0)
    n_iota = iota((LANE, LANE), 1)
    picks = [pick[k : k + 1, :] for k in range(2)]
    hits = [(e_iota == p).astype(F32) for p in picks]
    both = (hits[0] + hits[1]).astype(BF16)
    before = jnp.dot(both, onehot(e_iota < n_iota), preferred_element_type=F32)
    spots = []
    for k in range(2):
        rank = jnp.sum(before * hits[k], axis=0, keepdims=True)
        spots.append(4 * picks[k] + rank.astype(jnp.int32))
        place[k : k + 1, :] = spots[k]
    first = prob[...] * jax.nn.sigmoid(logits[0:1, :] - logits[1:2, :])
    second = prob[...] * jax.nn.sigmoid(logits[1:2, :] - logits[0:1, :])
    rows = [spots[0].astype(F32), spots[1].astype(F32), first, second]
    table = jnp.zeros((LANE, LANE), F32)
    for i, row in enumerate(rows):
        table = jnp.where(e_iota == i, row, table)
    cols[...] = table.T


def taps_and_norm(ext, taps, vecs, b, start, rows, n_taps):
    lanes = pl.ds(pl.multiple_of(b * LANE, LANE), LANE)
    acc = jnp.broadcast_to(vecs[0:1, lanes], (rows, LANE))
    for j in range(n_taps):
        at = start + HALO - (n_taps - 1) + j
        acc = acc + taps[b, j : j + 1, :] * ext[b, at : at + rows, :]
    centre = jnp.mean(acc, axis=-1, keepdims=True)
    away = acc - centre
    variance = jnp.mean(away * away, axis=-1, keepdims=True)
    v = away * lax.rsqrt(variance + EPS) * vecs[1:2, lanes] + vecs[2:3, lanes]
    return (v / (1.0 + jnp.exp(-v))).astype(BF16)


def conv_body(
    value_in, gate_in, kernel_in, bias_in, gain_in, shift_in, weight_in,
    rest, front, taps, vecs, weight,
    value, gate, kernel, ext, sems,
):
    n_taps, width = kernel.shape
    length = value.shape[0]
    blocks = width // LANE
    *small, large = fetch(
        (kernel_in, bias_in, gain_in, shift_in, value_in, gate_in, weight_in),
        (kernel, vecs.at[0:1], vecs.at[1:2], vecs.at[2:3], value, gate, weight),
        sems,
    )
    for copy in small:
        copy.wait()
    for b in range(blocks):
        lanes = slice(b * LANE, (b + 1) * LANE)
        taps[b, 0:n_taps, :] = kernel[:, lanes].astype(F32)
        glued = value[:, lanes].astype(F32) * jax.nn.sigmoid(gate[:, lanes].astype(F32))
        ext[b, HALO : HALO + length, :] = glued.astype(BF16).astype(F32)
        front[b, :, :] = ext[b, HALO : 2 * HALO, :]

    def block(b, carry):
        lanes = pl.ds(pl.multiple_of(b * LANE, LANE), LANE)
        for r in range(HALO, length, HALO):
            rest[r : r + HALO, lanes] = taps_and_norm(ext, taps, vecs, b, r, HALO, n_taps)
        return carry

    lax.fori_loop(0, blocks, block, 0)
    large.wait()


def head_body(me, rest, front, taps, vecs, halo, mine, theirs, ext, mixed):
    n_taps = 31
    blocks, _, _ = front.shape
    half = mine.shape[0]
    for b in range(blocks):
        lanes = slice(b * LANE, (b + 1) * LANE)
        ext[b, 0:HALO, :] = halo[:, lanes].astype(F32)
        ext[b, HALO : 2 * HALO, :] = front[b, :, :]
    for b in range(blocks):
        lanes = slice(b * LANE, (b + 1) * LANE)
        mixed[:, lanes] = taps_and_norm(ext, taps, vecs, b, 0, HALO, n_taps)

    @pl.when(me[0] == 0)
    def _():
        mine[0:HALO, :] = mixed[...]
        mine[HALO:half, :] = rest[HALO:half, :]
        theirs[...] = rest[half : 2 * half, :]

    @pl.when(me[0] != 0)
    def _():
        theirs[0:HALO, :] = mixed[...]
        theirs[HALO:half, :] = rest[HALO:half, :]
        mine[...] = rest[half : 2 * half, :]


def slots(stacked, place, out):
    tokens = place.shape[1]
    part = iota((LANE, tokens), 0) // RANKS % PARTS
    for b in range(out.shape[0] // LANE):
        row = iota((LANE, tokens), 0) + b * LANE
        code = row // (RANKS * PARTS) * RANKS + row % RANKS
        hit = jnp.logical_or(code == place[0:1, :], code == place[1:2, :])
        lhs = jnp.concatenate(
            [onehot(jnp.logical_and(hit, part == q)) for q in range(PARTS)], axis=1
        )
        out[b * LANE : (b + 1) * LANE, :] = jnp.dot(
            lhs, stacked[...], preferred_element_type=F32
        ).astype(BF16)


def project_body(me, mine, other, weight, residual, gain, place, hidden, out, stacked):
    half = mine.shape[1]
    width = residual.shape[1]
    tokens = mine.shape[0]
    step = width // PARTS
    here = pl.ds(pl.multiple_of(me[0] * half, half), half)
    there = pl.ds(pl.multiple_of((1 - me[0]) * half, half), half)
    total = jnp.zeros((tokens, 1), F32)
    for q in range(PARTS):
        lanes = slice(q * step, (q + 1) * step)
        acc = jnp.dot(mine[...], weight[here, lanes], preferred_element_type=F32)
        acc = acc + jnp.dot(other[...], weight[there, lanes], preferred_element_type=F32)
        full = (acc + residual[:, lanes].astype(F32)).astype(BF16)
        hidden[:, lanes] = full
        wide = full.astype(F32)
        total = total + jnp.sum(wide * wide, axis=-1, keepdims=True)
    scale = lax.rsqrt(total / width + EPS)
    for q in range(PARTS):
        lanes = slice(q * step, (q + 1) * step)
        stacked[q * tokens : (q + 1) * tokens, :] = (
            hidden[:, lanes].astype(F32) * scale * gain[:, lanes]
        ).astype(BF16)
    slots(stacked, place, out)


def perm(back):
    i, j = iota((LANE, LANE), 0), iota((LANE, LANE), 1)
    if back:
        i, j = j, i
    rows = LANE // PARTS
    return onehot(j == (i % rows) // RANKS * (RANKS * PARTS) + i // rows * RANKS + i % RANKS)


def unpack(message, flat):
    p = perm(False)
    rows = LANE // PARTS
    step = message.shape[1]
    for b in range(message.shape[0] // LANE):
        y = jnp.dot(p, message[b * LANE : (b + 1) * LANE, :], preferred_element_type=F32).astype(BF16)
        for q in range(PARTS):
            flat[b * rows : (b + 1) * rows, q * step : (q + 1) * step] = y[q * rows : (q + 1) * rows]


def expert_body(message, gate, up, down, out, flat, answer):
    unpack(message, flat)
    x = flat[...]
    g = jnp.dot(x, gate[...], preferred_element_type=F32)
    u = jnp.dot(x, up[...], preferred_element_type=F32)
    active = (g / (1.0 + jnp.exp(-g)) * u).astype(BF16)
    answer[...] = jnp.dot(active, down[...], preferred_element_type=F32).astype(BF16)
    p = perm(True)
    rows = LANE // PARTS
    step = out.shape[1]
    for b in range(out.shape[0] // LANE):
        z = jnp.concatenate(
            [answer[b * rows : (b + 1) * rows, q * step : (q + 1) * step] for q in range(PARTS)], axis=0
        )
        out[b * LANE : (b + 1) * LANE, :] = jnp.dot(p, z, preferred_element_type=F32).astype(BF16)


def combine_body(message, cols, base, out, flat):
    unpack(message, flat)
    rows = flat.shape[0]
    tokens, width = out.shape
    step = width // 4
    code = iota((tokens, rows), 1).astype(F32)
    picked = [onehot(cols[:, k : k + 1] == code) for k in range(2)]
    for q in range(4):
        lanes = slice(q * step, (q + 1) * step)
        acc = base[:, lanes].astype(F32)
        for k in range(2):
            acc = acc + cols[:, 2 + k : 3 + k] * jnp.dot(
                picked[k], flat[:, lanes], preferred_element_type=F32
            )
        out[:, lanes] = acc.astype(out.dtype)


def local(
    glu_value,
    glu_gate,
    conv_kernel,
    conv_bias,
    group_gain,
    group_shift,
    out_weight,
    residual,
    ffn_gain,
    expert_pick,
    pair_logits,
    group_prob,
    gate_weight,
    up_weight,
    down_weight,
):
    shape = jax.ShapeDtypeStruct
    length, width = glu_value.shape
    tokens, model = residual.shape
    experts = lax.axis_size("sp") * lax.axis_size("tp")
    peers = lax.axis_size("sp")
    me = lax.axis_index("tp").astype(jnp.int32).reshape(1)

    tail = (
        glu_value[length - HALO :].astype(F32) * jax.nn.sigmoid(glu_gate[length - HALO :].astype(F32))
    ).astype(BF16)
    halo = lax.ppermute(tail, "sp", [(i, i + 1) for i in range(peers - 1)])

    n_taps = conv_kernel.shape[0]
    blocks = width // LANE
    rest, front, taps, vecs, weight = call(
        conv_body,
        (
            shape((length, width), BF16),
            shape((blocks, HALO, LANE), F32),
            shape((blocks, 32, LANE), F32),
            shape((8, width), F32),
            shape(out_weight.shape, BF16),
        ),
        scratch=(
            pltpu.VMEM((length, width), BF16),
            pltpu.VMEM((length, width), BF16),
            pltpu.VMEM((n_taps, width), BF16),
            pltpu.VMEM((blocks, HALO + length, LANE), F32),
            pltpu.SemaphoreType.DMA((7,)),
        ),
        hbm=range(7),
        n_in=7,
        limit=8,
        flops=3_000_000_000,
        name="conv",
    )(
        glu_value,
        glu_gate,
        conv_kernel,
        conv_bias.reshape(1, width),
        group_gain.reshape(1, width),
        group_shift.reshape(1, width),
        out_weight,
    )
    mine, theirs = call(
        head_body,
        (shape((length // 2, width), BF16), shape((length // 2, width), BF16)),
        scratch=(pltpu.VMEM((blocks, 2 * HALO, LANE), F32), pltpu.VMEM((HALO, width), BF16)),
        smem=(0,),
        n_in=6,
        limit=4,
        flops=500_000_000,
        name="head",
    )(me, rest, front, taps, vecs, halo)
    place, cols = call(
        route_body,
        (shape((2, tokens), jnp.int32), shape((tokens, LANE), F32)),
        scratch=(
            pltpu.VMEM((2, tokens), jnp.int32),
            pltpu.VMEM((2, tokens), F32),
            pltpu.VMEM((1, tokens), F32),
            pltpu.SemaphoreType.DMA((3,)),
        ),
        hbm=range(3),
        n_in=3,
        limit=4,
        flops=500_000_000,
        name="route",
    )(expert_pick.T, pair_logits.T, group_prob.reshape(1, tokens))
    other = lax.ppermute(theirs, "tp", [(0, 1), (1, 0)])

    step = model // PARTS
    rows = experts * RANKS * PARTS
    message = shape((rows, step), BF16)
    flat = pltpu.VMEM((RANKS * experts, model), BF16)
    hidden, send = call(
        project_body,
        (shape((tokens, model), BF16), message),
        scratch=(pltpu.VMEM((PARTS * tokens, step), BF16),),
        smem=(0,),
        n_in=7,
        limit=16,
        flops=1_000_000_000,
        name="project",
    )(me, mine, other, weight, residual, ffn_gain.reshape(1, model), place)

    def exchange(x):
        x = x.reshape(experts, RANKS * PARTS, step)
        return lax.all_to_all(x, ("sp", "tp"), 0, 0, tiled=True).reshape(rows, step)

    got = exchange(send)
    (done,) = call(
        expert_body,
        (message,),
        scratch=(flat, flat),
        n_in=4,
        limit=24,
        flops=4_000_000_000,
        name="expert",
    )(got, gate_weight[0], up_weight[0], down_weight[0])
    back = exchange(done)
    (result,) = call(
        combine_body,
        (shape((tokens, model), BF16),),
        scratch=(flat,),
        n_in=3,
        limit=12,
        flops=1_000_000_000,
        name="combine",
    )(back, cols, hidden)
    return result


def solution(mesh):
    in_specs = (
        P("sp", "tp"),
        P("sp", "tp"),
        P(None, "tp"),
        P("tp"),
        P("tp"),
        P("tp"),
        P(),
        P(("sp", "tp"), None),
        P(),
        P(("sp", "tp"), None),
        P(("sp", "tp"), None),
        P(("sp", "tp")),
        P(("sp", "tp"), None, None),
        P(("sp", "tp"), None, None),
        P(("sp", "tp"), None, None),
    )
    out_specs = P(("sp", "tp"), None)
    return jax.shard_map(local, mesh=mesh, in_specs=in_specs, out_specs=out_specs, check_vma=False)
```

time: 129 us -> 97.6 us (0.76)
  blocking collectives: 0 us -> 74.7 us
  waiting for transfers between devices: 58.5 us -> 0.01 us
  starting transfers between devices: 30.8 us -> 4.96 us
  local copies, waits for them, and re-layouts: 22.7 us -> 4.15 us
  Pallas kernels: 15.3 us -> 12.6 us
    all_to_all x0 -> x2, blocking collectives: none -> 74.7 us  [exchange(): return lax.all_to_all(x, ('sp', 'tp'), 0, 0, tiled=True).reshape(rows, step)]
    all_to_all x4 -> x0, waiting for transfers between devices: 57.5 us -> none  [exchange(): return lax.all_to_all(x, ('sp', 'tp'), 0, 0, tiled=True).reshape(rows, step)]
    all_to_all x4 -> x0, starting transfers between devices: 25.2 us -> none  [exchange(): return lax.all_to_all(x, ('sp', 'tp'), 0, 0, tiled=True).reshape(rows, step)]
    unnamed x46 -> x14, local copies, waits for them, and re-layouts: 22.7 us -> 4.15 us
    pallas_call x8 -> x6, Pallas kernels: 15.3 us -> 12.6 us  [call(): run(*(pltpu.with_memory_space_constraint(a, pltpu.HBM) if i in hbm else a...]
  transfers between devices with their start and end apart: 6 -> 2, of which waited for: 5 -> 0; matrix products, arithmetic and copies ran while one was open for 0% -> 0% of each run, Pallas kernels for 7% -> 4%
where the time goes in v2:
time: 97.6 us; the launch traced here: 97.3 us
  blocking collectives  74.7 us (77%)
  Pallas kernels  12.6 us (13%)
  starting transfers between devices  4.96 us (5%)
  local copies, waits for them, and re-layouts  4.15 us (4%)
    all_to_all x2, blocking collectives, exchange(): return lax.all_to_all(x, ('sp', 'tp'), 0, 0, tiled=True).reshape(rows, step)  74.7 us
    pallas_call x6, Pallas kernels, call(): run(*(pltpu.with_memory_space_constraint(a, pltpu.HBM) if i in hbm else a...  12.6 us
    unnamed x14, local copies, waits for them, and re-layouts  4.15 us
    ppermute x1, starting transfers between devices, local(): halo = lax.ppermute(tail, 'sp', [(i, i + 1) for i in range(peers - 1)])  3.93 us
  transfers between devices with their start and end apart: 2, of which 0 were waited for; matrix products, arithmetic and copies ran while one was open for 0% of the time, Pallas kernels for 4%

profile of v2, /device:TPU:1, one launch (start us, length us, event | category | flops | bytes accessed | tf_op | source)
XLA Modules:
  0.0 97.3 jit_solution(9538527934038311078)
XLA Ops:
  0.0 0.8 multiply_convert_fusion
  0.8 3.9 %collective-permute-start = (bf16[32,512]{1,0:T(8,128)(2,1)S(1)}, bf16[32,512]{1,0:T(8,128)(2,1)S(1)}, u32[]{:S(2)}, u32[]{:S(2)}) collective-permute-start(bf16[32,512]{1,0:T(8,128)(2,1)S(1)} %multiply_convert_fusion), channel_id=1, source_target_pairs={{0,2},{2,4},{4,6},{6,8},{8,10},{10,12},{12,14},{14,16},{16,18},{18... | collective-permute-start | bytes 98312 | tf_op jit(solution)/shard_map/ppermute | solution.py:269
  4.8 3.0 %conv.1 = (bf16[256,512]{1,0:T(8,128)(2,1)S(1)}, f32[4,32,128]{2,1,0:T(8,128)S(1)}, f32[4,32,128]{2,1,0:T(8,128)S(1)}, f32[8,512]{1,0:T(8,128)S(1)}, bf16[1024,2048]{1,0:T(8,128)(2,1)S(1)}) custom-call(bf16[256,512]{1,0:T(8,128)(2,1)} %value_in.1, bf16[256,512]{1,0:T(8,128)(2,1)} %gate_in.1, bf16[31,512]{1,0:T(8,128)(2,1)} %kernel_in.1, f32[1,512]{1,0:T(1,128)} %bitcast.23, ...), custom_call_target="tpu_custom_call" | custom-call | flops 3000000000 | tf_op jit(solution)/shard_map/conv/pallas_call | solution.py:42
  7.8 0.0 copy-start
  7.8 1.9 %copy-done = bf16[1024,2048]{1,0:T(8,128)(2,1)} copy-done((bf16[1024,2048]{1,0:T(8,128)(2,1)}, bf16[1024,2048]{1,0:T(8,128)(2,1)S(1)}, u32[]{:S(2)}) %copy-start) | copy-done | bytes 4194328
  9.7 0.0 copy-start.2
  9.7 0.0 copy-start.3
  9.7 0.0 collective-permute-done.halo
  9.7 0.4 head.1
  10.1 1.0 %collective-permute-start.1 = (bf16[128,512]{1,0:T(8,128)(2,1)S(1)}, bf16[128,512]{1,0:T(8,128)(2,1)S(1)}, u32[]{:S(2)}, u32[]{:S(2)}) collective-permute-start(bf16[128,512]{1,0:T(8,128)(2,1)S(1)} %get-tuple-element.21), channel_id=1, source_target_pairs={{0,1},{1,0},{2,3},{3,2},{4,5},{5,4},{6,7},{7,6},{8,9},{9,8},{10,11... | collective-permute-start | bytes 393224 | tf_op jit(solution)/shard_map/ppermute | solution.py:328
  11.1 1.0 %route.1 = (s32[2,128]{1,0:T(2,128)S(1)}, f32[128,128]{1,0:T(8,128)S(1)}) custom-call(s32[2,128]{1,0:T(2,128)} %bitcast.26, f32[2,128]{1,0:T(2,128)} %bitcast.27, f32[1,128]{1,0:T(1,128)} %bitcast.28), custom_call_target="tpu_custom_call" | custom-call | flops 500000000 | tf_op jit(solution)/shard_map/route/pallas_call | solution.py:42
  12.1 0.0 collective-permute-done.1.other
  12.1 0.0 copy-done.2
  12.1 0.0 copy-done.3
  12.1 0.0 copy-start.1
  12.2 2.2 %copy-done.1 = bf16[1024,2048]{1,0:T(8,128)(2,1)S(1)} copy-done((bf16[1024,2048]{1,0:T(8,128)(2,1)S(1)}, bf16[1024,2048]{1,0:T(8,128)(2,1)}, u32[]{:S(2)}) %copy-start.1) | copy-done | bytes 4194328
  14.3 0.0 copy-start.6
  14.3 1.6 %project.1 = (bf16[128,2048]{1,0:T(8,128)(2,1)S(1)}, bf16[1024,1024]{1,0:T(8,128)(2,1)S(1)}) custom-call(s32[1]{0:T(128)} %bitcast.me, bf16[128,512]{1,0:T(8,128)(2,1)S(1)} %get-tuple-element.20.mine, bf16[128,512]{1,0:T(8,128)(2,1)S(1)} %collective-permute-done.1.other, bf16[1024,2048]{1,0:T(8,128)(2,1)S(1)} %copy-done.1, bf16[128,2048]{1,0:T(8,128)(2,1)S(1)} %copy-done.2, ...), custom_call_target="tpu_custom_call" | custom-call | flops 1000000000 | tf_op jit(solution)/shard_map/project/pallas_call | solution.py:42
  16.0 0.0 copy-start.4
  16.0 0.0 copy-start.5
  16.0 40.3 %all_to_all.10 = bf16[128,8,1024]{2,1,0:T(8,128)(2,1)S(1)} all-to-all(bf16[128,8,1024]{2,1,0:T(8,128)(2,1)S(1)} %bitcast.15), channel_id=1, replica_groups=mesh['sp'=64,'tp'=2] {'sp','tp'}, dimensions={0} | all-to-all | bytes 4194304 | tf_op jit(solution)/shard_map/all_to_all | solution.py:347
  56.3 0.0 copy-done.6
  56.3 0.0 copy-done.4
  56.3 0.0 copy-done.5
  56.3 4.5 %expert.1 = bf16[1024,1024]{1,0:T(8,128)(2,1)S(1)} custom-call(bf16[1024,1024]{1,0:T(8,128)(2,1)S(1)} %bitcast.17, bf16[2048,512]{1,0:T(8,128)(2,1)S(1)} %bitcast.20, bf16[2048,512]{1,0:T(8,128)(2,1)S(1)} %bitcast.21, bf16[512,2048]{1,0:T(8,128)(2,1)S(1)} %bitcast.22), custom_call_target="tpu_custom_call" | custom-call | flops 4000000000 | tf_op jit(solution)/shard_map/expert/pallas_call | solution.py:42
  60.8 34.4 %all_to_all.11 = bf16[128,8,1024]{2,1,0:T(8,128)(2,1)S(1)} all-to-all(bf16[128,8,1024]{2,1,0:T(8,128)(2,1)S(1)} %bitcast.18), channel_id=1, replica_groups=mesh['sp'=64,'tp'=2] {'sp','tp'}, dimensions={0} | all-to-all | bytes 4194304 | tf_op jit(solution)/shard_map/all_to_all | solution.py:347
  95.2 2.1 %combine.1 = bf16[128,2048]{1,0:T(8,128)(2,1)} custom-call(bf16[1024,1024]{1,0:T(8,128)(2,1)S(1)} %bitcast.16, f32[128,128]{1,0:T(8,128)S(1)} %get-tuple-element.25.cols, bf16[128,2048]{1,0:T(8,128)(2,1)S(1)} %get-tuple-element.26.base), custom_call_target="tpu_custom_call" | custom-call | flops 1000000000 | tf_op jit(solution)/shard_map/combine/pallas_call | solution.py:42
Async XLA Ops:
  0.8 8.9 %collective-permute-start = (bf16[32,512]{1,0:T(8,128)(2,1)S(1)}, bf16[32,512]{1,0:T(8,128)(2,1)S(1)}, u32[]{:S(2)}, u32[]{:S(2)}) collective-permute-start(bf16[32,512]{1,0:T(8,128)(2,1)S(1)} %multiply_convert_fusion), channel_id=1, source_target_pairs={{0,2},{2,4},{4,6},{6,8},{8,10},{10,12},{12,14},{14,16},{16,18},{18... | collective-permute-start | bytes 98312 | tf_op jit(solution)/shard_map/ppermute | solution.py:269
  7.8 2.0 %copy-start = (bf16[1024,2048]{1,0:T(8,128)(2,1)}, bf16[1024,2048]{1,0:T(8,128)(2,1)S(1)}, u32[]{:S(2)}) copy-start(bf16[1024,2048]{1,0:T(8,128)(2,1)S(1)} %get-tuple-element.22.weight) | copy-start | bytes 12582916
  9.7 2.4 %copy-start.2 = (bf16[128,2048]{1,0:T(8,128)(2,1)S(1)}, bf16[128,2048]{1,0:T(8,128)(2,1)}, u32[]{:S(2)}) copy-start(bf16[128,2048]{1,0:T(8,128)(2,1)} %residual.1) | copy-start | bytes 1572868
  9.7 2.4 %copy-start.3 = (f32[2048]{0:T(1024)S(1)}, f32[2048]{0:T(1024)}, u32[]{:S(2)}) copy-start(f32[2048]{0:T(1024)} %param.23) | copy-start | bytes 24580
  10.1 2.0 %collective-permute-start.1 = (bf16[128,512]{1,0:T(8,128)(2,1)S(1)}, bf16[128,512]{1,0:T(8,128)(2,1)S(1)}, u32[]{:S(2)}, u32[]{:S(2)}) collective-permute-start(bf16[128,512]{1,0:T(8,128)(2,1)S(1)} %get-tuple-element.21), channel_id=1, source_target_pairs={{0,1},{1,0},{2,3},{3,2},{4,5},{5,4},{6,7},{7,6},{8,9},{9,8},{10,11... | collective-permute-start | bytes 393224 | tf_op jit(solution)/shard_map/ppermute | solution.py:328
  12.1 2.2 %copy-start.1 = (bf16[1024,2048]{1,0:T(8,128)(2,1)S(1)}, bf16[1024,2048]{1,0:T(8,128)(2,1)}, u32[]{:S(2)}) copy-start(bf16[1024,2048]{1,0:T(8,128)(2,1)} %copy-done) | copy-start | bytes 12582916
  14.3 42.0 %copy-start.6 = (bf16[1,512,2048]{2,1,0:T(8,128)(2,1)S(1)}, bf16[1,512,2048]{2,1,0:T(8,128)(2,1)}, u32[]{:S(2)}) copy-start(bf16[1,512,2048]{2,1,0:T(8,128)(2,1)} %param.29) | copy-start | bytes 6291460
  16.0 40.3 %copy-start.4 = (bf16[1,2048,512]{2,1,0:T(8,128)(2,1)S(1)}, bf16[1,2048,512]{2,1,0:T(8,128)(2,1)}, u32[]{:S(2)}) copy-start(bf16[1,2048,512]{2,1,0:T(8,128)(2,1)} %param.27) | copy-start | bytes 6291460
  16.0 40.3 %copy-start.5 = (bf16[1,2048,512]{2,1,0:T(8,128)(2,1)S(1)}, bf16[1,2048,512]{2,1,0:T(8,128)(2,1)}, u32[]{:S(2)}) copy-start(bf16[1,2048,512]{2,1,0:T(8,128)(2,1)} %param.28) | copy-start | bytes 6291460

commit v3 on v2

--- a/solution.py
+++ b/solution.py
@@ -91,7 +91,7 @@
 
 
 def conv_body(
-    value_in, gate_in, kernel_in, bias_in, gain_in, shift_in, weight_in,
+    _, value_in, gate_in, kernel_in, bias_in, gain_in, shift_in, weight_in,
     rest, front, taps, vecs, weight,
     value, gate, kernel, ext, sems,
 ):
@@ -128,7 +128,7 @@
     half = mine.shape[0]
     for b in range(blocks):
         lanes = slice(b * LANE, (b + 1) * LANE)
-        ext[b, 0:HALO, :] = halo[:, lanes].astype(F32)
+        ext[b, 0:HALO, :] = jnp.where(me[1] > 0, halo[:, lanes].astype(F32), 0.0)
         ext[b, HALO : 2 * HALO, :] = front[b, :, :]
     for b in range(blocks):
         lanes = slice(b * LANE, (b + 1) * LANE)
@@ -261,12 +261,12 @@
     tokens, model = residual.shape
     experts = lax.axis_size("sp") * lax.axis_size("tp")
     peers = lax.axis_size("sp")
-    me = lax.axis_index("tp").astype(jnp.int32).reshape(1)
+    me = jnp.stack([lax.axis_index("tp"), lax.axis_index("sp")]).astype(jnp.int32)
 
     tail = (
         glu_value[length - HALO :].astype(F32) * jax.nn.sigmoid(glu_gate[length - HALO :].astype(F32))
     ).astype(BF16)
-    halo = lax.ppermute(tail, "sp", [(i, i + 1) for i in range(peers - 1)])
+    halo = lax.ppermute(tail, "sp", [(i, (i + 1) % peers) for i in range(peers)])
 
     n_taps = conv_kernel.shape[0]
     blocks = width // LANE
@@ -286,12 +286,14 @@
             pltpu.VMEM((blocks, HALO + length, LANE), F32),
             pltpu.SemaphoreType.DMA((7,)),
         ),
-        hbm=range(7),
-        n_in=7,
+        smem=(0,),
+        hbm=range(1, 8),
+        n_in=8,
         limit=8,
         flops=3_000_000_000,
         name="conv",
     )(
+        me,
         glu_value,
         glu_gate,
         conv_kernel,

time: 97.6 us -> 93.3 us (0.956)
  blocking collectives: 74.7 us -> 69.2 us
  waiting for transfers between devices: 0.01 us -> 4.87 us
  local copies, waits for them, and re-layouts: 4.15 us -> 0.03 us
  Pallas kernels: 12.6 us -> 14.3 us
  starting transfers between devices: 4.96 us -> 3.71 us
    all_to_all x2, blocking collectives: 74.7 us -> 69.2 us  [exchange(): return lax.all_to_all(x, ('sp', 'tp'), 0, 0, tiled=True).reshape(rows, step)]
    ppermute x1, waiting for transfers between devices: 0.01 us -> 4.86 us  [local(): lax.ppermute(tail, 'sp', [(i, (i + 1) % peers) for i in range(peers)])]
    unnamed x14 -> x10, local copies, waits for them, and re-layouts: 4.15 us -> 0.03 us
    ppermute x1, starting transfers between devices: 3.93 us -> 2.1 us  [local(): lax.ppermute(tail, 'sp', [(i, (i + 1) % peers) for i in range(peers)])]
    pallas_call x6, Pallas kernels: 12.6 us -> 14.3 us  [call(): run(*(pltpu.with_memory_space_constraint(a, pltpu.HBM) if i in hbm else a...]
  transfers between devices with their start and end apart: 2 -> 2, of which waited for: 0 -> 1; matrix products, arithmetic and copies ran while one was open for 0% -> 0% of each run, Pallas kernels for 4% -> 5%
where the time goes in v3:
time: 93.3 us; the launch traced here: 93.1 us
  blocking collectives  69.2 us (74%)
  Pallas kernels  14.3 us (15%)
  waiting for transfers between devices  4.87 us (5%)
  starting transfers between devices  3.71 us (4%)
    all_to_all x2, blocking collectives, exchange(): return lax.all_to_all(x, ('sp', 'tp'), 0, 0, tiled=True).reshape(rows, step)  69.2 us
    pallas_call x6, Pallas kernels, call(): run(*(pltpu.with_memory_space_constraint(a, pltpu.HBM) if i in hbm else a...  14.3 us
    ppermute x1, waiting for transfers between devices, local(): lax.ppermute(tail, 'sp', [(i, (i + 1) % peers) for i in range(peers)])  4.86 us
    ppermute x1, starting transfers between devices, local(): lax.ppermute(tail, 'sp', [(i, (i + 1) % peers) for i in range(peers)])  2.1 us
  transfers between devices with their start and end apart: 2, of which 1 were waited for; matrix products, arithmetic and copies ran while one was open for 0% of the time, Pallas kernels for 5%

profile of v3, /device:TPU:1, one launch (start us, length us, event | category | flops | bytes accessed | tf_op | source)
XLA Modules:
  0.0 93.1 jit_solution(16155286839638578337)
XLA Ops:
  0.0 0.8 multiply_convert_fusion
  0.8 2.1 %collective-permute-start = (bf16[32,512]{1,0:T(8,128)(2,1)S(1)}, bf16[32,512]{1,0:T(8,128)(2,1)S(1)}, u32[]{:S(2)}, u32[]{:S(2)}) collective-permute-start(bf16[32,512]{1,0:T(8,128)(2,1)S(1)} %multiply_convert_fusion), channel_id=1, source_target_pairs={{0,2},{2,4},{4,6},{6,8},{8,10},{10,12},{12,14},{14,16},{16,18},{18... | collective-permute-start | bytes 98312 | tf_op jit(solution)/shard_map/ppermute | solution.py:269
  2.9 0.1 pad_add_fusion._.me
  3.0 3.5 %conv.1 = (bf16[256,512]{1,0:T(8,128)(2,1)S(1)}, f32[4,32,128]{2,1,0:T(8,128)S(1)}, f32[4,32,128]{2,1,0:T(8,128)S(1)}, f32[8,512]{1,0:T(8,128)S(1)}, bf16[1024,2048]{1,0:T(8,128)(2,1)S(1)}) custom-call(s32[2]{0:T(128)S(1)} %pad_add_fusion._.me, bf16[256,512]{1,0:T(8,128)(2,1)} %value_in.1, bf16[256,512]{1,0:T(8,128)(2,1)} %gate_in.1, ...), custom_call_target="tpu_custom_call" | custom-call | flops 3000000000 | tf_op jit(solution)/shard_map/conv/pallas_call | solution.py:42
  6.5 0.0 copy-start
  6.5 0.0 copy-start.1
  6.5 4.9 %collective-permute-done.halo = bf16[32,512]{1,0:T(8,128)(2,1)S(1)} collective-permute-done((bf16[32,512]{1,0:T(8,128)(2,1)S(1)}, bf16[32,512]{1,0:T(8,128)(2,1)S(1)}, u32[]{:S(2)}, u32[]{:S(2)}) %collective-permute-start) | collective-permute-done | bytes 32800 | tf_op jit(solution)/shard_map/ppermute | solution.py:269
  11.4 0.9 head.1
  12.3 1.6 %collective-permute-start.1 = (bf16[128,512]{1,0:T(8,128)(2,1)S(1)}, bf16[128,512]{1,0:T(8,128)(2,1)S(1)}, u32[]{:S(2)}, u32[]{:S(2)}) collective-permute-start(bf16[128,512]{1,0:T(8,128)(2,1)S(1)} %get-tuple-element.21), channel_id=1, source_target_pairs={{0,1},{1,0},{2,3},{3,2},{4,5},{5,4},{6,7},{7,6},{8,9},{9,8},{10,11... | collective-permute-start | bytes 393224 | tf_op jit(solution)/shard_map/ppermute | solution.py:330
  13.9 1.0 %route.1 = (s32[2,128]{1,0:T(2,128)S(1)}, f32[128,128]{1,0:T(8,128)S(1)}) custom-call(s32[2,128]{1,0:T(2,128)} %bitcast.27, f32[2,128]{1,0:T(2,128)} %bitcast.28, f32[1,128]{1,0:T(1,128)} %bitcast.29), custom_call_target="tpu_custom_call" | custom-call | flops 500000000 | tf_op jit(solution)/shard_map/route/pallas_call | solution.py:42
  14.9 0.0 collective-permute-done.1.other
  14.9 0.0 copy-done
  14.9 0.0 copy-done.1
  14.9 0.0 copy-start.4
  15.0 2.2 %project.1 = (bf16[128,2048]{1,0:T(8,128)(2,1)S(1)}, bf16[1024,1024]{1,0:T(8,128)(2,1)S(1)}) custom-call(s32[2]{0:T(128)S(1)} %pad_add_fusion._.me, bf16[128,512]{1,0:T(8,128)(2,1)S(1)} %get-tuple-element.20.mine, bf16[128,512]{1,0:T(8,128)(2,1)S(1)} %collective-permute-done.1.other, bf16[1024,2048]{1,0:T(8,128)(2,1)S(1)} %get-tuple-element.22.weight, ...), custom_call_target="tpu_custom_call" | custom-call | flops 1000000000 | tf_op jit(solution)/shard_map/project/pallas_call | solution.py:42
  17.2 0.0 copy-start.2
  17.2 0.0 copy-start.3
  17.2 34.8 %all_to_all.10 = bf16[128,8,1024]{2,1,0:T(8,128)(2,1)S(1)} all-to-all(bf16[128,8,1024]{2,1,0:T(8,128)(2,1)S(1)} %bitcast.16), channel_id=1, replica_groups=mesh['sp'=64,'tp'=2] {'sp','tp'}, dimensions={0} | all-to-all | bytes 4194304 | tf_op jit(solution)/shard_map/all_to_all | solution.py:349
  52.0 0.0 copy-done.4
  52.0 0.0 copy-done.2
  52.0 0.0 copy-done.3
  52.0 4.5 %expert.1 = bf16[1024,1024]{1,0:T(8,128)(2,1)S(1)} custom-call(bf16[1024,1024]{1,0:T(8,128)(2,1)S(1)} %bitcast.18, bf16[2048,512]{1,0:T(8,128)(2,1)S(1)} %bitcast.21, bf16[2048,512]{1,0:T(8,128)(2,1)S(1)} %bitcast.22, bf16[512,2048]{1,0:T(8,128)(2,1)S(1)} %bitcast.23), custom_call_target="tpu_custom_call" | custom-call | flops 4000000000 | tf_op jit(solution)/shard_map/expert/pallas_call | solution.py:42
  56.6 34.4 %all_to_all.11 = bf16[128,8,1024]{2,1,0:T(8,128)(2,1)S(1)} all-to-all(bf16[128,8,1024]{2,1,0:T(8,128)(2,1)S(1)} %bitcast.19), channel_id=1, replica_groups=mesh['sp'=64,'tp'=2] {'sp','tp'}, dimensions={0} | all-to-all | bytes 4194304 | tf_op jit(solution)/shard_map/all_to_all | solution.py:349
  90.9 2.1 %combine.1 = bf16[128,2048]{1,0:T(8,128)(2,1)} custom-call(bf16[1024,1024]{1,0:T(8,128)(2,1)S(1)} %bitcast.17, f32[128,128]{1,0:T(8,128)S(1)} %get-tuple-element.25.cols, bf16[128,2048]{1,0:T(8,128)(2,1)S(1)} %get-tuple-element.26.base), custom_call_target="tpu_custom_call" | custom-call | flops 1000000000 | tf_op jit(solution)/shard_map/combine/pallas_call | solution.py:42
Async XLA Ops:
  0.8 10.6 %collective-permute-start = (bf16[32,512]{1,0:T(8,128)(2,1)S(1)}, bf16[32,512]{1,0:T(8,128)(2,1)S(1)}, u32[]{:S(2)}, u32[]{:S(2)}) collective-permute-start(bf16[32,512]{1,0:T(8,128)(2,1)S(1)} %multiply_convert_fusion), channel_id=1, source_target_pairs={{0,2},{2,4},{4,6},{6,8},{8,10},{10,12},{12,14},{14,16},{16,18},{18... | collective-permute-start | bytes 98312 | tf_op jit(solution)/shard_map/ppermute | solution.py:269
  6.5 8.4 %copy-start = (bf16[128,2048]{1,0:T(8,128)(2,1)S(1)}, bf16[128,2048]{1,0:T(8,128)(2,1)}, u32[]{:S(2)}) copy-start(bf16[128,2048]{1,0:T(8,128)(2,1)} %residual.1) | copy-start | bytes 1572868
  6.5 8.4 %copy-start.1 = (f32[2048]{0:T(1024)S(1)}, f32[2048]{0:T(1024)}, u32[]{:S(2)}) copy-start(f32[2048]{0:T(1024)} %param.23) | copy-start | bytes 24580
  12.3 2.6 %collective-permute-start.1 = (bf16[128,512]{1,0:T(8,128)(2,1)S(1)}, bf16[128,512]{1,0:T(8,128)(2,1)S(1)}, u32[]{:S(2)}, u32[]{:S(2)}) collective-permute-start(bf16[128,512]{1,0:T(8,128)(2,1)S(1)} %get-tuple-element.21), channel_id=1, source_target_pairs={{0,1},{1,0},{2,3},{3,2},{4,5},{5,4},{6,7},{7,6},{8,9},{9,8},{10,11... | collective-permute-start | bytes 393224 | tf_op jit(solution)/shard_map/ppermute | solution.py:330
  14.9 37.1 %copy-start.4 = (bf16[1,512,2048]{2,1,0:T(8,128)(2,1)S(1)}, bf16[1,512,2048]{2,1,0:T(8,128)(2,1)}, u32[]{:S(2)}) copy-start(bf16[1,512,2048]{2,1,0:T(8,128)(2,1)} %param.29) | copy-start | bytes 6291460
  17.2 34.9 %copy-start.2 = (bf16[1,2048,512]{2,1,0:T(8,128)(2,1)S(1)}, bf16[1,2048,512]{2,1,0:T(8,128)(2,1)}, u32[]{:S(2)}) copy-start(bf16[1,2048,512]{2,1,0:T(8,128)(2,1)} %param.27) | copy-start | bytes 6291460
  17.2 34.9 %copy-start.3 = (bf16[1,2048,512]{2,1,0:T(8,128)(2,1)S(1)}, bf16[1,2048,512]{2,1,0:T(8,128)(2,1)}, u32[]{:S(2)}) copy-start(bf16[1,2048,512]{2,1,0:T(8,128)(2,1)} %param.28) | copy-start | bytes 6291460

commit v4 on v3

--- a/solution.py
+++ b/solution.py
@@ -98,13 +98,15 @@
     n_taps, width = kernel.shape
     length = value.shape[0]
     blocks = width // LANE
-    *small, large = fetch(
-        (kernel_in, bias_in, gain_in, shift_in, value_in, gate_in, weight_in),
-        (kernel, vecs.at[0:1], vecs.at[1:2], vecs.at[2:3], value, gate, weight),
+    small = fetch(
+        (value_in, gate_in, kernel_in, bias_in, gain_in, shift_in),
+        (value, gate, kernel, vecs.at[0:1], vecs.at[1:2], vecs.at[2:3]),
         sems,
     )
     for copy in small:
         copy.wait()
+    large = pltpu.make_async_copy(weight_in, weight, sems.at[len(small)])
+    large.start()
     for b in range(blocks):
         lanes = slice(b * LANE, (b + 1) * LANE)
         taps[b, 0:n_taps, :] = kernel[:, lanes].astype(F32)
@@ -122,25 +124,27 @@
     large.wait()
 
 
-def head_body(me, rest, front, taps, vecs, halo, mine, theirs, ext, mixed):
+def head_body(cores, me, rest, front, taps, vecs, halo, mine, theirs, ext, mixed):
     n_taps = 31
     blocks, _, _ = front.shape
     half = mine.shape[0]
     for b in range(blocks):
         lanes = slice(b * LANE, (b + 1) * LANE)
-        ext[b, 0:HALO, :] = jnp.where(me[1] > 0, halo[:, lanes].astype(F32), 0.0)
+        ext[b, 0:HALO, :] = jnp.where(me[0] >= cores, halo[:, lanes].astype(F32), 0.0)
         ext[b, HALO : 2 * HALO, :] = front[b, :, :]
     for b in range(blocks):
         lanes = slice(b * LANE, (b + 1) * LANE)
         mixed[:, lanes] = taps_and_norm(ext, taps, vecs, b, 0, HALO, n_taps)
 
-    @pl.when(me[0] == 0)
+    core = lax.rem(me[0], cores)
+
+    @pl.when(core == 0)
     def _():
         mine[0:HALO, :] = mixed[...]
         mine[HALO:half, :] = rest[HALO:half, :]
         theirs[...] = rest[half : 2 * half, :]
 
-    @pl.when(me[0] != 0)
+    @pl.when(core != 0)
     def _():
         theirs[0:HALO, :] = mixed[...]
         theirs[HALO:half, :] = rest[HALO:half, :]
@@ -162,13 +166,14 @@
         ).astype(BF16)
 
 
-def project_body(me, mine, other, weight, residual, gain, place, hidden, out, stacked):
+def project_body(cores, me, mine, other, weight, residual, gain, place, hidden, out, stacked):
     half = mine.shape[1]
     width = residual.shape[1]
     tokens = mine.shape[0]
     step = width // PARTS
-    here = pl.ds(pl.multiple_of(me[0] * half, half), half)
-    there = pl.ds(pl.multiple_of((1 - me[0]) * half, half), half)
+    core = lax.rem(me[0], cores)
+    here = pl.ds(pl.multiple_of(core * half, half), half)
+    there = pl.ds(pl.multiple_of((1 - core) * half, half), half)
     total = jnp.zeros((tokens, 1), F32)
     for q in range(PARTS):
         lanes = slice(q * step, (q + 1) * step)
@@ -222,21 +227,32 @@
         out[b * LANE : (b + 1) * LANE, :] = jnp.dot(p, z, preferred_element_type=F32).astype(BF16)
 
 
-def combine_body(message, cols, base, out, flat):
-    unpack(message, flat)
-    rows = flat.shape[0]
+def combine_body(message, cols, base, out_hbm, out, sems):
     tokens, width = out.shape
-    step = width // 4
-    code = iota((tokens, rows), 1).astype(F32)
-    picked = [onehot(cols[:, k : k + 1] == code) for k in range(2)]
-    for q in range(4):
-        lanes = slice(q * step, (q + 1) * step)
-        acc = base[:, lanes].astype(F32)
-        for k in range(2):
-            acc = acc + cols[:, 2 + k : 3 + k] * jnp.dot(
-                picked[k], flat[:, lanes], preferred_element_type=F32
+    rows, step = message.shape
+    slot = iota((tokens, rows), 1)
+    code = (slot // (RANKS * PARTS) * RANKS + slot % RANKS).astype(F32)
+    share = jnp.where(cols[:, 0:1] == code, cols[:, 2:3], 0.0)
+    share = jnp.where(cols[:, 1:2] == code, cols[:, 3:4], share)
+    part = slot // RANKS % PARTS
+    picked = jnp.concatenate(
+        [jnp.where(part == q, share, 0.0).astype(BF16) for q in range(PARTS)], axis=0
+    )
+    pieces = 4
+    size = step // pieces
+    copies = []
+    for p in range(pieces):
+        got = jnp.dot(picked, message[:, p * size : (p + 1) * size], preferred_element_type=F32)
+        for q in range(PARTS):
+            lanes = slice(q * step + p * size, q * step + (p + 1) * size)
+            out[:, lanes] = (base[:, lanes].astype(F32) + got[q * tokens : (q + 1) * tokens]).astype(BF16)
+            copy = pltpu.make_async_copy(
+                out.at[:, lanes], out_hbm.at[:, lanes], sems.at[p * PARTS + q]
             )
-        out[:, lanes] = acc.astype(out.dtype)
+            copy.start()
+            copies.append(copy)
+    for copy in copies:
+        copy.wait()
 
 
 def local(
@@ -261,7 +277,7 @@
     tokens, model = residual.shape
     experts = lax.axis_size("sp") * lax.axis_size("tp")
     peers = lax.axis_size("sp")
-    me = jnp.stack([lax.axis_index("tp"), lax.axis_index("sp")]).astype(jnp.int32)
+    me = lax.axis_index(("sp", "tp")).astype(jnp.int32).reshape(1)
 
     tail = (
         glu_value[length - HALO :].astype(F32) * jax.nn.sigmoid(glu_gate[length - HALO :].astype(F32))
@@ -303,7 +319,7 @@
         out_weight,
     )
     mine, theirs = call(
-        head_body,
+        functools.partial(head_body, lax.axis_size("tp")),
         (shape((length // 2, width), BF16), shape((length // 2, width), BF16)),
         scratch=(pltpu.VMEM((blocks, 2 * HALO, LANE), F32), pltpu.VMEM((HALO, width), BF16)),
         smem=(0,),
@@ -334,7 +350,7 @@
     message = shape((rows, step), BF16)
     flat = pltpu.VMEM((RANKS * experts, model), BF16)
     hidden, send = call(
-        project_body,
+        functools.partial(project_body, lax.axis_size("tp")),
         (shape((tokens, model), BF16), message),
         scratch=(pltpu.VMEM((PARTS * tokens, step), BF16),),
         smem=(0,),
@@ -362,8 +378,9 @@
     (result,) = call(
         combine_body,
         (shape((tokens, model), BF16),),
-        scratch=(flat,),
+        scratch=(pltpu.VMEM((tokens, model), BF16), pltpu.SemaphoreType.DMA((8,))),
         n_in=3,
+        out_hbm=(0,),
         limit=12,
         flops=1_000_000_000,
         name="combine",

time: 93.3 us -> 91.4 us (0.980)
  Pallas kernels: 14.3 us -> 12.4 us
    pallas_call x6, Pallas kernels: 14.3 us -> 12.4 us  [call(): run(*(pltpu.with_memory_space_constraint(a, pltpu.HBM) if i in hbm else a...]
where the time goes in v4:
time: 91.4 us; the launch traced here: 91.1 us
  blocking collectives  68.9 us (75%)
  Pallas kernels  12.4 us (14%)
  waiting for transfers between devices  5.18 us (6%)
  starting transfers between devices  3.71 us (4%)
    all_to_all x2, blocking collectives, exchange(): return lax.all_to_all(x, ('sp', 'tp'), 0, 0, tiled=True).reshape(rows, step)  68.9 us
    pallas_call x6, Pallas kernels, call(): run(*(pltpu.with_memory_space_constraint(a, pltpu.HBM) if i in hbm else a...  12.4 us
    ppermute x1, waiting for transfers between devices, local(): lax.ppermute(tail, 'sp', [(i, (i + 1) % peers) for i in range(peers)])  5.18 us
    ppermute x1, starting transfers between devices, local(): lax.ppermute(tail, 'sp', [(i, (i + 1) % peers) for i in range(peers)])  2.1 us
  transfers between devices with their start and end apart: 2, of which 1 were waited for; matrix products, arithmetic and copies ran while one was open for 0% of the time, Pallas kernels for 5%

profile of v4, /device:TPU:1, one launch (start us, length us, event | category | flops | bytes accessed | tf_op | source)
XLA Modules:
  0.0 91.1 jit_solution(14002307558700897127)
XLA Ops:
  0.0 0.8 multiply_convert_fusion
  0.8 2.1 %collective-permute-start = (bf16[32,512]{1,0:T(8,128)(2,1)S(1)}, bf16[32,512]{1,0:T(8,128)(2,1)S(1)}, u32[]{:S(2)}, u32[]{:S(2)}) collective-permute-start(bf16[32,512]{1,0:T(8,128)(2,1)S(1)} %multiply_convert_fusion), channel_id=1, source_target_pairs={{0,2},{2,4},{4,6},{6,8},{8,10},{10,12},{12,14},{14,16},{16,18},{18... | collective-permute-start | bytes 98312 | tf_op jit(solution)/shard_map/ppermute | solution.py:285
  2.9 3.3 %conv.1 = (bf16[256,512]{1,0:T(8,128)(2,1)S(1)}, f32[4,32,128]{2,1,0:T(8,128)S(1)}, f32[4,32,128]{2,1,0:T(8,128)S(1)}, f32[8,512]{1,0:T(8,128)S(1)}, bf16[1024,2048]{1,0:T(8,128)(2,1)S(1)}) custom-call(s32[1]{0:T(128)} %bitcast._.me, bf16[256,512]{1,0:T(8,128)(2,1)} %value_in.1, bf16[256,512]{1,0:T(8,128)(2,1)} %gate_in.1, bf16[31,512]{1,0:T(8,128)(2,1)} %kernel_in.1, ...), custom_call_target="tpu_custom_call" | custom-call | flops 3000000000 | tf_op jit(solution)/shard_map/conv/pallas_call | solution.py:42
  6.2 0.0 copy-start
  6.2 0.0 copy-start.1
  6.2 5.2 %collective-permute-done.halo = bf16[32,512]{1,0:T(8,128)(2,1)S(1)} collective-permute-done((bf16[32,512]{1,0:T(8,128)(2,1)S(1)}, bf16[32,512]{1,0:T(8,128)(2,1)S(1)}, u32[]{:S(2)}, u32[]{:S(2)}) %collective-permute-start) | collective-permute-done | bytes 32800 | tf_op jit(solution)/shard_map/ppermute | solution.py:285
  11.4 0.4 head.1
  11.8 1.6 %collective-permute-start.1 = (bf16[128,512]{1,0:T(8,128)(2,1)S(1)}, bf16[128,512]{1,0:T(8,128)(2,1)S(1)}, u32[]{:S(2)}, u32[]{:S(2)}) collective-permute-start(bf16[128,512]{1,0:T(8,128)(2,1)S(1)} %get-tuple-element.21), channel_id=1, source_target_pairs={{0,1},{1,0},{2,3},{3,2},{4,5},{5,4},{6,7},{7,6},{8,9},{9,8},{10,11... | collective-permute-start | bytes 393224 | tf_op jit(solution)/shard_map/ppermute | solution.py:346
  13.4 1.0 %route.1 = (s32[2,128]{1,0:T(2,128)S(1)}, f32[128,128]{1,0:T(8,128)S(1)}) custom-call(s32[2,128]{1,0:T(2,128)} %bitcast.26, f32[2,128]{1,0:T(2,128)} %bitcast.27, f32[1,128]{1,0:T(1,128)} %bitcast.28), custom_call_target="tpu_custom_call" | custom-call | flops 500000000 | tf_op jit(solution)/shard_map/route/pallas_call | solution.py:42
  14.4 0.0 collective-permute-done.1.other
  14.4 0.0 copy-done
  14.4 0.0 copy-done.1
  14.4 0.0 copy-start.4
  14.4 1.6 %project.1 = (bf16[128,2048]{1,0:T(8,128)(2,1)S(1)}, bf16[1024,1024]{1,0:T(8,128)(2,1)S(1)}) custom-call(s32[1]{0:T(128)} %bitcast._.me, bf16[128,512]{1,0:T(8,128)(2,1)S(1)} %get-tuple-element.20.mine, bf16[128,512]{1,0:T(8,128)(2,1)S(1)} %collective-permute-done.1.other, bf16[1024,2048]{1,0:T(8,128)(2,1)S(1)} %get-tuple-element.22.weight, ...), custom_call_target="tpu_custom_call" | custom-call | flops 1000000000 | tf_op jit(solution)/shard_map/project/pallas_call | solution.py:42
  16.1 0.0 copy-start.2
  16.1 0.0 copy-start.3
  16.1 34.5 %all_to_all.10 = bf16[128,8,1024]{2,1,0:T(8,128)(2,1)S(1)} all-to-all(bf16[128,8,1024]{2,1,0:T(8,128)(2,1)S(1)} %bitcast.15), channel_id=1, replica_groups=mesh['sp'=64,'tp'=2] {'sp','tp'}, dimensions={0} | all-to-all | bytes 4194304 | tf_op jit(solution)/shard_map/all_to_all | solution.py:365
  50.6 0.0 copy-done.4
  50.6 0.0 copy-done.2
  50.6 0.0 copy-done.3
  50.6 4.6 %expert.1 = bf16[1024,1024]{1,0:T(8,128)(2,1)S(1)} custom-call(bf16[1024,1024]{1,0:T(8,128)(2,1)S(1)} %bitcast.17, bf16[2048,512]{1,0:T(8,128)(2,1)S(1)} %bitcast.20, bf16[2048,512]{1,0:T(8,128)(2,1)S(1)} %bitcast.21, bf16[512,2048]{1,0:T(8,128)(2,1)S(1)} %bitcast.22), custom_call_target="tpu_custom_call" | custom-call | flops 4000000000 | tf_op jit(solution)/shard_map/expert/pallas_call | solution.py:42
  55.2 34.3 %all_to_all.11 = bf16[128,8,1024]{2,1,0:T(8,128)(2,1)S(1)} all-to-all(bf16[128,8,1024]{2,1,0:T(8,128)(2,1)S(1)} %bitcast.18), channel_id=1, replica_groups=mesh['sp'=64,'tp'=2] {'sp','tp'}, dimensions={0} | all-to-all | bytes 4194304 | tf_op jit(solution)/shard_map/all_to_all | solution.py:365
  89.5 1.6 %combine.1 = bf16[128,2048]{1,0:T(8,128)(2,1)} custom-call(bf16[1024,1024]{1,0:T(8,128)(2,1)S(1)} %bitcast.16, f32[128,128]{1,0:T(8,128)S(1)} %get-tuple-element.25.cols, bf16[128,2048]{1,0:T(8,128)(2,1)S(1)} %get-tuple-element.26.base), custom_call_target="tpu_custom_call" | custom-call | flops 1000000000 | tf_op jit(solution)/shard_map/combine/pallas_call | solution.py:42
Async XLA Ops:
  0.8 10.6 %collective-permute-start = (bf16[32,512]{1,0:T(8,128)(2,1)S(1)}, bf16[32,512]{1,0:T(8,128)(2,1)S(1)}, u32[]{:S(2)}, u32[]{:S(2)}) collective-permute-start(bf16[32,512]{1,0:T(8,128)(2,1)S(1)} %multiply_convert_fusion), channel_id=1, source_target_pairs={{0,2},{2,4},{4,6},{6,8},{8,10},{10,12},{12,14},{14,16},{16,18},{18... | collective-permute-start | bytes 98312 | tf_op jit(solution)/shard_map/ppermute | solution.py:285
  6.2 8.2 %copy-start = (bf16[128,2048]{1,0:T(8,128)(2,1)S(1)}, bf16[128,2048]{1,0:T(8,128)(2,1)}, u32[]{:S(2)}) copy-start(bf16[128,2048]{1,0:T(8,128)(2,1)} %residual.1) | copy-start | bytes 1572868
  6.2 8.2 %copy-start.1 = (f32[2048]{0:T(1024)S(1)}, f32[2048]{0:T(1024)}, u32[]{:S(2)}) copy-start(f32[2048]{0:T(1024)} %param.23) | copy-start | bytes 24580
  11.8 2.6 %collective-permute-start.1 = (bf16[128,512]{1,0:T(8,128)(2,1)S(1)}, bf16[128,512]{1,0:T(8,128)(2,1)S(1)}, u32[]{:S(2)}, u32[]{:S(2)}) collective-permute-start(bf16[128,512]{1,0:T(8,128)(2,1)S(1)} %get-tuple-element.21), channel_id=1, source_target_pairs={{0,1},{1,0},{2,3},{3,2},{4,5},{5,4},{6,7},{7,6},{8,9},{9,8},{10,11... | collective-permute-start | bytes 393224 | tf_op jit(solution)/shard_map/ppermute | solution.py:346
  14.4 36.2 %copy-start.4 = (bf16[1,512,2048]{2,1,0:T(8,128)(2,1)S(1)}, bf16[1,512,2048]{2,1,0:T(8,128)(2,1)}, u32[]{:S(2)}) copy-start(bf16[1,512,2048]{2,1,0:T(8,128)(2,1)} %param.29) | copy-start | bytes 6291460
  16.1 34.6 %copy-start.2 = (bf16[1,2048,512]{2,1,0:T(8,128)(2,1)S(1)}, bf16[1,2048,512]{2,1,0:T(8,128)(2,1)}, u32[]{:S(2)}) copy-start(bf16[1,2048,512]{2,1,0:T(8,128)(2,1)} %param.27) | copy-start | bytes 6291460
  16.1 34.5 %copy-start.3 = (bf16[1,2048,512]{2,1,0:T(8,128)(2,1)S(1)}, bf16[1,2048,512]{2,1,0:T(8,128)(2,1)}, u32[]{:S(2)}) copy-start(bf16[1,2048,512]{2,1,0:T(8,128)(2,1)} %param.28) | copy-start | bytes 6291460

commit v5 on v4

--- a/solution.py
+++ b/solution.py
@@ -54,27 +54,75 @@
     return copies
 
 
-def route_body(pick_in, logits_in, prob_in, place, cols, pick, logits, prob, sems):
-    for copy in fetch((pick_in, logits_in, prob_in), (pick, logits, prob), sems):
-        copy.wait()
+def route(pick, logits, prob, cols, spread):
     e_iota = iota((LANE, LANE), 0)
     n_iota = iota((LANE, LANE), 1)
     picks = [pick[k : k + 1, :] for k in range(2)]
     hits = [(e_iota == p).astype(F32) for p in picks]
     both = (hits[0] + hits[1]).astype(BF16)
     before = jnp.dot(both, onehot(e_iota < n_iota), preferred_element_type=F32)
-    spots = []
+    places = []
     for k in range(2):
         rank = jnp.sum(before * hits[k], axis=0, keepdims=True)
-        spots.append(4 * picks[k] + rank.astype(jnp.int32))
-        place[k : k + 1, :] = spots[k]
+        places.append(RANKS * picks[k] + rank.astype(jnp.int32))
     first = prob[...] * jax.nn.sigmoid(logits[0:1, :] - logits[1:2, :])
     second = prob[...] * jax.nn.sigmoid(logits[1:2, :] - logits[0:1, :])
-    rows = [spots[0].astype(F32), spots[1].astype(F32), first, second]
+    rows = [places[0].astype(F32), places[1].astype(F32), first, second]
     table = jnp.zeros((LANE, LANE), F32)
     for i, row in enumerate(rows):
         table = jnp.where(e_iota == i, row, table)
     cols[...] = table.T
+    part = e_iota // RANKS % PARTS
+    for b in range(spread.shape[0] // LANE):
+        row = e_iota + b * LANE
+        code = row // (RANKS * PARTS) * RANKS + row % RANKS
+        hit = jnp.logical_or(code == places[0], code == places[1])
+        for q in range(PARTS):
+            spread[b * LANE : (b + 1) * LANE, q * LANE : (q + 1) * LANE] = onehot(
+                jnp.logical_and(hit, part == q)
+            )
+
+
+def select(cols, picked):
+    tokens, rows = cols.shape[0], picked.shape[1]
+    slot = iota((tokens, rows), 1)
+    code = (slot // (RANKS * PARTS) * RANKS + slot % RANKS).astype(F32)
+    share = jnp.where(cols[:, 0:1] == code, cols[:, 2:3], 0.0)
+    share = jnp.where(cols[:, 1:2] == code, cols[:, 3:4], share)
+    part = slot // RANKS % PARTS
+    for q in range(PARTS):
+        picked[q * tokens : (q + 1) * tokens, :] = jnp.where(part == q, share, 0.0).astype(BF16)
+
+
+def load_body(
+    value_in, gate_in, kernel_in, bias_in, gain_in, shift_in, pick_in, logits_in, prob_in,
+    value, gate, tail, kernel, vecs, pick, logits, prob,
+    sems,
+):
+    length = value.shape[0]
+    cut = length - HALO
+    last = fetch(
+        (value_in.at[cut:length, :], gate_in.at[cut:length, :]),
+        (value.at[cut:length, :], gate.at[cut:length, :]),
+        sems,
+    )
+    rest = fetch(
+        (
+            value_in.at[0:cut, :], gate_in.at[0:cut, :],
+            kernel_in, bias_in, gain_in, shift_in, pick_in, logits_in, prob_in,
+        ),
+        (
+            value.at[0:cut, :], gate.at[0:cut, :],
+            kernel, vecs.at[0:1], vecs.at[1:2], vecs.at[2:3], pick, logits, prob,
+        ),
+        sems.at[2:11],
+    )
+    for copy in last:
+        copy.wait()
+    glued = value[cut:length, :].astype(F32) * jax.nn.sigmoid(gate[cut:length, :].astype(F32))
+    tail[...] = glued.astype(BF16)
+    for copy in rest:
+        copy.wait()
 
 
 def taps_and_norm(ext, taps, vecs, b, start, rows, n_taps):
@@ -91,22 +139,15 @@
 
 
 def conv_body(
-    _, value_in, gate_in, kernel_in, bias_in, gain_in, shift_in, weight_in,
-    rest, front, taps, vecs, weight,
-    value, gate, kernel, ext, sems,
+    _, value, gate, kernel, vecs, pick, logits, prob, weight_in,
+    rest, front, taps, spread, picked, weight,
+    ext, cols, sem,
 ):
+    large = pltpu.make_async_copy(weight_in, weight, sem.at[0])
+    large.start()
     n_taps, width = kernel.shape
     length = value.shape[0]
     blocks = width // LANE
-    small = fetch(
-        (value_in, gate_in, kernel_in, bias_in, gain_in, shift_in),
-        (value, gate, kernel, vecs.at[0:1], vecs.at[1:2], vecs.at[2:3]),
-        sems,
-    )
-    for copy in small:
-        copy.wait()
-    large = pltpu.make_async_copy(weight_in, weight, sems.at[len(small)])
-    large.start()
     for b in range(blocks):
         lanes = slice(b * LANE, (b + 1) * LANE)
         taps[b, 0:n_taps, :] = kernel[:, lanes].astype(F32)
@@ -121,6 +162,8 @@
         return carry
 
     lax.fori_loop(0, blocks, block, 0)
+    route(pick, logits, prob, cols, spread)
+    select(cols, picked)
     large.wait()
 
 
@@ -151,45 +194,40 @@
         mine[...] = rest[half : 2 * half, :]
 
 
-def slots(stacked, place, out):
-    tokens = place.shape[1]
-    part = iota((LANE, tokens), 0) // RANKS % PARTS
-    for b in range(out.shape[0] // LANE):
-        row = iota((LANE, tokens), 0) + b * LANE
-        code = row // (RANKS * PARTS) * RANKS + row % RANKS
-        hit = jnp.logical_or(code == place[0:1, :], code == place[1:2, :])
-        lhs = jnp.concatenate(
-            [onehot(jnp.logical_and(hit, part == q)) for q in range(PARTS)], axis=1
-        )
-        out[b * LANE : (b + 1) * LANE, :] = jnp.dot(
-            lhs, stacked[...], preferred_element_type=F32
-        ).astype(BF16)
-
-
-def project_body(cores, me, mine, other, weight, residual, gain, place, hidden, out, stacked):
+def own_body(cores, me, mine, weight, residual, partial):
     half = mine.shape[1]
-    width = residual.shape[1]
-    tokens = mine.shape[0]
-    step = width // PARTS
-    core = lax.rem(me[0], cores)
-    here = pl.ds(pl.multiple_of(core * half, half), half)
-    there = pl.ds(pl.multiple_of((1 - core) * half, half), half)
-    total = jnp.zeros((tokens, 1), F32)
-    for q in range(PARTS):
+    step = partial.shape[1] // 4
+    here = pl.ds(pl.multiple_of(lax.rem(me[0], cores) * half, half), half)
+    for q in range(4):
         lanes = slice(q * step, (q + 1) * step)
         acc = jnp.dot(mine[...], weight[here, lanes], preferred_element_type=F32)
-        acc = acc + jnp.dot(other[...], weight[there, lanes], preferred_element_type=F32)
-        full = (acc + residual[:, lanes].astype(F32)).astype(BF16)
+        partial[:, lanes] = acc + residual[:, lanes].astype(F32)
+
+
+def project_body(cores, me, other, weight, partial, gain, spread, hidden, out, stacked):
+    tokens, half = other.shape
+    width = partial.shape[1]
+    step = width // 4
+    there = pl.ds(pl.multiple_of((1 - lax.rem(me[0], cores)) * half, half), half)
+    total = jnp.zeros((tokens, 1), F32)
+    for q in range(4):
+        lanes = slice(q * step, (q + 1) * step)
+        acc = jnp.dot(other[...], weight[there, lanes], preferred_element_type=F32)
+        full = (acc + partial[:, lanes]).astype(BF16)
         hidden[:, lanes] = full
         wide = full.astype(F32)
         total = total + jnp.sum(wide * wide, axis=-1, keepdims=True)
     scale = lax.rsqrt(total / width + EPS)
+    step = width // PARTS
     for q in range(PARTS):
         lanes = slice(q * step, (q + 1) * step)
         stacked[q * tokens : (q + 1) * tokens, :] = (
             hidden[:, lanes].astype(F32) * scale * gain[:, lanes]
         ).astype(BF16)
-    slots(stacked, place, out)
+    chunk = 2 * LANE
+    for b in range(out.shape[0] // chunk):
+        rows = slice(b * chunk, (b + 1) * chunk)
+        out[rows, :] = jnp.dot(spread[rows, :], stacked[...], preferred_element_type=F32).astype(BF16)
 
 
 def perm(back):
@@ -227,22 +265,14 @@
         out[b * LANE : (b + 1) * LANE, :] = jnp.dot(p, z, preferred_element_type=F32).astype(BF16)
 
 
-def combine_body(message, cols, base, out_hbm, out, sems):
-    tokens, width = out.shape
-    rows, step = message.shape
-    slot = iota((tokens, rows), 1)
-    code = (slot // (RANKS * PARTS) * RANKS + slot % RANKS).astype(F32)
-    share = jnp.where(cols[:, 0:1] == code, cols[:, 2:3], 0.0)
-    share = jnp.where(cols[:, 1:2] == code, cols[:, 3:4], share)
-    part = slot // RANKS % PARTS
-    picked = jnp.concatenate(
-        [jnp.where(part == q, share, 0.0).astype(BF16) for q in range(PARTS)], axis=0
-    )
+def combine_body(message, picked, base, out_hbm, out, sems):
+    tokens = out.shape[0]
+    step = message.shape[1]
     pieces = 4
     size = step // pieces
     copies = []
     for p in range(pieces):
-        got = jnp.dot(picked, message[:, p * size : (p + 1) * size], preferred_element_type=F32)
+        got = jnp.dot(picked[...], message[:, p * size : (p + 1) * size], preferred_element_type=F32)
         for q in range(PARTS):
             lanes = slice(q * step + p * size, q * step + (p + 1) * size)
             out[:, lanes] = (base[:, lanes].astype(F32) + got[q * tokens : (q + 1) * tokens]).astype(BF16)
@@ -279,47 +309,66 @@
     peers = lax.axis_size("sp")
     me = lax.axis_index(("sp", "tp")).astype(jnp.int32).reshape(1)
 
-    tail = (
-        glu_value[length - HALO :].astype(F32) * jax.nn.sigmoid(glu_gate[length - HALO :].astype(F32))
-    ).astype(BF16)
-    halo = lax.ppermute(tail, "sp", [(i, (i + 1) % peers) for i in range(peers)])
-
     n_taps = conv_kernel.shape[0]
     blocks = width // LANE
-    rest, front, taps, vecs, weight = call(
-        conv_body,
+    cores = lax.axis_size("tp")
+    step = model // PARTS
+    rows = experts * RANKS * PARTS
+    message = shape((rows, step), BF16)
+    value, gate, tail, kernel, vecs, pick, logits, prob = call(
+        load_body,
         (
             shape((length, width), BF16),
-            shape((blocks, HALO, LANE), F32),
-            shape((blocks, 32, LANE), F32),
+            shape((length, width), BF16),
+            shape((HALO, width), BF16),
+            shape((n_taps, width), BF16),
             shape((8, width), F32),
-            shape(out_weight.shape, BF16),
+            shape((2, tokens), jnp.int32),
+            shape((2, tokens), F32),
+            shape((1, tokens), F32),
         ),
-        scratch=(
-            pltpu.VMEM((length, width), BF16),
-            pltpu.VMEM((length, width), BF16),
-            pltpu.VMEM((n_taps, width), BF16),
-            pltpu.VMEM((blocks, HALO + length, LANE), F32),
-            pltpu.SemaphoreType.DMA((7,)),
-        ),
-        smem=(0,),
-        hbm=range(1, 8),
-        n_in=8,
-        limit=8,
-        flops=3_000_000_000,
-        name="conv",
+        scratch=(pltpu.SemaphoreType.DMA((11,)),),
+        hbm=range(9),
+        n_in=9,
+        limit=4,
+        flops=1_000_000,
+        name="load",
     )(
-        me,
         glu_value,
         glu_gate,
         conv_kernel,
         conv_bias.reshape(1, width),
         group_gain.reshape(1, width),
         group_shift.reshape(1, width),
-        out_weight,
-    )
+        expert_pick.T,
+        pair_logits.T,
+        group_prob.reshape(1, tokens),
+    )
+    halo = lax.ppermute(tail, "sp", [(i, (i + 1) % peers) for i in range(peers)])
+    rest, front, taps, spread, picked, weight = call(
+        conv_body,
+        (
+            shape((length, width), BF16),
+            shape((blocks, HALO, LANE), F32),
+            shape((blocks, 32, LANE), F32),
+            shape((rows, PARTS * tokens), BF16),
+            shape((PARTS * tokens, rows), BF16),
+            shape(out_weight.shape, BF16),
+        ),
+        scratch=(
+            pltpu.VMEM((blocks, HALO + length, LANE), F32),
+            pltpu.VMEM((tokens, LANE), F32),
+            pltpu.SemaphoreType.DMA((1,)),
+        ),
+        smem=(0,),
+        hbm=(8,),
+        n_in=9,
+        limit=8,
+        flops=3_000_000_000,
+        name="conv",
+    )(me, value, gate, kernel, vecs, pick, logits, prob, out_weight)
     mine, theirs = call(
-        functools.partial(head_body, lax.axis_size("tp")),
+        functools.partial(head_body, cores),
         (shape((length // 2, width), BF16), shape((length // 2, width), BF16)),
         scratch=(pltpu.VMEM((blocks, 2 * HALO, LANE), F32), pltpu.VMEM((HALO, width), BF16)),
         smem=(0,),
@@ -328,37 +377,27 @@
         flops=500_000_000,
         name="head",
     )(me, rest, front, taps, vecs, halo)
-    place, cols = call(
-        route_body,
-        (shape((2, tokens), jnp.int32), shape((tokens, LANE), F32)),
-        scratch=(
-            pltpu.VMEM((2, tokens), jnp.int32),
-            pltpu.VMEM((2, tokens), F32),
-            pltpu.VMEM((1, tokens), F32),
-            pltpu.SemaphoreType.DMA((3,)),
-        ),
-        hbm=range(3),
-        n_in=3,
+    other = lax.ppermute(theirs, "tp", [(0, 1), (1, 0)])
+    (partial,) = call(
+        functools.partial(own_body, cores),
+        (shape((tokens, model), F32),),
+        smem=(0,),
+        n_in=4,
         limit=4,
         flops=500_000_000,
-        name="route",
-    )(expert_pick.T, pair_logits.T, group_prob.reshape(1, tokens))
-    other = lax.ppermute(theirs, "tp", [(0, 1), (1, 0)])
-
-    step = model // PARTS
-    rows = experts * RANKS * PARTS
-    message = shape((rows, step), BF16)
-    flat = pltpu.VMEM((RANKS * experts, model), BF16)
+        name="own",
+    )(me, mine, weight, residual)
     hidden, send = call(
-        functools.partial(project_body, lax.axis_size("tp")),
+        functools.partial(project_body, cores),
         (shape((tokens, model), BF16), message),
         scratch=(pltpu.VMEM((PARTS * tokens, step), BF16),),
         smem=(0,),
-        n_in=7,
+        n_in=6,
         limit=16,
         flops=1_000_000_000,
         name="project",
-    )(me, mine, other, weight, residual, ffn_gain.reshape(1, model), place)
+    )(me, other, weight, partial, ffn_gain.reshape(1, model), spread)
+    flat = pltpu.VMEM((RANKS * experts, model), BF16)
 
     def exchange(x):
         x = x.reshape(experts, RANKS * PARTS, step)
@@ -384,7 +423,7 @@
         limit=12,
         flops=1_000_000_000,
         name="combine",
-    )(back, cols, hidden)
+    )(back, picked, hidden)
     return result
 
 

time: 91.4 us -> 90.7 us (level)
  waiting for transfers between devices: 5.18 us -> 6.69 us
    ppermute x1, waiting for transfers between devices: 5.18 us -> 6.17 us  [local(): lax.ppermute(tail, 'sp', [(i, (i + 1) % peers) for i in range(peers)])]
    pallas_call x6 -> x7, Pallas kernels: 12.4 us -> 11.6 us  [call(): run(*(pltpu.with_memory_space_constraint(a, pltpu.HBM) if i in hbm else a...]
  transfers between devices with their start and end apart: 2 -> 2, of which waited for: 1 -> 2; matrix products, arithmetic and copies ran while one was open for 0% -> 0% of each run, Pallas kernels for 5% -> 3%
where the time goes in v5:
time: 90.7 us; the launch traced here: 90.5 us
  blocking collectives  68.4 us (75%)
  Pallas kernels  11.6 us (13%)
  waiting for transfers between devices  6.69 us (7%)
  starting transfers between devices  3.71 us (4%)
    all_to_all x2, blocking collectives, exchange(): return lax.all_to_all(x, ('sp', 'tp'), 0, 0, tiled=True).reshape(rows, step)  68.4 us
    pallas_call x7, Pallas kernels, call(): run(*(pltpu.with_memory_space_constraint(a, pltpu.HBM) if i in hbm else a...  11.6 us
    ppermute x1, waiting for transfers between devices, local(): lax.ppermute(tail, 'sp', [(i, (i + 1) % peers) for i in range(peers)])  6.17 us
    ppermute x1, starting transfers between devices, local(): lax.ppermute(tail, 'sp', [(i, (i + 1) % peers) for i in range(peers)])  2.1 us
  transfers between devices with their start and end apart: 2, of which 2 were waited for; matrix products, arithmetic and copies ran while one was open for 0% of the time, Pallas kernels for 3%

profile of v5, /device:TPU:1, one launch (start us, length us, event | category | flops | bytes accessed | tf_op | source)
XLA Modules:
  0.0 90.5 jit_solution(13061726291339875463)
XLA Ops:
  0.0 1.2 %load.1 = (bf16[256,512]{1,0:T(8,128)(2,1)S(1)}, bf16[256,512]{1,0:T(8,128)(2,1)S(1)}, bf16[32,512]{1,0:T(8,128)(2,1)S(1)}, bf16[31,512]{1,0:T(8,128)(2,1)S(1)},...) custom-call(bf16[256,512]{1,0:T(8,128)(2,1)} %value_in.1, ...), custom_call_target="tpu_custom_call" | custom-call | flops 1000000 | tf_op jit(solution)/shard_map/load/pallas_call | solution.py:42
  1.2 2.1 %collective-permute-start = (bf16[32,512]{1,0:T(8,128)(2,1)S(1)}, bf16[32,512]{1,0:T(8,128)(2,1)S(1)}, u32[]{:S(2)}, u32[]{:S(2)}) collective-permute-start(bf16[32,512]{1,0:T(8,128)(2,1)S(1)} %get-tuple-element.33), channel_id=1, source_target_pairs={{0,2},{2,4},{4,6},{6,8},{8,10},{10,12},{12,14},{14,16},{16,18},{18... | collective-permute-start | bytes 98312 | tf_op jit(solution)/shard_map/ppermute | solution.py:347
  3.3 2.3 %conv.1 = (bf16[256,512]{1,0:T(8,128)(2,1)S(1)}, f32[4,32,128]{2,1,0:T(8,128)S(1)}, f32[4,32,128]{2,1,0:T(8,128)S(1)}, bf16[1024,256]{1,0:T(8,128)(2,1)S(1)}, bf...) custom-call(s32[1]{0:T(128)} %bitcast._.me, bf16[256,512]{1,0:T(8,128)(2,1)S(1)} %get-tuple-element.23.value, ...), custom_call_target="tpu_custom_call" | custom-call | flops 3000000000 | tf_op jit(solution)/shard_map/conv/pallas_call | solution.py:42
  5.6 0.0 copy-start
  5.6 6.2 %collective-permute-done.halo = bf16[32,512]{1,0:T(8,128)(2,1)S(1)} collective-permute-done((bf16[32,512]{1,0:T(8,128)(2,1)S(1)}, bf16[32,512]{1,0:T(8,128)(2,1)S(1)}, u32[]{:S(2)}, u32[]{:S(2)}) %collective-permute-start) | collective-permute-done | bytes 32800 | tf_op jit(solution)/shard_map/ppermute | solution.py:347
  11.8 0.4 head.1
  12.2 1.6 %collective-permute-start.1 = (bf16[128,512]{1,0:T(8,128)(2,1)S(1)}, bf16[128,512]{1,0:T(8,128)(2,1)S(1)}, u32[]{:S(2)}, u32[]{:S(2)}) collective-permute-start(bf16[128,512]{1,0:T(8,128)(2,1)S(1)} %get-tuple-element.34), channel_id=1, source_target_pairs={{0,1},{1,0},{2,3},{3,2},{4,5},{5,4},{6,7},{7,6},{8,9},{9,8},{10,11... | collective-permute-start | bytes 393224 | tf_op jit(solution)/shard_map/ppermute | solution.py:380
  13.8 0.0 copy-done
  13.8 0.0 copy-start.1
  13.8 0.5 own.1.partial
  14.2 0.5 collective-permute-done.1.other
  14.8 0.0 copy-done.1
  14.8 0.0 copy-start.4
  14.8 1.3 %project.1 = (bf16[128,2048]{1,0:T(8,128)(2,1)S(1)}, bf16[1024,1024]{1,0:T(8,128)(2,1)S(1)}) custom-call(s32[1]{0:T(128)} %bitcast._.me, bf16[128,512]{1,0:T(8,128)(2,1)S(1)} %collective-permute-done.1.other, bf16[1024,2048]{1,0:T(8,128)(2,1)S(1)} %get-tuple-element.35.weight, f32[128,2048]{1,0:T(8,128)S(1)} %own.1.partial, f32[1,2048]{1,0:T(1,128)S(1)} %bitcast.19, ...), custom_call_target="tpu_custom_call" | custom-call | flops 1000000000 | tf_op jit(solution)/shard_map/project/pallas_call | solution.py:42
  16.1 0.0 copy-start.2
  16.1 0.0 copy-start.3
  16.1 34.0 %all_to_all.10 = bf16[128,8,1024]{2,1,0:T(8,128)(2,1)S(1)} all-to-all(bf16[128,8,1024]{2,1,0:T(8,128)(2,1)S(1)} %bitcast.15), channel_id=1, replica_groups=mesh['sp'=64,'tp'=2] {'sp','tp'}, dimensions={0} | all-to-all | bytes 4194304 | tf_op jit(solution)/shard_map/all_to_all | solution.py:404
  50.1 0.0 copy-done.4
  50.1 0.0 copy-done.2
  50.1 0.0 copy-done.3
  50.1 4.5 %expert.1 = bf16[1024,1024]{1,0:T(8,128)(2,1)S(1)} custom-call(bf16[1024,1024]{1,0:T(8,128)(2,1)S(1)} %bitcast.17, bf16[2048,512]{1,0:T(8,128)(2,1)S(1)} %bitcast.20, bf16[2048,512]{1,0:T(8,128)(2,1)S(1)} %bitcast.21, bf16[512,2048]{1,0:T(8,128)(2,1)S(1)} %bitcast.22), custom_call_target="tpu_custom_call" | custom-call | flops 4000000000 | tf_op jit(solution)/shard_map/expert/pallas_call | solution.py:42
  54.7 34.4 %all_to_all.11 = bf16[128,8,1024]{2,1,0:T(8,128)(2,1)S(1)} all-to-all(bf16[128,8,1024]{2,1,0:T(8,128)(2,1)S(1)} %bitcast.18), channel_id=1, replica_groups=mesh['sp'=64,'tp'=2] {'sp','tp'}, dimensions={0} | all-to-all | bytes 4194304 | tf_op jit(solution)/shard_map/all_to_all | solution.py:404
  89.0 1.5 %combine.1 = bf16[128,2048]{1,0:T(8,128)(2,1)} custom-call(bf16[1024,1024]{1,0:T(8,128)(2,1)S(1)} %bitcast.16, bf16[256,1024]{1,0:T(8,128)(2,1)S(1)} %get-tuple-element.39.picked, bf16[128,2048]{1,0:T(8,128)(2,1)S(1)} %get-tuple-element.40.base), custom_call_target="tpu_custom_call" | custom-call | flops 1000000000 | tf_op jit(solution)/shard_map/combine/pallas_call | solution.py:42
Async XLA Ops:
  1.2 10.6 %collective-permute-start = (bf16[32,512]{1,0:T(8,128)(2,1)S(1)}, bf16[32,512]{1,0:T(8,128)(2,1)S(1)}, u32[]{:S(2)}, u32[]{:S(2)}) collective-permute-start(bf16[32,512]{1,0:T(8,128)(2,1)S(1)} %get-tuple-element.33), channel_id=1, source_target_pairs={{0,2},{2,4},{4,6},{6,8},{8,10},{10,12},{12,14},{14,16},{16,18},{18... | collective-permute-start | bytes 98312 | tf_op jit(solution)/shard_map/ppermute | solution.py:347
  5.6 8.2 %copy-start = (bf16[128,2048]{1,0:T(8,128)(2,1)S(1)}, bf16[128,2048]{1,0:T(8,128)(2,1)}, u32[]{:S(2)}) copy-start(bf16[128,2048]{1,0:T(8,128)(2,1)} %residual.1) | copy-start | bytes 1572868
  12.2 2.6 %collective-permute-start.1 = (bf16[128,512]{1,0:T(8,128)(2,1)S(1)}, bf16[128,512]{1,0:T(8,128)(2,1)S(1)}, u32[]{:S(2)}, u32[]{:S(2)}) collective-permute-start(bf16[128,512]{1,0:T(8,128)(2,1)S(1)} %get-tuple-element.34), channel_id=1, source_target_pairs={{0,1},{1,0},{2,3},{3,2},{4,5},{5,4},{6,7},{7,6},{8,9},{9,8},{10,11... | collective-permute-start | bytes 393224 | tf_op jit(solution)/shard_map/ppermute | solution.py:380
  13.8 1.0 %copy-start.1 = (f32[2048]{0:T(1024)S(1)}, f32[2048]{0:T(1024)}, u32[]{:S(2)}) copy-start(f32[2048]{0:T(1024)} %param.23) | copy-start | bytes 24580
  14.8 35.4 %copy-start.4 = (bf16[1,512,2048]{2,1,0:T(8,128)(2,1)S(1)}, bf16[1,512,2048]{2,1,0:T(8,128)(2,1)}, u32[]{:S(2)}) copy-start(bf16[1,512,2048]{2,1,0:T(8,128)(2,1)} %param.29) | copy-start | bytes 6291460
  16.1 34.0 %copy-start.2 = (bf16[1,2048,512]{2,1,0:T(8,128)(2,1)S(1)}, bf16[1,2048,512]{2,1,0:T(8,128)(2,1)}, u32[]{:S(2)}) copy-start(bf16[1,2048,512]{2,1,0:T(8,128)(2,1)} %param.27) | copy-start | bytes 6291460
  16.1 34.0 %copy-start.3 = (bf16[1,2048,512]{2,1,0:T(8,128)(2,1)S(1)}, bf16[1,2048,512]{2,1,0:T(8,128)(2,1)}, u32[]{:S(2)}) copy-start(bf16[1,2048,512]{2,1,0:T(8,128)(2,1)} %param.28) | copy-start | bytes 6291460

commit v6 on v5

--- a/solution.py
+++ b/solution.py
@@ -96,32 +96,23 @@
 
 def load_body(
     value_in, gate_in, kernel_in, bias_in, gain_in, shift_in, pick_in, logits_in, prob_in,
-    value, gate, tail, kernel, vecs, pick, logits, prob,
-    sems,
+    tail, kernel, vecs, pick, logits, prob,
+    value, gate, sems,
 ):
-    length = value.shape[0]
-    cut = length - HALO
-    last = fetch(
-        (value_in.at[cut:length, :], gate_in.at[cut:length, :]),
-        (value.at[cut:length, :], gate.at[cut:length, :]),
+    cut = value_in.shape[0] - HALO
+    copies = fetch(
+        (
+            value_in.at[pl.ds(cut, HALO), :], gate_in.at[pl.ds(cut, HALO), :],
+            kernel_in, bias_in, gain_in, shift_in, pick_in, logits_in, prob_in,
+        ),
+        (value, gate, kernel, vecs.at[0:1], vecs.at[1:2], vecs.at[2:3], pick, logits, prob),
         sems,
     )
-    rest = fetch(
-        (
-            value_in.at[0:cut, :], gate_in.at[0:cut, :],
-            kernel_in, bias_in, gain_in, shift_in, pick_in, logits_in, prob_in,
-        ),
-        (
-            value.at[0:cut, :], gate.at[0:cut, :],
-            kernel, vecs.at[0:1], vecs.at[1:2], vecs.at[2:3], pick, logits, prob,
-        ),
-        sems.at[2:11],
-    )
-    for copy in last:
+    for copy in copies[:2]:
         copy.wait()
-    glued = value[cut:length, :].astype(F32) * jax.nn.sigmoid(gate[cut:length, :].astype(F32))
+    glued = value[...].astype(F32) * jax.nn.sigmoid(gate[...].astype(F32))
     tail[...] = glued.astype(BF16)
-    for copy in rest:
+    for copy in copies[2:]:
         copy.wait()
 
 
@@ -139,12 +130,15 @@
 
 
 def conv_body(
-    _, value, gate, kernel, vecs, pick, logits, prob, weight_in,
+    _, value_in, gate_in, kernel, vecs, pick, logits, prob, weight_in,
     rest, front, taps, spread, picked, weight,
-    ext, cols, sem,
+    value, gate, ext, cols, sems,
 ):
-    large = pltpu.make_async_copy(weight_in, weight, sem.at[0])
-    large.start()
+    *copies, large = fetch((value_in, gate_in, weight_in), (value, gate, weight), sems)
+    route(pick, logits, prob, cols, spread)
+    select(cols, picked)
+    for copy in copies:
+        copy.wait()
     n_taps, width = kernel.shape
     length = value.shape[0]
     blocks = width // LANE
@@ -162,8 +156,6 @@
         return carry
 
     lax.fori_loop(0, blocks, block, 0)
-    route(pick, logits, prob, cols, spread)
-    select(cols, picked)
     large.wait()
 
 
@@ -230,39 +222,35 @@
         out[rows, :] = jnp.dot(spread[rows, :], stacked[...], preferred_element_type=F32).astype(BF16)
 
 
-def perm(back):
-    i, j = iota((LANE, LANE), 0), iota((LANE, LANE), 1)
-    if back:
-        i, j = j, i
-    rows = LANE // PARTS
-    return onehot(j == (i % rows) // RANKS * (RANKS * PARTS) + i // rows * RANKS + i % RANKS)
-
-
-def unpack(message, flat):
-    p = perm(False)
-    rows = LANE // PARTS
-    step = message.shape[1]
-    for b in range(message.shape[0] // LANE):
-        y = jnp.dot(p, message[b * LANE : (b + 1) * LANE, :], preferred_element_type=F32).astype(BF16)
-        for q in range(PARTS):
-            flat[b * rows : (b + 1) * rows, q * step : (q + 1) * step] = y[q * rows : (q + 1) * rows]
-
-
-def expert_body(message, gate, up, down, out, flat, answer):
-    unpack(message, flat)
+def trade(a, b):
+    low = iota(a.shape, 1) < RANKS
+    return jnp.where(low, a, pltpu.roll(b, RANKS, 1)), jnp.where(low, pltpu.roll(a, RANKS, 1), b)
+
+
+def expert_body(message, gate, up, down, out, flat):
+    rows, step = message.shape
+    tile = RANKS * PARTS
+    pairs = rows // (2 * tile)
+    pieces = 4
+    size = step // pieces
+    for p in range(pieces):
+        here = slice(p * size, (p + 1) * size)
+        wide = message[:, here].astype(F32).reshape(pairs, 2, tile, size)
+        for q, half in enumerate(trade(wide[:, 0], wide[:, 1])):
+            flat[:, q * step + p * size : q * step + (p + 1) * size] = half.reshape(rows // 2, size).astype(BF16)
     x = flat[...]
     g = jnp.dot(x, gate[...], preferred_element_type=F32)
     u = jnp.dot(x, up[...], preferred_element_type=F32)
     active = (g / (1.0 + jnp.exp(-g)) * u).astype(BF16)
-    answer[...] = jnp.dot(active, down[...], preferred_element_type=F32).astype(BF16)
-    p = perm(True)
-    rows = LANE // PARTS
-    step = out.shape[1]
-    for b in range(out.shape[0] // LANE):
-        z = jnp.concatenate(
-            [answer[b * rows : (b + 1) * rows, q * step : (q + 1) * step] for q in range(PARTS)], axis=0
-        )
-        out[b * LANE : (b + 1) * LANE, :] = jnp.dot(p, z, preferred_element_type=F32).astype(BF16)
+    for p in range(pieces):
+        halves = [
+            jnp.dot(
+                active, down[:, q * step + p * size : q * step + (p + 1) * size], preferred_element_type=F32
+            ).reshape(pairs, tile, size)
+            for q in range(PARTS)
+        ]
+        both = jnp.stack(trade(*halves), axis=1)
+        out[:, p * size : (p + 1) * size] = both.reshape(rows, size).astype(BF16)
 
 
 def combine_body(message, picked, base, out_hbm, out, sems):
@@ -315,11 +303,9 @@
     step = model // PARTS
     rows = experts * RANKS * PARTS
     message = shape((rows, step), BF16)
-    value, gate, tail, kernel, vecs, pick, logits, prob = call(
+    tail, kernel, vecs, pick, logits, prob = call(
         load_body,
         (
-            shape((length, width), BF16),
-            shape((length, width), BF16),
             shape((HALO, width), BF16),
             shape((n_taps, width), BF16),
             shape((8, width), F32),
@@ -327,7 +313,11 @@
             shape((2, tokens), F32),
             shape((1, tokens), F32),
         ),
-        scratch=(pltpu.SemaphoreType.DMA((11,)),),
+        scratch=(
+            pltpu.VMEM((HALO, width), BF16),
+            pltpu.VMEM((HALO, width), BF16),
+            pltpu.SemaphoreType.DMA((9,)),
+        ),
         hbm=range(9),
         n_in=9,
         limit=4,
@@ -356,17 +346,19 @@
             shape(out_weight.shape, BF16),
         ),
         scratch=(
+            pltpu.VMEM((length, width), BF16),
+            pltpu.VMEM((length, width), BF16),
             pltpu.VMEM((blocks, HALO + length, LANE), F32),
             pltpu.VMEM((tokens, LANE), F32),
-            pltpu.SemaphoreType.DMA((1,)),
+            pltpu.SemaphoreType.DMA((3,)),
         ),
         smem=(0,),
-        hbm=(8,),
+        hbm=(1, 2, 8),
         n_in=9,
         limit=8,
         flops=3_000_000_000,
         name="conv",
-    )(me, value, gate, kernel, vecs, pick, logits, prob, out_weight)
+    )(me, glu_value, glu_gate, kernel, vecs, pick, logits, prob, out_weight)
     mine, theirs = call(
         functools.partial(head_body, cores),
         (shape((length // 2, width), BF16), shape((length // 2, width), BF16)),
@@ -407,7 +399,7 @@
     (done,) = call(
         expert_body,
         (message,),
-        scratch=(flat, flat),
+        scratch=(flat,),
         n_in=4,
         limit=24,
         flops=4_000_000_000,

time: 90.7 us -> 89.6 us (0.988)
  transfers between devices with their start and end apart: 2 -> 2, of which waited for: 2 -> 2; matrix products, arithmetic and copies ran while one was open for 0% -> 0% of each run, Pallas kernels for 3% -> 4%
where the time goes in v6:
time: 89.6 us; the launch traced here: 89.4 us
  blocking collectives  68.6 us (77%)
  Pallas kernels  10.9 us (12%)
  waiting for transfers between devices  6.08 us (7%)
  starting transfers between devices  3.71 us (4%)
    all_to_all x2, blocking collectives, exchange(): return lax.all_to_all(x, ('sp', 'tp'), 0, 0, tiled=True).reshape(rows, step)  68.6 us
    pallas_call x7, Pallas kernels, call(): run(*(pltpu.with_memory_space_constraint(a, pltpu.HBM) if i in hbm else a...  10.9 us
    ppermute x1, waiting for transfers between devices, local(): lax.ppermute(tail, 'sp', [(i, (i + 1) % peers) for i in range(peers)])  5.56 us
    ppermute x1, starting transfers between devices, local(): lax.ppermute(tail, 'sp', [(i, (i + 1) % peers) for i in range(peers)])  2.1 us
  transfers between devices with their start and end apart: 2, of which 2 were waited for; matrix products, arithmetic and copies ran while one was open for 0% of the time, Pallas kernels for 4%

profile of v6, /device:TPU:1, one launch (start us, length us, event | category | flops | bytes accessed | tf_op | source)
XLA Modules:
  0.0 89.4 jit_solution(13383329731101474457)
XLA Ops:
  0.0 0.9 load.1
  0.9 2.1 %collective-permute-start = (bf16[32,512]{1,0:T(8,128)(2,1)S(1)}, bf16[32,512]{1,0:T(8,128)(2,1)S(1)}, u32[]{:S(2)}, u32[]{:S(2)}) collective-permute-start(bf16[32,512]{1,0:T(8,128)(2,1)S(1)} %get-tuple-element.29), channel_id=1, source_target_pairs={{0,2},{2,4},{4,6},{6,8},{8,10},{10,12},{12,14},{14,16},{16,18},{18... | collective-permute-start | bytes 98312 | tf_op jit(solution)/shard_map/ppermute | solution.py:337
  3.0 2.9 %conv.1 = (bf16[256,512]{1,0:T(8,128)(2,1)S(1)}, f32[4,32,128]{2,1,0:T(8,128)S(1)}, f32[4,32,128]{2,1,0:T(8,128)S(1)}, bf16[1024,256]{1,0:T(8,128)(2,1)S(1)}, bf...) custom-call(s32[1]{0:T(128)} %bitcast._.me, bf16[256,512]{1,0:T(8,128)(2,1)} %value_in.3, ...), custom_call_target="tpu_custom_call" | custom-call | flops 3000000000 | tf_op jit(solution)/shard_map/conv/pallas_call | solution.py:42
  5.9 0.0 copy-start
  5.9 5.6 %collective-permute-done.halo = bf16[32,512]{1,0:T(8,128)(2,1)S(1)} collective-permute-done((bf16[32,512]{1,0:T(8,128)(2,1)S(1)}, bf16[32,512]{1,0:T(8,128)(2,1)S(1)}, u32[]{:S(2)}, u32[]{:S(2)}) %collective-permute-start) | collective-permute-done | bytes 32800 | tf_op jit(solution)/shard_map/ppermute | solution.py:337
  11.5 0.4 head.1
  11.9 1.6 %collective-permute-start.1 = (bf16[128,512]{1,0:T(8,128)(2,1)S(1)}, bf16[128,512]{1,0:T(8,128)(2,1)S(1)}, u32[]{:S(2)}, u32[]{:S(2)}) collective-permute-start(bf16[128,512]{1,0:T(8,128)(2,1)S(1)} %get-tuple-element.30), channel_id=1, source_target_pairs={{0,1},{1,0},{2,3},{3,2},{4,5},{5,4},{6,7},{7,6},{8,9},{9,8},{10,11... | collective-permute-start | bytes 393224 | tf_op jit(solution)/shard_map/ppermute | solution.py:372
  13.5 0.0 copy-done
  13.5 0.0 copy-start.1
  13.5 0.5 own.1.partial
  13.9 0.5 collective-permute-done.1.other
  14.5 0.0 copy-done.1
  14.5 0.0 copy-start.4
  14.5 1.3 %project.1 = (bf16[128,2048]{1,0:T(8,128)(2,1)S(1)}, bf16[1024,1024]{1,0:T(8,128)(2,1)S(1)}) custom-call(s32[1]{0:T(128)} %bitcast._.me, bf16[128,512]{1,0:T(8,128)(2,1)S(1)} %collective-permute-done.1.other, bf16[1024,2048]{1,0:T(8,128)(2,1)S(1)} %get-tuple-element.31.weight, f32[128,2048]{1,0:T(8,128)S(1)} %own.1.partial, f32[1,2048]{1,0:T(1,128)S(1)} %bitcast.19, ...), custom_call_target="tpu_custom_call" | custom-call | flops 1000000000 | tf_op jit(solution)/shard_map/project/pallas_call | solution.py:42
  15.8 0.0 copy-start.2
  15.8 0.0 copy-start.3
  15.8 34.2 %all_to_all.10 = bf16[128,8,1024]{2,1,0:T(8,128)(2,1)S(1)} all-to-all(bf16[128,8,1024]{2,1,0:T(8,128)(2,1)S(1)} %bitcast.15), channel_id=1, replica_groups=mesh['sp'=64,'tp'=2] {'sp','tp'}, dimensions={0} | all-to-all | bytes 4194304 | tf_op jit(solution)/shard_map/all_to_all | solution.py:396
  50.0 0.0 copy-done.4
  50.0 0.0 copy-done.2
  50.0 0.0 copy-done.3
  50.0 3.5 %expert.1 = bf16[1024,1024]{1,0:T(8,128)(2,1)S(1)} custom-call(bf16[1024,1024]{1,0:T(8,128)(2,1)S(1)} %bitcast.17, bf16[2048,512]{1,0:T(8,128)(2,1)S(1)} %bitcast.20, bf16[2048,512]{1,0:T(8,128)(2,1)S(1)} %bitcast.21, bf16[512,2048]{1,0:T(8,128)(2,1)S(1)} %bitcast.22), custom_call_target="tpu_custom_call" | custom-call | flops 4000000000 | tf_op jit(solution)/shard_map/expert/pallas_call | solution.py:42
  53.5 34.4 %all_to_all.11 = bf16[128,8,1024]{2,1,0:T(8,128)(2,1)S(1)} all-to-all(bf16[128,8,1024]{2,1,0:T(8,128)(2,1)S(1)} %bitcast.18), channel_id=1, replica_groups=mesh['sp'=64,'tp'=2] {'sp','tp'}, dimensions={0} | all-to-all | bytes 4194304 | tf_op jit(solution)/shard_map/all_to_all | solution.py:396
  87.9 1.5 %combine.1 = bf16[128,2048]{1,0:T(8,128)(2,1)} custom-call(bf16[1024,1024]{1,0:T(8,128)(2,1)S(1)} %bitcast.16, bf16[256,1024]{1,0:T(8,128)(2,1)S(1)} %get-tuple-element.35.picked, bf16[128,2048]{1,0:T(8,128)(2,1)S(1)} %get-tuple-element.36.base), custom_call_target="tpu_custom_call" | custom-call | flops 1000000000 | tf_op jit(solution)/shard_map/combine/pallas_call | solution.py:42
Async XLA Ops:
  0.9 10.6 %collective-permute-start = (bf16[32,512]{1,0:T(8,128)(2,1)S(1)}, bf16[32,512]{1,0:T(8,128)(2,1)S(1)}, u32[]{:S(2)}, u32[]{:S(2)}) collective-permute-start(bf16[32,512]{1,0:T(8,128)(2,1)S(1)} %get-tuple-element.29), channel_id=1, source_target_pairs={{0,2},{2,4},{4,6},{6,8},{8,10},{10,12},{12,14},{14,16},{16,18},{18... | collective-permute-start | bytes 98312 | tf_op jit(solution)/shard_map/ppermute | solution.py:337
  5.9 7.6 %copy-start = (bf16[128,2048]{1,0:T(8,128)(2,1)S(1)}, bf16[128,2048]{1,0:T(8,128)(2,1)}, u32[]{:S(2)}) copy-start(bf16[128,2048]{1,0:T(8,128)(2,1)} %residual.1) | copy-start | bytes 1572868
  11.9 2.6 %collective-permute-start.1 = (bf16[128,512]{1,0:T(8,128)(2,1)S(1)}, bf16[128,512]{1,0:T(8,128)(2,1)S(1)}, u32[]{:S(2)}, u32[]{:S(2)}) collective-permute-start(bf16[128,512]{1,0:T(8,128)(2,1)S(1)} %get-tuple-element.30), channel_id=1, source_target_pairs={{0,1},{1,0},{2,3},{3,2},{4,5},{5,4},{6,7},{7,6},{8,9},{9,8},{10,11... | collective-permute-start | bytes 393224 | tf_op jit(solution)/shard_map/ppermute | solution.py:372
  13.5 1.0 %copy-start.1 = (f32[2048]{0:T(1024)S(1)}, f32[2048]{0:T(1024)}, u32[]{:S(2)}) copy-start(f32[2048]{0:T(1024)} %param.23) | copy-start | bytes 24580
  14.5 35.5 %copy-start.4 = (bf16[1,512,2048]{2,1,0:T(8,128)(2,1)S(1)}, bf16[1,512,2048]{2,1,0:T(8,128)(2,1)}, u32[]{:S(2)}) copy-start(bf16[1,512,2048]{2,1,0:T(8,128)(2,1)} %param.29) | copy-start | bytes 6291460
  15.8 34.2 %copy-start.2 = (bf16[1,2048,512]{2,1,0:T(8,128)(2,1)S(1)}, bf16[1,2048,512]{2,1,0:T(8,128)(2,1)}, u32[]{:S(2)}) copy-start(bf16[1,2048,512]{2,1,0:T(8,128)(2,1)} %param.27) | copy-start | bytes 6291460
  15.8 34.2 %copy-start.3 = (bf16[1,2048,512]{2,1,0:T(8,128)(2,1)S(1)}, bf16[1,2048,512]{2,1,0:T(8,128)(2,1)}, u32[]{:S(2)}) copy-start(bf16[1,2048,512]{2,1,0:T(8,128)(2,1)} %param.28) | copy-start | bytes 6291460

commit v7 on v6

--- a/solution.py
+++ b/solution.py
@@ -5,6 +5,7 @@
 from jax.experimental import pallas as pl
 from jax.experimental.pallas import tpu as pltpu
 from jax.sharding import PartitionSpec as P
+
 
 EPS = 1e-06
 F32 = jnp.float32
@@ -24,7 +25,7 @@
     return jnp.where(cond, 1.0, 0.0).astype(BF16)
 
 
-def call(body, out_shape, scratch=(), limit=16, smem=(), hbm=(), n_in=0, out_hbm=(), flops=0, name=None):
+def call(body, out_shape, scratch=(), limit=16, smem=(), hbm=(), n_in=0, out_hbm=(), flops=0):
     kind = {**dict.fromkeys(smem, pltpu.SMEM), **dict.fromkeys(hbm, pltpu.HBM)}
     n_out = len(out_shape)
     run = pl.pallas_call(
@@ -37,7 +38,6 @@
         scratch_shapes=list(scratch),
         compiler_params=pltpu.CompilerParams(vmem_limit_bytes=limit * MIB),
         cost_estimate=pl.CostEstimate(flops=flops, bytes_accessed=0, transcendentals=0),
-        name=name,
     )
     return lambda *args: run(
         *(pltpu.with_memory_space_constraint(a, pltpu.HBM) if i in hbm else a for i, a in enumerate(args))
@@ -130,9 +130,9 @@
 
 
 def conv_body(
-    _, value_in, gate_in, kernel, vecs, pick, logits, prob, weight_in,
-    rest, front, taps, spread, picked, weight,
-    value, gate, ext, cols, sems,
+    cores, me, value_in, gate_in, kernel, vecs, pick, logits, prob, weight_in,
+    mine, packet, front, taps, spread, picked, weight,
+    value, gate, ext, mixed, cols, sems,
 ):
     *copies, large = fetch((value_in, gate_in, weight_in), (value, gate, weight), sems)
     route(pick, logits, prob, cols, spread)
@@ -141,73 +141,99 @@
         copy.wait()
     n_taps, width = kernel.shape
     length = value.shape[0]
+    half = length // 2
     blocks = width // LANE
     for b in range(blocks):
         lanes = slice(b * LANE, (b + 1) * LANE)
         taps[b, 0:n_taps, :] = kernel[:, lanes].astype(F32)
-        glued = value[:, lanes].astype(F32) * jax.nn.sigmoid(gate[:, lanes].astype(F32))
-        ext[b, HALO : HALO + length, :] = glued.astype(BF16).astype(F32)
+        glued = (value[:, lanes].astype(F32) * jax.nn.sigmoid(gate[:, lanes].astype(F32))).astype(BF16)
+        ext[b, HALO : HALO + length, :] = glued.astype(F32)
         front[b, :, :] = ext[b, HALO : 2 * HALO, :]
+        packet[half : half + HALO, lanes] = glued[0:HALO]
+    packet[half + HALO : half + HALO + n_taps, :] = kernel[...]
+    piece = iota((16, width), 0)
+    pieces = jnp.zeros((16, width), F32)
+    for i in range(3):
+        left = vecs[i : i + 1, :]
+        for j in range(3):
+            top = left.astype(BF16).astype(F32)
+            pieces = jnp.where(piece == 3 * i + j, top, pieces)
+            left = left - top
+    packet[half + 2 * HALO : half + 2 * HALO + 16, :] = pieces.astype(BF16)
+    mixed[0:HALO, :] = jnp.zeros((HALO, width), BF16)
 
     def block(b, carry):
         lanes = pl.ds(pl.multiple_of(b * LANE, LANE), LANE)
         for r in range(HALO, length, HALO):
-            rest[r : r + HALO, lanes] = taps_and_norm(ext, taps, vecs, b, r, HALO, n_taps)
+            mixed[r : r + HALO, lanes] = taps_and_norm(ext, taps, vecs, b, r, HALO, n_taps)
         return carry
 
     lax.fori_loop(0, blocks, block, 0)
+    core = lax.rem(me[0], cores)
+    mine[...] = mixed[pl.ds(pl.multiple_of(core * half, half), half), :]
+    packet[0:half, :] = mixed[pl.ds(pl.multiple_of((1 - core) * half, half), half), :]
     large.wait()
 
 
-def head_body(cores, me, rest, front, taps, vecs, halo, mine, theirs, ext, mixed):
-    n_taps = 31
-    blocks, _, _ = front.shape
-    half = mine.shape[0]
-    for b in range(blocks):
+def head(me, cores, halo, front, taps, vecs, ext, out, n_taps):
+    for b in range(front.shape[0]):
         lanes = slice(b * LANE, (b + 1) * LANE)
         ext[b, 0:HALO, :] = jnp.where(me[0] >= cores, halo[:, lanes].astype(F32), 0.0)
         ext[b, HALO : 2 * HALO, :] = front[b, :, :]
-    for b in range(blocks):
+    for b in range(front.shape[0]):
         lanes = slice(b * LANE, (b + 1) * LANE)
-        mixed[:, lanes] = taps_and_norm(ext, taps, vecs, b, 0, HALO, n_taps)
-
+        out[0:HALO, lanes] = taps_and_norm(ext, taps, vecs, b, 0, HALO, n_taps)
+
+
+def own_body(cores, n_taps, me, mine, halo, front, taps, vecs, weight, residual, partial, ext, full):
+    half = mine.shape[1]
+    step = partial.shape[1] // 4
     core = lax.rem(me[0], cores)
+    full[...] = mine[...]
 
     @pl.when(core == 0)
     def _():
-        mine[0:HALO, :] = mixed[...]
-        mine[HALO:half, :] = rest[HALO:half, :]
-        theirs[...] = rest[half : 2 * half, :]
-
-    @pl.when(core != 0)
-    def _():
-        theirs[0:HALO, :] = mixed[...]
-        theirs[HALO:half, :] = rest[HALO:half, :]
-        mine[...] = rest[half : 2 * half, :]
-
-
-def own_body(cores, me, mine, weight, residual, partial):
-    half = mine.shape[1]
-    step = partial.shape[1] // 4
-    here = pl.ds(pl.multiple_of(lax.rem(me[0], cores) * half, half), half)
+        head(me, cores, halo, front, taps, vecs, ext, full, n_taps)
+
+    here = pl.ds(pl.multiple_of(core * half, half), half)
     for q in range(4):
         lanes = slice(q * step, (q + 1) * step)
-        acc = jnp.dot(mine[...], weight[here, lanes], preferred_element_type=F32)
+        acc = jnp.dot(full[...], weight[here, lanes], preferred_element_type=F32)
         partial[:, lanes] = acc + residual[:, lanes].astype(F32)
 
 
-def project_body(cores, me, other, weight, partial, gain, spread, hidden, out, stacked):
-    tokens, half = other.shape
-    width = partial.shape[1]
+def project_body(
+    cores, n_taps, me, packet, halo, weight, partial, gain, spread,
+    hidden, out,
+    stacked, ext, front, taps, vecs, full,
+):
+    tokens, width = partial.shape
+    half = packet.shape[1]
+    core = lax.rem(me[0], cores)
+    full[...] = packet[0:tokens, :]
+
+    @pl.when(core == 0)
+    def _():
+        pieces = packet[tokens + 2 * HALO : tokens + 2 * HALO + 16, :].astype(F32)
+        for i in range(3):
+            vecs[i : i + 1, :] = (pieces[3 * i : 3 * i + 1] + pieces[3 * i + 1 : 3 * i + 2]) + pieces[
+                3 * i + 2 : 3 * i + 3
+            ]
+        for b in range(front.shape[0]):
+            lanes = slice(b * LANE, (b + 1) * LANE)
+            front[b, :, :] = packet[tokens : tokens + HALO, lanes].astype(F32)
+            taps[b, 0:n_taps, :] = packet[tokens + HALO : tokens + HALO + n_taps, lanes].astype(F32)
+        head(me, cores, halo, front, taps, vecs, ext, full, n_taps)
+
     step = width // 4
-    there = pl.ds(pl.multiple_of((1 - lax.rem(me[0], cores)) * half, half), half)
+    there = pl.ds(pl.multiple_of((1 - core) * half, half), half)
     total = jnp.zeros((tokens, 1), F32)
     for q in range(4):
         lanes = slice(q * step, (q + 1) * step)
-        acc = jnp.dot(other[...], weight[there, lanes], preferred_element_type=F32)
-        full = (acc + partial[:, lanes]).astype(BF16)
-        hidden[:, lanes] = full
-        wide = full.astype(F32)
+        acc = jnp.dot(full[...], weight[there, lanes], preferred_element_type=F32)
+        rounded = (acc + partial[:, lanes]).astype(BF16)
+        hidden[:, lanes] = rounded
+        wide = rounded.astype(F32)
         total = total + jnp.sum(wide * wide, axis=-1, keepdims=True)
     scale = lax.rsqrt(total / width + EPS)
     step = width // PARTS
@@ -322,7 +348,6 @@
         n_in=9,
         limit=4,
         flops=1_000_000,
-        name="load",
     )(
         glu_value,
         glu_gate,
@@ -334,12 +359,25 @@
         pair_logits.T,
         group_prob.reshape(1, tokens),
     )
-    halo = lax.ppermute(tail, "sp", [(i, (i + 1) % peers) for i in range(peers)])
-    rest, front, taps, spread, picked, weight = call(
-        conv_body,
+    behind = lax.ppermute(tail, "sp", [(i, (i + 1) % peers) for i in range(peers)])
+    crossed = lax.ppermute(
+        tail,
+        ("sp", "tp"),
+        [
+            (i * cores + c, (i + 1) % peers * cores + (c + 1) % cores)
+            for i in range(peers)
+            for c in range(cores)
+        ],
+    )
+    half = length // 2
+    front_shape = (blocks, HALO, LANE)
+    ext_shape = (blocks, 2 * HALO, LANE)
+    mine, packet, front, taps, spread, picked, weight = call(
+        functools.partial(conv_body, cores),
         (
-            shape((length, width), BF16),
-            shape((blocks, HALO, LANE), F32),
+            shape((half, width), BF16),
+            shape((half + 2 * HALO + 16, width), BF16),
+            shape(front_shape, F32),
             shape((blocks, 32, LANE), F32),
             shape((rows, PARTS * tokens), BF16),
             shape((PARTS * tokens, rows), BF16),
@@ -349,6 +387,7 @@
             pltpu.VMEM((length, width), BF16),
             pltpu.VMEM((length, width), BF16),
             pltpu.VMEM((blocks, HALO + length, LANE), F32),
+            pltpu.VMEM((length, width), BF16),
             pltpu.VMEM((tokens, LANE), F32),
             pltpu.SemaphoreType.DMA((3,)),
         ),
@@ -357,38 +396,33 @@
         n_in=9,
         limit=8,
         flops=3_000_000_000,
-        name="conv",
     )(me, glu_value, glu_gate, kernel, vecs, pick, logits, prob, out_weight)
-    mine, theirs = call(
-        functools.partial(head_body, cores),
-        (shape((length // 2, width), BF16), shape((length // 2, width), BF16)),
-        scratch=(pltpu.VMEM((blocks, 2 * HALO, LANE), F32), pltpu.VMEM((HALO, width), BF16)),
+    other = lax.ppermute(packet, "tp", [(0, 1), (1, 0)])
+    (partial,) = call(
+        functools.partial(own_body, cores, n_taps),
+        (shape((tokens, model), F32),),
+        scratch=(pltpu.VMEM(ext_shape, F32), pltpu.VMEM((half, width), BF16)),
         smem=(0,),
-        n_in=6,
+        n_in=8,
         limit=4,
         flops=500_000_000,
-        name="head",
-    )(me, rest, front, taps, vecs, halo)
-    other = lax.ppermute(theirs, "tp", [(0, 1), (1, 0)])
-    (partial,) = call(
-        functools.partial(own_body, cores),
-        (shape((tokens, model), F32),),
+    )(me, mine, behind, front, taps, vecs, weight, residual)
+    hidden, send = call(
+        functools.partial(project_body, cores, n_taps),
+        (shape((tokens, model), BF16), message),
+        scratch=(
+            pltpu.VMEM((PARTS * tokens, step), BF16),
+            pltpu.VMEM(ext_shape, F32),
+            pltpu.VMEM(front_shape, F32),
+            pltpu.VMEM((blocks, 32, LANE), F32),
+            pltpu.VMEM((8, width), F32),
+            pltpu.VMEM((half, width), BF16),
+        ),
         smem=(0,),
-        n_in=4,
-        limit=4,
-        flops=500_000_000,
-        name="own",
-    )(me, mine, weight, residual)
-    hidden, send = call(
-        functools.partial(project_body, cores),
-        (shape((tokens, model), BF16), message),
-        scratch=(pltpu.VMEM((PARTS * tokens, step), BF16),),
-        smem=(0,),
-        n_in=6,
+        n_in=7,
         limit=16,
         flops=1_000_000_000,
-        name="project",
-    )(me, other, weight, partial, ffn_gain.reshape(1, model), spread)
+    )(me, other, crossed, weight, partial, ffn_gain.reshape(1, model), spread)
     flat = pltpu.VMEM((RANKS * experts, model), BF16)
 
     def exchange(x):
@@ -397,13 +431,7 @@
 
     got = exchange(send)
     (done,) = call(
-        expert_body,
-        (message,),
-        scratch=(flat,),
-        n_in=4,
-        limit=24,
-        flops=4_000_000_000,
-        name="expert",
+        expert_body, (message,), scratch=(flat,), n_in=4, limit=24, flops=4_000_000_000
     )(got, gate_weight[0], up_weight[0], down_weight[0])
     back = exchange(done)
     (result,) = call(
@@ -414,7 +442,6 @@
         out_hbm=(0,),
         limit=12,
         flops=1_000_000_000,
-        name="combine",
     )(back, picked, hidden)
     return result
 
@@ -438,4 +465,5 @@
         P(("sp", "tp"), None, None),
     )
     out_specs = P(("sp", "tp"), None)
+
     return jax.shard_map(local, mesh=mesh, in_specs=in_specs, out_specs=out_specs, check_vma=False)

time: 89.6 us -> 92.4 us (1.031)
  waiting for transfers between devices: 6.08 us -> 7.62 us
    ppermute x1, waiting for transfers between devices: 5.56 us -> 7.41 us  [local(): lax.ppermute(tail, 'sp', [(i, (i + 1) % peers) for i in range(peers)])]
    ppermute x1 -> x2, starting transfers between devices: 1.61 us -> 2.92 us  [the longest x1 1.46 us: local(): other = lax.ppermute(packet, 'tp', [(0, 1), (1, 0)])]
    pallas_call x7 -> x6, Pallas kernels: 10.9 us -> 10.7 us  [call(): run(*(pltpu.with_memory_space_constraint(a, pltpu.HBM) if i in hbm else a...]
  transfers between devices with their start and end apart: 2 -> 3, of which waited for: 2 -> 2; matrix products, arithmetic and copies ran while one was open for 0% -> 0% of each run, Pallas kernels for 4% -> 1%
where the time goes in v7:
time: 92.4 us; the launch traced here: 92.2 us
  blocking collectives  69.5 us (75%)
  Pallas kernels  10.7 us (12%)
  waiting for transfers between devices  7.62 us (8%)
  starting transfers between devices  4.24 us (5%)
    all_to_all x2, blocking collectives, exchange(): return lax.all_to_all(x, ('sp', 'tp'), 0, 0, tiled=True).reshape(rows, step)  69.5 us
    pallas_call x6, Pallas kernels, call(): run(*(pltpu.with_memory_space_constraint(a, pltpu.HBM) if i in hbm else a...  10.7 us
    ppermute x1, waiting for transfers between devices, local(): lax.ppermute(tail, 'sp', [(i, (i + 1) % peers) for i in range(peers)])  7.41 us
  transfers between devices with their start and end apart: 3, of which 2 were waited for; matrix products, arithmetic and copies ran while one was open for 0% of the time, Pallas kernels for 1%

profile of v7, /device:TPU:1, one launch (start us, length us, event | category | flops | bytes accessed | tf_op | source)
XLA Modules:
  0.0 92.2 jit_solution(11895615575477949422)
XLA Ops:
  0.0 0.9 shard_map.145
  0.9 0.0 copy-start
  0.9 3.0 %shard_map.146 = (bf16[128,512]{1,0:T(8,128)(2,1)S(1)}, bf16[208,512]{1,0:T(8,128)(2,1)S(1)}, f32[4,32,128]{2,1,0:T(8,128)S(1)}, f32[4,32,128]{2,1,0:T(8,128)S(1...) custom-call(s32[1]{0:T(128)} %bitcast.me, ...), custom_call_target="tpu_custom_call" | custom-call | flops 3000000000 | tf_op jit(solution)/shard_map/pallas_call | solution.py:42
  3.9 1.5 %collective-permute-start = (bf16[208,512]{1,0:T(8,128)(2,1)S(1)}, bf16[208,512]{1,0:T(8,128)(2,1)S(1)}, u32[]{:S(2)}, u32[]{:S(2)}) collective-permute-start(bf16[208,512]{1,0:T(8,128)(2,1)S(1)} %get-tuple-element.25), channel_id=1, source_target_pairs={{0,1},{1,0},{2,3},{3,2},{4,5},{5,4},{6,7},{7,6},{8,9},{9,8},{10,11... | collective-permute-start | bytes 638984 | tf_op jit(solution)/shard_map/ppermute | solution.py:400
  5.4 1.3 %collective-permute-start.2 = (bf16[32,512]{1,0:T(8,128)(2,1)S(1)}, bf16[32,512]{1,0:T(8,128)(2,1)S(1)}, u32[]{:S(2)}, u32[]{:S(2)}) collective-permute-start(bf16[32,512]{1,0:T(8,128)(2,1)S(1)} %get-tuple-element.26), channel_id=1, source_target_pairs={{0,2},{2,4},{4,6},{6,8},{8,10},{10,12},{12,14},{14,16},{16,18},{18... | collective-permute-start | bytes 98312 | tf_op jit(solution)/shard_map/ppermute | solution.py:362
  6.7 1.5 %collective-permute-start.1 = (bf16[32,512]{1,0:T(8,128)(2,1)S(1)}, bf16[32,512]{1,0:T(8,128)(2,1)S(1)}, u32[]{:S(2)}, u32[]{:S(2)}) collective-permute-start(bf16[32,512]{1,0:T(8,128)(2,1)S(1)} %get-tuple-element.26), channel_id=1, source_target_pairs={{0,3},{1,2},{2,5},{3,4},{4,7},{5,6},{6,9},{7,8},{8,11},{9,10},{10,... | collective-permute-start | bytes 98312 | tf_op jit(solution)/shard_map/ppermute | solution.py:363
  8.2 7.4 %collective-permute-done.2.halo = bf16[32,512]{1,0:T(8,128)(2,1)S(1)} collective-permute-done((bf16[32,512]{1,0:T(8,128)(2,1)S(1)}, bf16[32,512]{1,0:T(8,128)(2,1)S(1)}, u32[]{:S(2)}, u32[]{:S(2)}) %collective-permute-start.2) | collective-permute-done | bytes 32800 | tf_op jit(solution)/shard_map/ppermute | solution.py:362
  15.6 0.0 copy-done
  15.6 0.0 copy-start.1
  15.6 0.5 shard_map.147.partial
  16.1 0.2 collective-permute-done.1.halo
  16.3 0.0 collective-permute-done.packet
  16.3 0.0 copy-done.1
  16.3 0.0 copy-start.4
  16.3 1.4 %shard_map.148 = (bf16[128,2048]{1,0:T(8,128)(2,1)S(1)}, bf16[1024,1024]{1,0:T(8,128)(2,1)S(1)}) custom-call(s32[1]{0:T(128)} %bitcast.me, bf16[208,512]{1,0:T(8,128)(2,1)S(1)} %collective-permute-done.packet, bf16[32,512]{1,0:T(8,128)(2,1)S(1)} %collective-permute-done.1.halo, bf16[1024,2048]{1,0:T(8,128)(2,1)S(1)} %get-tuple-element.27.weight, ...), custom_call_target="tpu_custom_call" | custom-call | flops 1000000000 | tf_op jit(solution)/shard_map/pallas_call | solution.py:42
  17.7 0.0 copy-start.2
  17.7 0.0 copy-start.3
  17.7 35.1 %all_to_all.10 = bf16[128,8,1024]{2,1,0:T(8,128)(2,1)S(1)} all-to-all(bf16[128,8,1024]{2,1,0:T(8,128)(2,1)S(1)} %bitcast.15), channel_id=1, replica_groups=mesh['sp'=64,'tp'=2] {'sp','tp'}, dimensions={0} | all-to-all | bytes 4194304 | tf_op jit(solution)/shard_map/all_to_all | solution.py:430
  52.8 0.0 copy-done.4
  52.8 0.0 copy-done.2
  52.8 0.0 copy-done.3
  52.8 3.5 %shard_map.149 = bf16[1024,1024]{1,0:T(8,128)(2,1)S(1)} custom-call(bf16[1024,1024]{1,0:T(8,128)(2,1)S(1)} %bitcast.17, bf16[2048,512]{1,0:T(8,128)(2,1)S(1)} %bitcast.20, bf16[2048,512]{1,0:T(8,128)(2,1)S(1)} %bitcast.21, bf16[512,2048]{1,0:T(8,128)(2,1)S(1)} %bitcast.22), custom_call_target="tpu_custom_call" | custom-call | flops 4000000000 | tf_op jit(solution)/shard_map/pallas_call | solution.py:42
  56.3 34.4 %all_to_all.11 = bf16[128,8,1024]{2,1,0:T(8,128)(2,1)S(1)} all-to-all(bf16[128,8,1024]{2,1,0:T(8,128)(2,1)S(1)} %bitcast.18), channel_id=1, replica_groups=mesh['sp'=64,'tp'=2] {'sp','tp'}, dimensions={0} | all-to-all | bytes 4194304 | tf_op jit(solution)/shard_map/all_to_all | solution.py:430
  90.7 1.5 %shard_map.150 = bf16[128,2048]{1,0:T(8,128)(2,1)} custom-call(bf16[1024,1024]{1,0:T(8,128)(2,1)S(1)} %bitcast.16, bf16[256,1024]{1,0:T(8,128)(2,1)S(1)} %get-tuple-element.33.picked, bf16[128,2048]{1,0:T(8,128)(2,1)S(1)} %get-tuple-element.34.base), custom_call_target="tpu_custom_call" | custom-call | flops 1000000000 | tf_op jit(solution)/shard_map/pallas_call | solution.py:42
Async XLA Ops:
  0.9 14.7 %copy-start = (bf16[128,2048]{1,0:T(8,128)(2,1)S(1)}, bf16[128,2048]{1,0:T(8,128)(2,1)}, u32[]{:S(2)}) copy-start(bf16[128,2048]{1,0:T(8,128)(2,1)} %residual.1) | copy-start | bytes 1572868
  3.9 12.4 %collective-permute-start = (bf16[208,512]{1,0:T(8,128)(2,1)S(1)}, bf16[208,512]{1,0:T(8,128)(2,1)S(1)}, u32[]{:S(2)}, u32[]{:S(2)}) collective-permute-start(bf16[208,512]{1,0:T(8,128)(2,1)S(1)} %get-tuple-element.25), channel_id=1, source_target_pairs={{0,1},{1,0},{2,3},{3,2},{4,5},{5,4},{6,7},{7,6},{8,9},{9,8},{10,11... | collective-permute-start | bytes 638984 | tf_op jit(solution)/shard_map/ppermute | solution.py:400
  5.4 10.2 %collective-permute-start.2 = (bf16[32,512]{1,0:T(8,128)(2,1)S(1)}, bf16[32,512]{1,0:T(8,128)(2,1)S(1)}, u32[]{:S(2)}, u32[]{:S(2)}) collective-permute-start(bf16[32,512]{1,0:T(8,128)(2,1)S(1)} %get-tuple-element.26), channel_id=1, source_target_pairs={{0,2},{2,4},{4,6},{6,8},{8,10},{10,12},{12,14},{14,16},{16,18},{18... | collective-permute-start | bytes 98312 | tf_op jit(solution)/shard_map/ppermute | solution.py:362
  6.7 9.6 %collective-permute-start.1 = (bf16[32,512]{1,0:T(8,128)(2,1)S(1)}, bf16[32,512]{1,0:T(8,128)(2,1)S(1)}, u32[]{:S(2)}, u32[]{:S(2)}) collective-permute-start(bf16[32,512]{1,0:T(8,128)(2,1)S(1)} %get-tuple-element.26), channel_id=1, source_target_pairs={{0,3},{1,2},{2,5},{3,4},{4,7},{5,6},{6,9},{7,8},{8,11},{9,10},{10,... | collective-permute-start | bytes 98312 | tf_op jit(solution)/shard_map/ppermute | solution.py:363
  15.6 0.7 copy-start.1
  16.3 36.5 %copy-start.4 = (bf16[1,512,2048]{2,1,0:T(8,128)(2,1)S(1)}, bf16[1,512,2048]{2,1,0:T(8,128)(2,1)}, u32[]{:S(2)}) copy-start(bf16[1,512,2048]{2,1,0:T(8,128)(2,1)} %param.29) | copy-start | bytes 6291460
  17.7 35.1 %copy-start.2 = (bf16[1,2048,512]{2,1,0:T(8,128)(2,1)S(1)}, bf16[1,2048,512]{2,1,0:T(8,128)(2,1)}, u32[]{:S(2)}) copy-start(bf16[1,2048,512]{2,1,0:T(8,128)(2,1)} %param.27) | copy-start | bytes 6291460
  17.7 35.1 %copy-start.3 = (bf16[1,2048,512]{2,1,0:T(8,128)(2,1)S(1)}, bf16[1,2048,512]{2,1,0:T(8,128)(2,1)}, u32[]{:S(2)}) copy-start(bf16[1,2048,512]{2,1,0:T(8,128)(2,1)} %param.28) | copy-start | bytes 6291460

commit v8 on v7

--- a/solution.py
+++ b/solution.py
@@ -359,15 +359,16 @@
         pair_logits.T,
         group_prob.reshape(1, tokens),
     )
-    behind = lax.ppermute(tail, "sp", [(i, (i + 1) % peers) for i in range(peers)])
+    ahead = [(i + 1) % peers * cores for i in range(peers)]
     crossed = lax.ppermute(
         tail,
         ("sp", "tp"),
-        [
-            (i * cores + c, (i + 1) % peers * cores + (c + 1) % cores)
-            for i in range(peers)
-            for c in range(cores)
-        ],
+        [(i * cores + 1, ahead[i]) for i in range(peers)] + [(i * cores, i * cores + 1) for i in range(peers)],
+    )
+    behind = lax.ppermute(
+        tail,
+        ("sp", "tp"),
+        [(i * cores, ahead[i]) for i in range(peers)] + [(i * cores + 1, i * cores + 1) for i in range(peers)],
     )
     half = length // 2
     front_shape = (blocks, HALO, LANE)

time: 92.4 us -> 94 us (1.017)
  waiting for transfers between devices: 7.62 us -> 0.53 us
  blocking collectives: 69.5 us -> 76.3 us
  starting transfers between devices: 4.24 us -> 6.15 us
    ppermute x2, waiting for transfers between devices: 7.62 us -> 0.53 us  [the longest x1 0.52 us: local(): lax.ppermute(tail, ('sp', 'tp'), [(i * cores + 1, ahead[i]) for i in rang...]
    all_to_all x2, blocking collectives: 69.5 us -> 76.3 us  [exchange(): return lax.all_to_all(x, ('sp', 'tp'), 0, 0, tiled=True).reshape(rows, step)]
    ppermute x2, starting transfers between devices: 2.78 us -> 4.69 us  [the longest x1 4.04 us: local(): lax.ppermute(tail, ('sp', 'tp'), [(i * cores + 1, ahead[i]) for i in rang...]
  transfers between devices with their start and end apart: 3 -> 3, of which waited for: 2 -> 1; matrix products, arithmetic and copies ran while one was open for 0% -> 0% of each run, Pallas kernels for 1% -> 1%
where the time goes in v8:
time: 94 us; the launch traced here: 93.8 us
  blocking collectives  76.3 us (81%)
  Pallas kernels  10.7 us (11%)
  starting transfers between devices  6.15 us (7%)
    all_to_all x2, blocking collectives, exchange(): return lax.all_to_all(x, ('sp', 'tp'), 0, 0, tiled=True).reshape(rows, step)  76.3 us
    pallas_call x6, Pallas kernels, call(): run(*(pltpu.with_memory_space_constraint(a, pltpu.HBM) if i in hbm else a...  10.7 us
    ppermute x1, starting transfers between devices, local(): lax.ppermute(tail, ('sp', 'tp'), [(i * cores + 1, ahead[i]) for i in rang...  4.04 us
  transfers between devices with their start and end apart: 3, of which 1 were waited for; matrix products, arithmetic and copies ran while one was open for 0% of the time, Pallas kernels for 1%

profile of v8, /device:TPU:1, one launch (start us, length us, event | category | flops | bytes accessed | tf_op | source)
XLA Modules:
  0.0 93.8 jit_solution(11015876002756590986)
XLA Ops:
  0.0 0.9 shard_map.145
  0.9 0.0 copy-start
  0.9 3.0 %shard_map.146 = (bf16[128,512]{1,0:T(8,128)(2,1)S(1)}, bf16[208,512]{1,0:T(8,128)(2,1)S(1)}, f32[4,32,128]{2,1,0:T(8,128)S(1)}, f32[4,32,128]{2,1,0:T(8,128)S(1...) custom-call(s32[1]{0:T(128)} %bitcast.me, ...), custom_call_target="tpu_custom_call" | custom-call | flops 3000000000 | tf_op jit(solution)/shard_map/pallas_call | solution.py:42
  3.9 1.5 %collective-permute-start = (bf16[208,512]{1,0:T(8,128)(2,1)S(1)}, bf16[208,512]{1,0:T(8,128)(2,1)S(1)}, u32[]{:S(2)}, u32[]{:S(2)}) collective-permute-start(bf16[208,512]{1,0:T(8,128)(2,1)S(1)} %get-tuple-element.25), channel_id=1, source_target_pairs={{0,1},{1,0},{2,3},{3,2},{4,5},{5,4},{6,7},{7,6},{8,9},{9,8},{10,11... | collective-permute-start | bytes 638984 | tf_op jit(solution)/shard_map/ppermute | solution.py:401
  5.4 0.7 collective-permute-start.2
  6.1 4.0 %collective-permute-start.1 = (bf16[32,512]{1,0:T(8,128)(2,1)S(1)}, bf16[32,512]{1,0:T(8,128)(2,1)S(1)}, u32[]{:S(2)}, u32[]{:S(2)}) collective-permute-start(bf16[32,512]{1,0:T(8,128)(2,1)S(1)} %get-tuple-element.26), channel_id=1, source_target_pairs={{1,2},{3,4},{5,6},{7,8},{9,10},{11,12},{13,14},{15,16},{17,18},{19... | collective-permute-start | bytes 98312 | tf_op jit(solution)/shard_map/ppermute | solution.py:363
  10.1 0.0 collective-permute-done.2.halo
  10.1 0.0 copy-done
  10.1 0.0 copy-start.1
  10.1 0.5 shard_map.147.partial
  10.6 0.5 collective-permute-done.1.halo
  11.1 0.0 collective-permute-done.packet
  11.1 0.0 copy-done.1
  11.1 0.0 copy-start.4
  11.1 1.4 %shard_map.148 = (bf16[128,2048]{1,0:T(8,128)(2,1)S(1)}, bf16[1024,1024]{1,0:T(8,128)(2,1)S(1)}) custom-call(s32[1]{0:T(128)} %bitcast.me, bf16[208,512]{1,0:T(8,128)(2,1)S(1)} %collective-permute-done.packet, bf16[32,512]{1,0:T(8,128)(2,1)S(1)} %collective-permute-done.1.halo, bf16[1024,2048]{1,0:T(8,128)(2,1)S(1)} %get-tuple-element.27.weight, ...), custom_call_target="tpu_custom_call" | custom-call | flops 1000000000 | tf_op jit(solution)/shard_map/pallas_call | solution.py:42
  12.5 0.0 copy-start.2
  12.5 0.0 copy-start.3
  12.5 41.9 %all_to_all.10 = bf16[128,8,1024]{2,1,0:T(8,128)(2,1)S(1)} all-to-all(bf16[128,8,1024]{2,1,0:T(8,128)(2,1)S(1)} %bitcast.15), channel_id=1, replica_groups=mesh['sp'=64,'tp'=2] {'sp','tp'}, dimensions={0} | all-to-all | bytes 4194304 | tf_op jit(solution)/shard_map/all_to_all | solution.py:431
  54.4 0.0 copy-done.4
  54.4 0.0 copy-done.2
  54.4 0.0 copy-done.3
  54.4 3.5 %shard_map.149 = bf16[1024,1024]{1,0:T(8,128)(2,1)S(1)} custom-call(bf16[1024,1024]{1,0:T(8,128)(2,1)S(1)} %bitcast.17, bf16[2048,512]{1,0:T(8,128)(2,1)S(1)} %bitcast.20, bf16[2048,512]{1,0:T(8,128)(2,1)S(1)} %bitcast.21, bf16[512,2048]{1,0:T(8,128)(2,1)S(1)} %bitcast.22), custom_call_target="tpu_custom_call" | custom-call | flops 4000000000 | tf_op jit(solution)/shard_map/pallas_call | solution.py:42
  57.9 34.4 %all_to_all.11 = bf16[128,8,1024]{2,1,0:T(8,128)(2,1)S(1)} all-to-all(bf16[128,8,1024]{2,1,0:T(8,128)(2,1)S(1)} %bitcast.18), channel_id=1, replica_groups=mesh['sp'=64,'tp'=2] {'sp','tp'}, dimensions={0} | all-to-all | bytes 4194304 | tf_op jit(solution)/shard_map/all_to_all | solution.py:431
  92.3 1.5 %shard_map.150 = bf16[128,2048]{1,0:T(8,128)(2,1)} custom-call(bf16[1024,1024]{1,0:T(8,128)(2,1)S(1)} %bitcast.16, bf16[256,1024]{1,0:T(8,128)(2,1)S(1)} %get-tuple-element.33.picked, bf16[128,2048]{1,0:T(8,128)(2,1)S(1)} %get-tuple-element.34.base), custom_call_target="tpu_custom_call" | custom-call | flops 1000000000 | tf_op jit(solution)/shard_map/pallas_call | solution.py:42
Async XLA Ops:
  0.9 9.2 %copy-start = (bf16[128,2048]{1,0:T(8,128)(2,1)S(1)}, bf16[128,2048]{1,0:T(8,128)(2,1)}, u32[]{:S(2)}) copy-start(bf16[128,2048]{1,0:T(8,128)(2,1)} %residual.1) | copy-start | bytes 1572868
  3.9 7.2 %collective-permute-start = (bf16[208,512]{1,0:T(8,128)(2,1)S(1)}, bf16[208,512]{1,0:T(8,128)(2,1)S(1)}, u32[]{:S(2)}, u32[]{:S(2)}) collective-permute-start(bf16[208,512]{1,0:T(8,128)(2,1)S(1)} %get-tuple-element.25), channel_id=1, source_target_pairs={{0,1},{1,0},{2,3},{3,2},{4,5},{5,4},{6,7},{7,6},{8,9},{9,8},{10,11... | collective-permute-start | bytes 638984 | tf_op jit(solution)/shard_map/ppermute | solution.py:401
  5.4 4.7 %collective-permute-start.2 = (bf16[32,512]{1,0:T(8,128)(2,1)S(1)}, bf16[32,512]{1,0:T(8,128)(2,1)S(1)}, u32[]{:S(2)}, u32[]{:S(2)}) collective-permute-start(bf16[32,512]{1,0:T(8,128)(2,1)S(1)} %get-tuple-element.26), channel_id=1, source_target_pairs={{0,2},{2,4},{4,6},{6,8},{8,10},{10,12},{12,14},{14,16},{16,18},{18... | collective-permute-start | bytes 98312 | tf_op jit(solution)/shard_map/ppermute | solution.py:368
  6.1 5.1 %collective-permute-start.1 = (bf16[32,512]{1,0:T(8,128)(2,1)S(1)}, bf16[32,512]{1,0:T(8,128)(2,1)S(1)}, u32[]{:S(2)}, u32[]{:S(2)}) collective-permute-start(bf16[32,512]{1,0:T(8,128)(2,1)S(1)} %get-tuple-element.26), channel_id=1, source_target_pairs={{1,2},{3,4},{5,6},{7,8},{9,10},{11,12},{13,14},{15,16},{17,18},{19... | collective-permute-start | bytes 98312 | tf_op jit(solution)/shard_map/ppermute | solution.py:363
  10.1 1.0 %copy-start.1 = (f32[2048]{0:T(1024)S(1)}, f32[2048]{0:T(1024)}, u32[]{:S(2)}) copy-start(f32[2048]{0:T(1024)} %param.23) | copy-start | bytes 24580
  11.1 43.3 %copy-start.4 = (bf16[1,512,2048]{2,1,0:T(8,128)(2,1)S(1)}, bf16[1,512,2048]{2,1,0:T(8,128)(2,1)}, u32[]{:S(2)}) copy-start(bf16[1,512,2048]{2,1,0:T(8,128)(2,1)} %param.29) | copy-start | bytes 6291460
  12.5 41.9 %copy-start.2 = (bf16[1,2048,512]{2,1,0:T(8,128)(2,1)S(1)}, bf16[1,2048,512]{2,1,0:T(8,128)(2,1)}, u32[]{:S(2)}) copy-start(bf16[1,2048,512]{2,1,0:T(8,128)(2,1)} %param.27) | copy-start | bytes 6291460
  12.5 41.9 %copy-start.3 = (bf16[1,2048,512]{2,1,0:T(8,128)(2,1)S(1)}, bf16[1,2048,512]{2,1,0:T(8,128)(2,1)}, u32[]{:S(2)}) copy-start(bf16[1,2048,512]{2,1,0:T(8,128)(2,1)} %param.28) | copy-start | bytes 6291460

commit v9 on v7

--- a/solution.py
+++ b/solution.py
@@ -129,28 +129,19 @@
     return (v / (1.0 + jnp.exp(-v))).astype(BF16)
 
 
-def conv_body(
-    cores, me, value_in, gate_in, kernel, vecs, pick, logits, prob, weight_in,
-    mine, packet, front, taps, spread, picked, weight,
-    value, gate, ext, mixed, cols, sems,
+def gate_body(
+    value, gate, kernel, vecs, pick, logits, prob,
+    ext, taps, aside, spread, picked,
+    cols,
 ):
-    *copies, large = fetch((value_in, gate_in, weight_in), (value, gate, weight), sems)
-    route(pick, logits, prob, cols, spread)
-    select(cols, picked)
-    for copy in copies:
-        copy.wait()
     n_taps, width = kernel.shape
-    length = value.shape[0]
-    half = length // 2
-    blocks = width // LANE
-    for b in range(blocks):
+    for b in range(width // LANE):
         lanes = slice(b * LANE, (b + 1) * LANE)
         taps[b, 0:n_taps, :] = kernel[:, lanes].astype(F32)
         glued = (value[:, lanes].astype(F32) * jax.nn.sigmoid(gate[:, lanes].astype(F32))).astype(BF16)
-        ext[b, HALO : HALO + length, :] = glued.astype(F32)
-        front[b, :, :] = ext[b, HALO : 2 * HALO, :]
-        packet[half : half + HALO, lanes] = glued[0:HALO]
-    packet[half + HALO : half + HALO + n_taps, :] = kernel[...]
+        ext[b, :, :] = glued.astype(F32)
+        aside[0:HALO, lanes] = glued[0:HALO]
+    aside[HALO : HALO + n_taps, :] = kernel[...]
     piece = iota((16, width), 0)
     pieces = jnp.zeros((16, width), F32)
     for i in range(3):
@@ -159,28 +150,36 @@
             top = left.astype(BF16).astype(F32)
             pieces = jnp.where(piece == 3 * i + j, top, pieces)
             left = left - top
-    packet[half + 2 * HALO : half + 2 * HALO + 16, :] = pieces.astype(BF16)
+    aside[2 * HALO : 2 * HALO + 16, :] = pieces.astype(BF16)
+    route(pick, logits, prob, cols, spread)
+    select(cols, picked)
+
+
+def conv_body(cores, n_taps, me, ext, taps, vecs, aside, mine, packet, mixed):
+    blocks, length, _ = ext.shape
+    half = length // 2
+    width = mixed.shape[1]
+    packet[half : half + aside.shape[0], :] = aside[...]
     mixed[0:HALO, :] = jnp.zeros((HALO, width), BF16)
 
     def block(b, carry):
         lanes = pl.ds(pl.multiple_of(b * LANE, LANE), LANE)
         for r in range(HALO, length, HALO):
-            mixed[r : r + HALO, lanes] = taps_and_norm(ext, taps, vecs, b, r, HALO, n_taps)
+            mixed[r : r + HALO, lanes] = taps_and_norm(ext, taps, vecs, b, r - HALO, HALO, n_taps)
         return carry
 
     lax.fori_loop(0, blocks, block, 0)
     core = lax.rem(me[0], cores)
     mine[...] = mixed[pl.ds(pl.multiple_of(core * half, half), half), :]
     packet[0:half, :] = mixed[pl.ds(pl.multiple_of((1 - core) * half, half), half), :]
-    large.wait()
 
 
 def head(me, cores, halo, front, taps, vecs, ext, out, n_taps):
-    for b in range(front.shape[0]):
+    for b in range(ext.shape[0]):
         lanes = slice(b * LANE, (b + 1) * LANE)
         ext[b, 0:HALO, :] = jnp.where(me[0] >= cores, halo[:, lanes].astype(F32), 0.0)
-        ext[b, HALO : 2 * HALO, :] = front[b, :, :]
-    for b in range(front.shape[0]):
+        ext[b, HALO : 2 * HALO, :] = front[b, 0:HALO, :]
+    for b in range(ext.shape[0]):
         lanes = slice(b * LANE, (b + 1) * LANE)
         out[0:HALO, lanes] = taps_and_norm(ext, taps, vecs, b, 0, HALO, n_taps)
 
@@ -347,7 +346,7 @@
         hbm=range(9),
         n_in=9,
         limit=4,
-        flops=1_000_000,
+        flops=5_000_000_000,
     )(
         glu_value,
         glu_gate,
@@ -372,31 +371,29 @@
     half = length // 2
     front_shape = (blocks, HALO, LANE)
     ext_shape = (blocks, 2 * HALO, LANE)
-    mine, packet, front, taps, spread, picked, weight = call(
-        functools.partial(conv_body, cores),
+    ext, taps, aside, spread, picked = call(
+        gate_body,
         (
-            shape((half, width), BF16),
-            shape((half + 2 * HALO + 16, width), BF16),
-            shape(front_shape, F32),
+            shape((blocks, length, LANE), F32),
             shape((blocks, 32, LANE), F32),
+            shape((2 * HALO + 16, width), BF16),
             shape((rows, PARTS * tokens), BF16),
             shape((PARTS * tokens, rows), BF16),
-            shape(out_weight.shape, BF16),
         ),
-        scratch=(
-            pltpu.VMEM((length, width), BF16),
-            pltpu.VMEM((length, width), BF16),
-            pltpu.VMEM((blocks, HALO + length, LANE), F32),
-            pltpu.VMEM((length, width), BF16),
-            pltpu.VMEM((tokens, LANE), F32),
-            pltpu.SemaphoreType.DMA((3,)),
-        ),
+        scratch=(pltpu.VMEM((tokens, LANE), F32),),
+        n_in=7,
+        limit=4,
+        flops=3_000_000_000,
+    )(glu_value, glu_gate, kernel, vecs, pick, logits, prob)
+    mine, packet = call(
+        functools.partial(conv_body, cores, n_taps),
+        (shape((half, width), BF16), shape((half + 2 * HALO + 16, width), BF16)),
+        scratch=(pltpu.VMEM((length, width), BF16),),
         smem=(0,),
-        hbm=(1, 2, 8),
-        n_in=9,
-        limit=8,
+        n_in=5,
+        limit=4,
         flops=3_000_000_000,
-    )(me, glu_value, glu_gate, kernel, vecs, pick, logits, prob, out_weight)
+    )(me, ext, taps, vecs, aside)
     other = lax.ppermute(packet, "tp", [(0, 1), (1, 0)])
     (partial,) = call(
         functools.partial(own_body, cores, n_taps),
@@ -406,7 +403,7 @@
         n_in=8,
         limit=4,
         flops=500_000_000,
-    )(me, mine, behind, front, taps, vecs, weight, residual)
+    )(me, mine, behind, ext, taps, vecs, out_weight, residual)
     hidden, send = call(
         functools.partial(project_body, cores, n_taps),
         (shape((tokens, model), BF16), message),
@@ -422,7 +419,7 @@
         n_in=7,
         limit=16,
         flops=1_000_000_000,
-    )(me, other, crossed, weight, partial, ffn_gain.reshape(1, model), spread)
+    )(me, other, crossed, out_weight, partial, ffn_gain.reshape(1, model), spread)
     flat = pltpu.VMEM((RANKS * experts, model), BF16)
 
     def exchange(x):

time: 92.4 us -> 91.9 us (level)
    pallas_call x6 -> x7, Pallas kernels: 10.7 us -> 10.1 us  [call(): run(*(pltpu.with_memory_space_constraint(a, pltpu.HBM) if i in hbm else a...]
where the time goes in v9:
time: 91.9 us; the launch traced here: 91.8 us
  blocking collectives  69.5 us (76%)
  Pallas kernels  10.1 us (11%)
  waiting for transfers between devices  7.62 us (8%)
  starting transfers between devices  4.24 us (5%)
    all_to_all x2, blocking collectives, exchange(): return lax.all_to_all(x, ('sp', 'tp'), 0, 0, tiled=True).reshape(rows, step)  69.5 us
    pallas_call x7, Pallas kernels, call(): run(*(pltpu.with_memory_space_constraint(a, pltpu.HBM) if i in hbm else a...  10.1 us
    ppermute x1, waiting for transfers between devices, local(): lax.ppermute(tail, 'sp', [(i, (i + 1) % peers) for i in range(peers)])  7.41 us
  transfers between devices with their start and end apart: 3, of which 2 were waited for; matrix products, arithmetic and copies ran while one was open for 0% of the time, Pallas kernels for 1%

profile of v9, /device:TPU:1, one launch (start us, length us, event | category | flops | bytes accessed | tf_op | source)
XLA Modules:
  0.0 91.8 jit_solution(4230558662358521493)
XLA Ops:
  0.0 0.0 copy-start.6
  0.0 0.0 copy-start.7
  0.0 0.9 %shard_map.145 = (bf16[32,512]{1,0:T(8,128)(2,1)S(1)}, bf16[31,512]{1,0:T(8,128)(2,1)S(1)}, f32[8,512]{1,0:T(8,128)S(1)}, s32[2,128]{1,0:T(2,128)S(1)}, f32[2,128]{1,0:T(2,128)S(1)}, /*index=5*/f32[1,128]{1,0:T(1,128)S(1)}) custom-call(bf16[256,512]{1,0:T(8,128)(2,1)} %value.1, bf16[256,512]{1,0:T(8,128)(2,1)} %gate.1, bf16[31,512]{1,0:T(8,128)(2,1)} %kernel_in.1, ...), custom_call_target="tpu_custom_call" | custom-call | flops 5000000000 | tf_op jit(solution)/shard_map/pallas_call | solution.py:42
  1.0 0.1 copy-done.6
  1.1 0.1 copy-done.7
  1.1 0.6 shard_map.146
  1.8 0.0 copy-start
  1.8 0.0 copy-start.1
  1.8 1.8 %shard_map.147 = (bf16[128,512]{1,0:T(8,128)(2,1)S(1)}, bf16[208,512]{1,0:T(8,128)(2,1)S(1)}) custom-call(s32[1]{0:T(128)} %bitcast.me, f32[4,256,128]{2,1,0:T(8,128)S(1)} %get-tuple-element.25.ext.front, f32[4,32,128]{2,1,0:T(8,128)S(1)} %get-tuple-element.26.taps, f32[8,512]{1,0:T(8,128)S(1)} %get-tuple-element.21.vecs, ...), custom_call_target="tpu_custom_call" | custom-call | flops 3000000000 | tf_op jit(solution)/shard_map/pallas_call | solution.py:42
  3.6 1.5 %collective-permute-start = (bf16[208,512]{1,0:T(8,128)(2,1)S(1)}, bf16[208,512]{1,0:T(8,128)(2,1)S(1)}, u32[]{:S(2)}, u32[]{:S(2)}) collective-permute-start(bf16[208,512]{1,0:T(8,128)(2,1)S(1)} %get-tuple-element.28), channel_id=1, source_target_pairs={{0,1},{1,0},{2,3},{3,2},{4,5},{5,4},{6,7},{7,6},{8,9},{9,8},{10,11... | collective-permute-start | bytes 638984 | tf_op jit(solution)/shard_map/ppermute | solution.py:397
  5.0 1.3 %collective-permute-start.2 = (bf16[32,512]{1,0:T(8,128)(2,1)S(1)}, bf16[32,512]{1,0:T(8,128)(2,1)S(1)}, u32[]{:S(2)}, u32[]{:S(2)}) collective-permute-start(bf16[32,512]{1,0:T(8,128)(2,1)S(1)} %get-tuple-element.29), channel_id=1, source_target_pairs={{0,2},{2,4},{4,6},{6,8},{8,10},{10,12},{12,14},{14,16},{16,18},{18... | collective-permute-start | bytes 98312 | tf_op jit(solution)/shard_map/ppermute | solution.py:361
  6.4 1.5 %collective-permute-start.1 = (bf16[32,512]{1,0:T(8,128)(2,1)S(1)}, bf16[32,512]{1,0:T(8,128)(2,1)S(1)}, u32[]{:S(2)}, u32[]{:S(2)}) collective-permute-start(bf16[32,512]{1,0:T(8,128)(2,1)S(1)} %get-tuple-element.29), channel_id=1, source_target_pairs={{0,3},{1,2},{2,5},{3,4},{4,7},{5,6},{6,9},{7,8},{8,11},{9,10},{10,... | collective-permute-start | bytes 98312 | tf_op jit(solution)/shard_map/ppermute | solution.py:362
  7.8 7.4 %collective-permute-done.2.halo = bf16[32,512]{1,0:T(8,128)(2,1)S(1)} collective-permute-done((bf16[32,512]{1,0:T(8,128)(2,1)S(1)}, bf16[32,512]{1,0:T(8,128)(2,1)S(1)}, u32[]{:S(2)}, u32[]{:S(2)}) %collective-permute-start.2) | collective-permute-done | bytes 32800 | tf_op jit(solution)/shard_map/ppermute | solution.py:361
  15.2 0.0 copy-done
  15.2 0.0 copy-done.1
  15.2 0.0 copy-start.2
  15.2 0.5 shard_map.148.partial
  15.7 0.2 collective-permute-done.1.halo
  15.9 0.0 collective-permute-done.packet
  15.9 0.0 copy-done.2
  15.9 0.0 copy-start.5
  15.9 1.4 %shard_map.149 = (bf16[128,2048]{1,0:T(8,128)(2,1)S(1)}, bf16[1024,1024]{1,0:T(8,128)(2,1)S(1)}) custom-call(s32[1]{0:T(128)} %bitcast.me, bf16[208,512]{1,0:T(8,128)(2,1)S(1)} %collective-permute-done.packet, bf16[32,512]{1,0:T(8,128)(2,1)S(1)} %collective-permute-done.1.halo, bf16[1024,2048]{1,0:T(8,128)(2,1)S(1)} %copy-done, ...), custom_call_target="tpu_custom_call" | custom-call | flops 1000000000 | tf_op jit(solution)/shard_map/pallas_call | solution.py:42
  17.3 0.0 copy-start.3
  17.3 0.0 copy-start.4
  17.3 35.1 %all_to_all.10 = bf16[128,8,1024]{2,1,0:T(8,128)(2,1)S(1)} all-to-all(bf16[128,8,1024]{2,1,0:T(8,128)(2,1)S(1)} %bitcast.15), channel_id=1, replica_groups=mesh['sp'=64,'tp'=2] {'sp','tp'}, dimensions={0} | all-to-all | bytes 4194304 | tf_op jit(solution)/shard_map/all_to_all | solution.py:427
  52.4 0.0 copy-done.5
  52.4 0.0 copy-done.3
  52.4 0.0 copy-done.4
  52.4 3.5 %shard_map.150 = bf16[1024,1024]{1,0:T(8,128)(2,1)S(1)} custom-call(bf16[1024,1024]{1,0:T(8,128)(2,1)S(1)} %bitcast.17, bf16[2048,512]{1,0:T(8,128)(2,1)S(1)} %bitcast.20, bf16[2048,512]{1,0:T(8,128)(2,1)S(1)} %bitcast.21, bf16[512,2048]{1,0:T(8,128)(2,1)S(1)} %bitcast.22), custom_call_target="tpu_custom_call" | custom-call | flops 4000000000 | tf_op jit(solution)/shard_map/pallas_call | solution.py:42
  56.0 34.4 %all_to_all.11 = bf16[128,8,1024]{2,1,0:T(8,128)(2,1)S(1)} all-to-all(bf16[128,8,1024]{2,1,0:T(8,128)(2,1)S(1)} %bitcast.18), channel_id=1, replica_groups=mesh['sp'=64,'tp'=2] {'sp','tp'}, dimensions={0} | all-to-all | bytes 4194304 | tf_op jit(solution)/shard_map/all_to_all | solution.py:427
  90.3 1.5 %shard_map.151 = bf16[128,2048]{1,0:T(8,128)(2,1)} custom-call(bf16[1024,1024]{1,0:T(8,128)(2,1)S(1)} %bitcast.16, bf16[256,1024]{1,0:T(8,128)(2,1)S(1)} %get-tuple-element.33.picked, bf16[128,2048]{1,0:T(8,128)(2,1)S(1)} %get-tuple-element.34.base), custom_call_target="tpu_custom_call" | custom-call | flops 1000000000 | tf_op jit(solution)/shard_map/pallas_call | solution.py:42
Async XLA Ops:
  0.0 1.1 %copy-start.6 = (bf16[256,512]{1,0:T(8,128)(2,1)S(1)}, bf16[256,512]{1,0:T(8,128)(2,1)}, u32[]{:S(2)}) copy-start(bf16[256,512]{1,0:T(8,128)(2,1)} %value.1) | copy-start | bytes 786436
  0.0 1.1 %copy-start.7 = (bf16[256,512]{1,0:T(8,128)(2,1)S(1)}, bf16[256,512]{1,0:T(8,128)(2,1)}, u32[]{:S(2)}) copy-start(bf16[256,512]{1,0:T(8,128)(2,1)} %gate.1) | copy-start | bytes 786436
  1.8 13.5 %copy-start = (bf16[1024,2048]{1,0:T(8,128)(2,1)S(1)}, bf16[1024,2048]{1,0:T(8,128)(2,1)}, u32[]{:S(2)}) copy-start(bf16[1024,2048]{1,0:T(8,128)(2,1)} %weight.3) | copy-start | bytes 12582916
  1.8 13.4 %copy-start.1 = (bf16[128,2048]{1,0:T(8,128)(2,1)S(1)}, bf16[128,2048]{1,0:T(8,128)(2,1)}, u32[]{:S(2)}) copy-start(bf16[128,2048]{1,0:T(8,128)(2,1)} %residual.1) | copy-start | bytes 1572868
  3.6 12.4 %collective-permute-start = (bf16[208,512]{1,0:T(8,128)(2,1)S(1)}, bf16[208,512]{1,0:T(8,128)(2,1)S(1)}, u32[]{:S(2)}, u32[]{:S(2)}) collective-permute-start(bf16[208,512]{1,0:T(8,128)(2,1)S(1)} %get-tuple-element.28), channel_id=1, source_target_pairs={{0,1},{1,0},{2,3},{3,2},{4,5},{5,4},{6,7},{7,6},{8,9},{9,8},{10,11... | collective-permute-start | bytes 638984 | tf_op jit(solution)/shard_map/ppermute | solution.py:397
  5.0 10.2 %collective-permute-start.2 = (bf16[32,512]{1,0:T(8,128)(2,1)S(1)}, bf16[32,512]{1,0:T(8,128)(2,1)S(1)}, u32[]{:S(2)}, u32[]{:S(2)}) collective-permute-start(bf16[32,512]{1,0:T(8,128)(2,1)S(1)} %get-tuple-element.29), channel_id=1, source_target_pairs={{0,2},{2,4},{4,6},{6,8},{8,10},{10,12},{12,14},{14,16},{16,18},{18... | collective-permute-start | bytes 98312 | tf_op jit(solution)/shard_map/ppermute | solution.py:361
  6.4 9.6 %collective-permute-start.1 = (bf16[32,512]{1,0:T(8,128)(2,1)S(1)}, bf16[32,512]{1,0:T(8,128)(2,1)S(1)}, u32[]{:S(2)}, u32[]{:S(2)}) collective-permute-start(bf16[32,512]{1,0:T(8,128)(2,1)S(1)} %get-tuple-element.29), channel_id=1, source_target_pairs={{0,3},{1,2},{2,5},{3,4},{4,7},{5,6},{6,9},{7,8},{8,11},{9,10},{10,... | collective-permute-start | bytes 98312 | tf_op jit(solution)/shard_map/ppermute | solution.py:362
  15.2 0.7 copy-start.2
  15.9 36.5 %copy-start.5 = (bf16[1,512,2048]{2,1,0:T(8,128)(2,1)S(1)}, bf16[1,512,2048]{2,1,0:T(8,128)(2,1)}, u32[]{:S(2)}) copy-start(bf16[1,512,2048]{2,1,0:T(8,128)(2,1)} %param.29) | copy-start | bytes 6291460
  17.3 35.1 %copy-start.3 = (bf16[1,2048,512]{2,1,0:T(8,128)(2,1)S(1)}, bf16[1,2048,512]{2,1,0:T(8,128)(2,1)}, u32[]{:S(2)}) copy-start(bf16[1,2048,512]{2,1,0:T(8,128)(2,1)} %param.27) | copy-start | bytes 6291460
  17.3 35.1 %copy-start.4 = (bf16[1,2048,512]{2,1,0:T(8,128)(2,1)S(1)}, bf16[1,2048,512]{2,1,0:T(8,128)(2,1)}, u32[]{:S(2)}) copy-start(bf16[1,2048,512]{2,1,0:T(8,128)(2,1)} %param.28) | copy-start | bytes 6291460

commit v10 on v6

--- a/solution.py
+++ b/solution.py
@@ -5,6 +5,7 @@
 from jax.experimental import pallas as pl
 from jax.experimental.pallas import tpu as pltpu
 from jax.sharding import PartitionSpec as P
+
 
 EPS = 1e-06
 F32 = jnp.float32
@@ -24,7 +25,7 @@
     return jnp.where(cond, 1.0, 0.0).astype(BF16)
 
 
-def call(body, out_shape, scratch=(), limit=16, smem=(), hbm=(), n_in=0, out_hbm=(), flops=0, name=None):
+def call(body, out_shape, scratch=(), limit=16, smem=(), hbm=(), n_in=0, out_hbm=(), flops=0):
     kind = {**dict.fromkeys(smem, pltpu.SMEM), **dict.fromkeys(hbm, pltpu.HBM)}
     n_out = len(out_shape)
     run = pl.pallas_call(
@@ -37,7 +38,6 @@
         scratch_shapes=list(scratch),
         compiler_params=pltpu.CompilerParams(vmem_limit_bytes=limit * MIB),
         cost_estimate=pl.CostEstimate(flops=flops, bytes_accessed=0, transcendentals=0),
-        name=name,
     )
     return lambda *args: run(
         *(pltpu.with_memory_space_constraint(a, pltpu.HBM) if i in hbm else a for i, a in enumerate(args))
@@ -130,66 +130,69 @@
 
 
 def conv_body(
-    _, value_in, gate_in, kernel, vecs, pick, logits, prob, weight_in,
-    rest, front, taps, spread, picked, weight,
-    value, gate, ext, cols, sems,
+    value, gate, kernel, vecs, pick, logits, prob,
+    mixed, ext, taps, spread, picked,
+    cols,
 ):
-    *copies, large = fetch((value_in, gate_in, weight_in), (value, gate, weight), sems)
-    route(pick, logits, prob, cols, spread)
-    select(cols, picked)
-    for copy in copies:
-        copy.wait()
     n_taps, width = kernel.shape
-    length = value.shape[0]
-    blocks = width // LANE
+    blocks, length, _ = ext.shape
     for b in range(blocks):
         lanes = slice(b * LANE, (b + 1) * LANE)
         taps[b, 0:n_taps, :] = kernel[:, lanes].astype(F32)
         glued = value[:, lanes].astype(F32) * jax.nn.sigmoid(gate[:, lanes].astype(F32))
-        ext[b, HALO : HALO + length, :] = glued.astype(BF16).astype(F32)
-        front[b, :, :] = ext[b, HALO : 2 * HALO, :]
+        ext[b, :, :] = glued.astype(BF16).astype(F32)
+    mixed[0:HALO, :] = jnp.zeros((HALO, width), BF16)
+    route(pick, logits, prob, cols, spread)
+    select(cols, picked)
 
     def block(b, carry):
         lanes = pl.ds(pl.multiple_of(b * LANE, LANE), LANE)
         for r in range(HALO, length, HALO):
-            rest[r : r + HALO, lanes] = taps_and_norm(ext, taps, vecs, b, r, HALO, n_taps)
+            mixed[r : r + HALO, lanes] = taps_and_norm(ext, taps, vecs, b, r - HALO, HALO, n_taps)
         return carry
 
     lax.fori_loop(0, blocks, block, 0)
-    large.wait()
-
-
-def head_body(cores, me, rest, front, taps, vecs, halo, mine, theirs, ext, mixed):
-    n_taps = 31
-    blocks, _, _ = front.shape
-    half = mine.shape[0]
-    for b in range(blocks):
+
+
+def head(me, cores, halo, front, taps, vecs, ext, out, n_taps):
+    for b in range(ext.shape[0]):
         lanes = slice(b * LANE, (b + 1) * LANE)
         ext[b, 0:HALO, :] = jnp.where(me[0] >= cores, halo[:, lanes].astype(F32), 0.0)
-        ext[b, HALO : 2 * HALO, :] = front[b, :, :]
-    for b in range(blocks):
+        ext[b, HALO : 2 * HALO, :] = front[b, 0:HALO, :]
+    for b in range(ext.shape[0]):
         lanes = slice(b * LANE, (b + 1) * LANE)
-        mixed[:, lanes] = taps_and_norm(ext, taps, vecs, b, 0, HALO, n_taps)
-
+        out[0:HALO, lanes] = taps_and_norm(ext, taps, vecs, b, 0, HALO, n_taps)
+
+
+def give_body(cores, n_taps, me, mixed, halo, front, taps, vecs, theirs, ext):
+    half = theirs.shape[0]
     core = lax.rem(me[0], cores)
 
     @pl.when(core == 0)
     def _():
-        mine[0:HALO, :] = mixed[...]
-        mine[HALO:half, :] = rest[HALO:half, :]
-        theirs[...] = rest[half : 2 * half, :]
+        theirs[...] = mixed[half : 2 * half, :]
 
     @pl.when(core != 0)
     def _():
-        theirs[0:HALO, :] = mixed[...]
-        theirs[HALO:half, :] = rest[HALO:half, :]
-        mine[...] = rest[half : 2 * half, :]
-
-
-def own_body(cores, me, mine, weight, residual, partial):
-    half = mine.shape[1]
+        theirs[...] = mixed[0:half, :]
+        head(me, cores, halo, front, taps, vecs, ext, theirs, n_taps)
+
+
+def own_body(cores, n_taps, me, mixed, halo, front, taps, vecs, weight, residual, partial, ext, mine):
+    half, width = mine.shape
     step = partial.shape[1] // 4
-    here = pl.ds(pl.multiple_of(lax.rem(me[0], cores) * half, half), half)
+    core = lax.rem(me[0], cores)
+
+    @pl.when(core == 0)
+    def _():
+        mine[...] = mixed[0:half, :]
+        head(me, cores, halo, front, taps, vecs, ext, mine, n_taps)
+
+    @pl.when(core != 0)
+    def _():
+        mine[...] = mixed[half : 2 * half, :]
+
+    here = pl.ds(pl.multiple_of(core * width, width), width)
     for q in range(4):
         lanes = slice(q * step, (q + 1) * step)
         acc = jnp.dot(mine[...], weight[here, lanes], preferred_element_type=F32)
@@ -205,9 +208,9 @@
     for q in range(4):
         lanes = slice(q * step, (q + 1) * step)
         acc = jnp.dot(other[...], weight[there, lanes], preferred_element_type=F32)
-        full = (acc + partial[:, lanes]).astype(BF16)
-        hidden[:, lanes] = full
-        wide = full.astype(F32)
+        rounded = (acc + partial[:, lanes]).astype(BF16)
+        hidden[:, lanes] = rounded
+        wide = rounded.astype(F32)
         total = total + jnp.sum(wide * wide, axis=-1, keepdims=True)
     scale = lax.rsqrt(total / width + EPS)
     step = width // PARTS
@@ -321,8 +324,7 @@
         hbm=range(9),
         n_in=9,
         limit=4,
-        flops=1_000_000,
-        name="load",
+        flops=5_000_000_000,
     )(
         glu_value,
         glu_gate,
@@ -335,50 +337,41 @@
         group_prob.reshape(1, tokens),
     )
     halo = lax.ppermute(tail, "sp", [(i, (i + 1) % peers) for i in range(peers)])
-    rest, front, taps, spread, picked, weight = call(
+    half = length // 2
+    ext_shape = (blocks, 2 * HALO, LANE)
+    mixed, ext, taps, spread, picked = call(
         conv_body,
         (
             shape((length, width), BF16),
-            shape((blocks, HALO, LANE), F32),
+            shape((blocks, length, LANE), F32),
             shape((blocks, 32, LANE), F32),
             shape((rows, PARTS * tokens), BF16),
             shape((PARTS * tokens, rows), BF16),
-            shape(out_weight.shape, BF16),
         ),
-        scratch=(
-            pltpu.VMEM((length, width), BF16),
-            pltpu.VMEM((length, width), BF16),
-            pltpu.VMEM((blocks, HALO + length, LANE), F32),
-            pltpu.VMEM((tokens, LANE), F32),
-            pltpu.SemaphoreType.DMA((3,)),
-        ),
-        smem=(0,),
-        hbm=(1, 2, 8),
-        n_in=9,
-        limit=8,
-        flops=3_000_000_000,
-        name="conv",
-    )(me, glu_value, glu_gate, kernel, vecs, pick, logits, prob, out_weight)
-    mine, theirs = call(
-        functools.partial(head_body, cores),
-        (shape((length // 2, width), BF16), shape((length // 2, width), BF16)),
-        scratch=(pltpu.VMEM((blocks, 2 * HALO, LANE), F32), pltpu.VMEM((HALO, width), BF16)),
+        scratch=(pltpu.VMEM((tokens, LANE), F32),),
+        n_in=7,
+        limit=4,
+        flops=6_000_000_000,
+    )(glu_value, glu_gate, kernel, vecs, pick, logits, prob)
+    (theirs,) = call(
+        functools.partial(give_body, cores, n_taps),
+        (shape((half, width), BF16),),
+        scratch=(pltpu.VMEM(ext_shape, F32),),
         smem=(0,),
         n_in=6,
         limit=4,
         flops=500_000_000,
-        name="head",
-    )(me, rest, front, taps, vecs, halo)
+    )(me, mixed, halo, ext, taps, vecs)
     other = lax.ppermute(theirs, "tp", [(0, 1), (1, 0)])
     (partial,) = call(
-        functools.partial(own_body, cores),
+        functools.partial(own_body, cores, n_taps),
         (shape((tokens, model), F32),),
+        scratch=(pltpu.VMEM(ext_shape, F32), pltpu.VMEM((half, width), BF16)),
         smem=(0,),
-        n_in=4,
+        n_in=8,
         limit=4,
         flops=500_000_000,
-        name="own",
-    )(me, mine, weight, residual)
+    )(me, mixed, halo, ext, taps, vecs, out_weight, residual)
     hidden, send = call(
         functools.partial(project_body, cores),
         (shape((tokens, model), BF16), message),
@@ -387,8 +380,7 @@
         n_in=6,
         limit=16,
         flops=1_000_000_000,
-        name="project",
-    )(me, other, weight, partial, ffn_gain.reshape(1, model), spread)
+    )(me, other, out_weight, partial, ffn_gain.reshape(1, model), spread)
     flat = pltpu.VMEM((RANKS * experts, model), BF16)
 
     def exchange(x):
@@ -397,13 +389,7 @@
 
     got = exchange(send)
     (done,) = call(
-        expert_body,
-        (message,),
-        scratch=(flat,),
-        n_in=4,
-        limit=24,
-        flops=4_000_000_000,
-        name="expert",
+        expert_body, (message,), scratch=(flat,), n_in=4, limit=24, flops=4_000_000_000
     )(got, gate_weight[0], up_weight[0], down_weight[0])
     back = exchange(done)
     (result,) = call(
@@ -414,7 +400,6 @@
         out_hbm=(0,),
         limit=12,
         flops=1_000_000_000,
-        name="combine",
     )(back, picked, hidden)
     return result
 
@@ -438,4 +423,5 @@
         P(("sp", "tp"), None, None),
     )
     out_specs = P(("sp", "tp"), None)
+
     return jax.shard_map(local, mesh=mesh, in_specs=in_specs, out_specs=out_specs, check_vma=False)

time: 89.6 us -> 92.6 us (1.033)
  local copies, waits for them, and re-layouts: 0.03 us -> 3.91 us
    unnamed x10 -> x18, local copies, waits for them, and re-layouts: 0.03 us -> 3.91 us
  transfers between devices with their start and end apart: 2 -> 2, of which waited for: 2 -> 1; matrix products, arithmetic and copies ran while one was open for 0% -> 0% of each run, Pallas kernels for 4% -> 3%
where the time goes in v10:
time: 92.6 us; the launch traced here: 92.4 us
  blocking collectives  68.5 us (74%)
  Pallas kernels  10.4 us (11%)
  waiting for transfers between devices  6.16 us (7%)
  local copies, waits for them, and re-layouts  3.91 us (4%)
  starting transfers between devices  3.4 us (4%)
    all_to_all x2, blocking collectives, exchange(): return lax.all_to_all(x, ('sp', 'tp'), 0, 0, tiled=True).reshape(rows, step)  68.5 us
    pallas_call x7, Pallas kernels, call(): run(*(pltpu.with_memory_space_constraint(a, pltpu.HBM) if i in hbm else a...  10.4 us
    ppermute x1, waiting for transfers between devices, local(): lax.ppermute(tail, 'sp', [(i, (i + 1) % peers) for i in range(peers)])  6.16 us
    unnamed x18, local copies, waits for them, and re-layouts  3.91 us
    ppermute x1, starting transfers between devices, local(): lax.ppermute(tail, 'sp', [(i, (i + 1) % peers) for i in range(peers)])  2.1 us
  transfers between devices with their start and end apart: 2, of which 1 were waited for; matrix products, arithmetic and copies ran while one was open for 0% of the time, Pallas kernels for 3%

profile of v10, /device:TPU:1, one launch (start us, length us, event | category | flops | bytes accessed | tf_op | source)
XLA Modules:
  0.0 92.4 jit_solution(3478095857590170603)
XLA Ops:
  0.0 0.0 copy-start.7
  0.0 0.0 copy-start.8
  0.0 0.9 %shard_map.145 = (bf16[32,512]{1,0:T(8,128)(2,1)S(1)}, bf16[31,512]{1,0:T(8,128)(2,1)S(1)}, f32[8,512]{1,0:T(8,128)S(1)}, s32[2,128]{1,0:T(2,128)S(1)}, f32[2,128]{1,0:T(2,128)S(1)}, /*index=5*/f32[1,128]{1,0:T(1,128)S(1)}) custom-call(bf16[256,512]{1,0:T(8,128)(2,1)} %value.1, bf16[256,512]{1,0:T(8,128)(2,1)} %gate.1, bf16[31,512]{1,0:T(8,128)(2,1)} %kernel_in.1, ...), custom_call_target="tpu_custom_call" | custom-call | flops 5000000000 | tf_op jit(solution)/shard_map/pallas_call | solution.py:42
  1.0 2.1 %collective-permute-start = (bf16[32,512]{1,0:T(8,128)(2,1)S(1)}, bf16[32,512]{1,0:T(8,128)(2,1)S(1)}, u32[]{:S(2)}, u32[]{:S(2)}) collective-permute-start(bf16[32,512]{1,0:T(8,128)(2,1)S(1)} %get-tuple-element.24), channel_id=1, source_target_pairs={{0,2},{2,4},{4,6},{6,8},{8,10},{10,12},{12,14},{14,16},{16,18},{18... | collective-permute-start | bytes 98312 | tf_op jit(solution)/shard_map/ppermute | solution.py:339
  3.1 0.0 copy-done.7
  3.1 0.0 copy-done.8
  3.1 2.3 %shard_map.146 = (bf16[256,512]{1,0:T(8,128)(2,1)S(1)}, f32[4,256,128]{2,1,0:T(8,128)S(1)}, f32[4,32,128]{2,1,0:T(8,128)S(1)}, bf16[1024,256]{1,0:T(8,128)(2,1)S(1)}, bf16[256,1024]{1,0:T(8,128)(2,1)S(1)}) custom-call(bf16[256,512]{1,0:T(8,128)(2,1)S(1)} %copy-done.7, bf16[256,512]{1,0:T(8,128)(2,1)S(1)} %copy-done.8, ...), custom_call_target="tpu_custom_call" | custom-call | flops 6000000000 | tf_op jit(solution)/shard_map/pallas_call | solution.py:42
  5.4 0.0 copy-start.2
  5.4 6.2 %collective-permute-done.halo = bf16[32,512]{1,0:T(8,128)(2,1)S(1)} collective-permute-done((bf16[32,512]{1,0:T(8,128)(2,1)S(1)}, bf16[32,512]{1,0:T(8,128)(2,1)S(1)}, u32[]{:S(2)}, u32[]{:S(2)}) %collective-permute-start) | collective-permute-done | bytes 32800 | tf_op jit(solution)/shard_map/ppermute | solution.py:339
  11.5 0.3 shard_map.147
  11.9 1.3 %collective-permute-start.1 = (bf16[128,512]{1,0:T(8,128)(2,1)S(1)}, bf16[128,512]{1,0:T(8,128)(2,1)S(1)}, u32[]{:S(2)}, u32[]{:S(2)}) collective-permute-start(bf16[128,512]{1,0:T(8,128)(2,1)S(1)} %shard_map.147), channel_id=1, source_target_pairs={{0,1},{1,0},{2,3},{3,2},{4,5},{5,4},{6,7},{7,6},{8,9},{9,8},{10,11... | collective-permute-start | bytes 393224 | tf_op jit(solution)/shard_map/ppermute | solution.py:365
  13.2 0.0 copy-done.2
  13.2 0.0 copy-start
  13.2 2.2 %copy-done = bf16[1024,2048]{1,0:T(8,128)(2,1)S(1)} copy-done((bf16[1024,2048]{1,0:T(8,128)(2,1)S(1)}, bf16[1024,2048]{1,0:T(8,128)(2,1)}, u32[]{:S(2)}) %copy-start) | copy-done | bytes 4194328
  15.4 0.0 copy-start.1
  15.4 0.0 copy-start.3
  15.4 0.5 shard_map.148.partial
  15.9 0.0 collective-permute-done.1.other
  15.9 1.7 %copy-done.1 = bf16[1024,2048]{1,0:T(8,128)(2,1)S(1)} copy-done((bf16[1024,2048]{1,0:T(8,128)(2,1)S(1)}, bf16[1024,2048]{1,0:T(8,128)(2,1)}, u32[]{:S(2)}) %copy-start.1) | copy-done | bytes 4194328
  17.6 0.0 copy-done.3
  17.6 0.0 copy-start.6
  17.6 1.3 %shard_map.149 = (bf16[128,2048]{1,0:T(8,128)(2,1)S(1)}, bf16[1024,1024]{1,0:T(8,128)(2,1)S(1)}) custom-call(s32[1]{0:T(128)} %bitcast.me, bf16[128,512]{1,0:T(8,128)(2,1)S(1)} %collective-permute-done.1.other, bf16[1024,2048]{1,0:T(8,128)(2,1)S(1)} %copy-done.1, f32[128,2048]{1,0:T(8,128)S(1)} %shard_map.148.partial, f32[1,2048]{1,0:T(1,128)S(1)} %bitcast.19, ...), custom_call_target="tpu_custom_call" | custom-call | flops 1000000000 | tf_op jit(solution)/shard_map/pallas_call | solution.py:42
  18.9 0.0 copy-start.4
  18.9 0.0 copy-start.5
  18.9 34.1 %all_to_all.10 = bf16[128,8,1024]{2,1,0:T(8,128)(2,1)S(1)} all-to-all(bf16[128,8,1024]{2,1,0:T(8,128)(2,1)S(1)} %bitcast.15), channel_id=1, replica_groups=mesh['sp'=64,'tp'=2] {'sp','tp'}, dimensions={0} | all-to-all | bytes 4194304 | tf_op jit(solution)/shard_map/all_to_all | solution.py:388
  53.1 0.0 copy-done.6
  53.1 0.0 copy-done.4
  53.1 0.0 copy-done.5
  53.1 3.5 %shard_map.150 = bf16[1024,1024]{1,0:T(8,128)(2,1)S(1)} custom-call(bf16[1024,1024]{1,0:T(8,128)(2,1)S(1)} %bitcast.17, bf16[2048,512]{1,0:T(8,128)(2,1)S(1)} %bitcast.20, bf16[2048,512]{1,0:T(8,128)(2,1)S(1)} %bitcast.21, bf16[512,2048]{1,0:T(8,128)(2,1)S(1)} %bitcast.22), custom_call_target="tpu_custom_call" | custom-call | flops 4000000000 | tf_op jit(solution)/shard_map/pallas_call | solution.py:42
  56.6 34.4 %all_to_all.11 = bf16[128,8,1024]{2,1,0:T(8,128)(2,1)S(1)} all-to-all(bf16[128,8,1024]{2,1,0:T(8,128)(2,1)S(1)} %bitcast.18), channel_id=1, replica_groups=mesh['sp'=64,'tp'=2] {'sp','tp'}, dimensions={0} | all-to-all | bytes 4194304 | tf_op jit(solution)/shard_map/all_to_all | solution.py:388
  91.0 1.5 %shard_map.151 = bf16[128,2048]{1,0:T(8,128)(2,1)} custom-call(bf16[1024,1024]{1,0:T(8,128)(2,1)S(1)} %bitcast.16, bf16[256,1024]{1,0:T(8,128)(2,1)S(1)} %get-tuple-element.29.picked, bf16[128,2048]{1,0:T(8,128)(2,1)S(1)} %get-tuple-element.30.base), custom_call_target="tpu_custom_call" | custom-call | flops 1000000000 | tf_op jit(solution)/shard_map/pallas_call | solution.py:42
Async XLA Ops:
  0.0 3.1 %copy-start.7 = (bf16[256,512]{1,0:T(8,128)(2,1)S(1)}, bf16[256,512]{1,0:T(8,128)(2,1)}, u32[]{:S(2)}) copy-start(bf16[256,512]{1,0:T(8,128)(2,1)} %value.1) | copy-start | bytes 786436
  0.0 3.1 %copy-start.8 = (bf16[256,512]{1,0:T(8,128)(2,1)S(1)}, bf16[256,512]{1,0:T(8,128)(2,1)}, u32[]{:S(2)}) copy-start(bf16[256,512]{1,0:T(8,128)(2,1)} %gate.1) | copy-start | bytes 786436
  1.0 10.6 %collective-permute-start = (bf16[32,512]{1,0:T(8,128)(2,1)S(1)}, bf16[32,512]{1,0:T(8,128)(2,1)S(1)}, u32[]{:S(2)}, u32[]{:S(2)}) collective-permute-start(bf16[32,512]{1,0:T(8,128)(2,1)S(1)} %get-tuple-element.24), channel_id=1, source_target_pairs={{0,2},{2,4},{4,6},{6,8},{8,10},{10,12},{12,14},{14,16},{16,18},{18... | collective-permute-start | bytes 98312 | tf_op jit(solution)/shard_map/ppermute | solution.py:339
  5.4 7.8 %copy-start.2 = (bf16[128,2048]{1,0:T(8,128)(2,1)S(1)}, bf16[128,2048]{1,0:T(8,128)(2,1)}, u32[]{:S(2)}) copy-start(bf16[128,2048]{1,0:T(8,128)(2,1)} %residual.1) | copy-start | bytes 1572868
  11.9 4.0 %collective-permute-start.1 = (bf16[128,512]{1,0:T(8,128)(2,1)S(1)}, bf16[128,512]{1,0:T(8,128)(2,1)S(1)}, u32[]{:S(2)}, u32[]{:S(2)}) collective-permute-start(bf16[128,512]{1,0:T(8,128)(2,1)S(1)} %shard_map.147), channel_id=1, source_target_pairs={{0,1},{1,0},{2,3},{3,2},{4,5},{5,4},{6,7},{7,6},{8,9},{9,8},{10,11... | collective-permute-start | bytes 393224 | tf_op jit(solution)/shard_map/ppermute | solution.py:365
  13.2 2.2 %copy-start = (bf16[1024,2048]{1,0:T(8,128)(2,1)S(1)}, bf16[1024,2048]{1,0:T(8,128)(2,1)}, u32[]{:S(2)}) copy-start(bf16[1024,2048]{1,0:T(8,128)(2,1)} %weight.3) | copy-start | bytes 12582916
  15.4 2.2 %copy-start.1 = (bf16[1024,2048]{1,0:T(8,128)(2,1)S(1)}, bf16[1024,2048]{1,0:T(8,128)(2,1)}, u32[]{:S(2)}) copy-start(bf16[1024,2048]{1,0:T(8,128)(2,1)} %weight.3) | copy-start | bytes 12582916
  15.4 2.2 %copy-start.3 = (f32[2048]{0:T(1024)S(1)}, f32[2048]{0:T(1024)}, u32[]{:S(2)}) copy-start(f32[2048]{0:T(1024)} %param.23) | copy-start | bytes 24580
  17.6 35.5 %copy-start.6 = (bf16[1,512,2048]{2,1,0:T(8,128)(2,1)S(1)}, bf16[1,512,2048]{2,1,0:T(8,128)(2,1)}, u32[]{:S(2)}) copy-start(bf16[1,512,2048]{2,1,0:T(8,128)(2,1)} %param.29) | copy-start | bytes 6291460
  18.9 34.2 %copy-start.4 = (bf16[1,2048,512]{2,1,0:T(8,128)(2,1)S(1)}, bf16[1,2048,512]{2,1,0:T(8,128)(2,1)}, u32[]{:S(2)}) copy-start(bf16[1,2048,512]{2,1,0:T(8,128)(2,1)} %param.27) | copy-start | bytes 6291460
  18.9 34.1 %copy-start.5 = (bf16[1,2048,512]{2,1,0:T(8,128)(2,1)S(1)}, bf16[1,2048,512]{2,1,0:T(8,128)(2,1)}, u32[]{:S(2)}) copy-start(bf16[1,2048,512]{2,1,0:T(8,128)(2,1)} %param.28) | copy-start | bytes 6291460

commit v11 on v10

--- a/solution.py
+++ b/solution.py
@@ -94,26 +94,12 @@
         picked[q * tokens : (q + 1) * tokens, :] = jnp.where(part == q, share, 0.0).astype(BF16)
 
 
-def load_body(
-    value_in, gate_in, kernel_in, bias_in, gain_in, shift_in, pick_in, logits_in, prob_in,
-    tail, kernel, vecs, pick, logits, prob,
-    value, gate, sems,
-):
-    cut = value_in.shape[0] - HALO
-    copies = fetch(
-        (
-            value_in.at[pl.ds(cut, HALO), :], gate_in.at[pl.ds(cut, HALO), :],
-            kernel_in, bias_in, gain_in, shift_in, pick_in, logits_in, prob_in,
-        ),
-        (value, gate, kernel, vecs.at[0:1], vecs.at[1:2], vecs.at[2:3], pick, logits, prob),
-        sems,
-    )
-    for copy in copies[:2]:
+def tail_body(value_in, gate_in, tail, value, gate, sems):
+    last = pl.ds(value_in.shape[0] - HALO, HALO)
+    for copy in fetch((value_in.at[last, :], gate_in.at[last, :]), (value, gate), sems):
         copy.wait()
     glued = value[...].astype(F32) * jax.nn.sigmoid(gate[...].astype(F32))
     tail[...] = glued.astype(BF16)
-    for copy in copies[2:]:
-        copy.wait()
 
 
 def taps_and_norm(ext, taps, vecs, b, start, rows, n_taps):
@@ -130,10 +116,12 @@
 
 
 def conv_body(
-    value, gate, kernel, vecs, pick, logits, prob,
-    mixed, ext, taps, spread, picked,
+    value, gate, kernel, bias, gain, shift, pick, logits, prob,
+    mixed, ext, taps, vecs, spread, picked,
     cols,
 ):
+    for i, row in enumerate((bias, gain, shift)):
+        vecs[i : i + 1, :] = row[...]
     n_taps, width = kernel.shape
     blocks, length, _ = ext.shape
     for b in range(blocks):
@@ -306,25 +294,36 @@
     step = model // PARTS
     rows = experts * RANKS * PARTS
     message = shape((rows, step), BF16)
-    tail, kernel, vecs, pick, logits, prob = call(
-        load_body,
-        (
-            shape((HALO, width), BF16),
-            shape((n_taps, width), BF16),
-            shape((8, width), F32),
-            shape((2, tokens), jnp.int32),
-            shape((2, tokens), F32),
-            shape((1, tokens), F32),
-        ),
+    (tail,) = call(
+        tail_body,
+        (shape((HALO, width), BF16),),
         scratch=(
             pltpu.VMEM((HALO, width), BF16),
             pltpu.VMEM((HALO, width), BF16),
-            pltpu.SemaphoreType.DMA((9,)),
+            pltpu.SemaphoreType.DMA((2,)),
         ),
-        hbm=range(9),
+        hbm=range(2),
+        n_in=2,
+        limit=4,
+        flops=5_000_000_000,
+    )(glu_value, glu_gate)
+    halo = lax.ppermute(tail, "sp", [(i, (i + 1) % peers) for i in range(peers)])
+    half = length // 2
+    ext_shape = (blocks, 2 * HALO, LANE)
+    mixed, ext, taps, vecs, spread, picked = call(
+        conv_body,
+        (
+            shape((length, width), BF16),
+            shape((blocks, length, LANE), F32),
+            shape((blocks, 32, LANE), F32),
+            shape((8, width), F32),
+            shape((rows, PARTS * tokens), BF16),
+            shape((PARTS * tokens, rows), BF16),
+        ),
+        scratch=(pltpu.VMEM((tokens, LANE), F32),),
         n_in=9,
         limit=4,
-        flops=5_000_000_000,
+        flops=6_000_000_000,
     )(
         glu_value,
         glu_gate,
@@ -336,23 +335,6 @@
         pair_logits.T,
         group_prob.reshape(1, tokens),
     )
-    halo = lax.ppermute(tail, "sp", [(i, (i + 1) % peers) for i in range(peers)])
-    half = length // 2
-    ext_shape = (blocks, 2 * HALO, LANE)
-    mixed, ext, taps, spread, picked = call(
-        conv_body,
-        (
-            shape((length, width), BF16),
-            shape((blocks, length, LANE), F32),
-            shape((blocks, 32, LANE), F32),
-            shape((rows, PARTS * tokens), BF16),
-            shape((PARTS * tokens, rows), BF16),
-        ),
-        scratch=(pltpu.VMEM((tokens, LANE), F32),),
-        n_in=7,
-        limit=4,
-        flops=6_000_000_000,
-    )(glu_value, glu_gate, kernel, vecs, pick, logits, prob)
     (theirs,) = call(
         functools.partial(give_body, cores, n_taps),
         (shape((half, width), BF16),),

time: 92.6 us -> 92.6 us (level)
    unnamed x18 -> x32, local copies, waits for them, and re-layouts: 3.91 us -> 3.95 us
where the time goes in v11:
time: 92.6 us; the launch traced here: 92.5 us
  blocking collectives  68.6 us (74%)
  Pallas kernels  10.3 us (11%)
  waiting for transfers between devices  6.1 us (7%)
  local copies, waits for them, and re-layouts  3.95 us (4%)
  starting transfers between devices  3.4 us (4%)
    all_to_all x2, blocking collectives, exchange(): return lax.all_to_all(x, ('sp', 'tp'), 0, 0, tiled=True).reshape(rows, step)  68.6 us
    pallas_call x7, Pallas kernels, call(): run(*(pltpu.with_memory_space_constraint(a, pltpu.HBM) if i in hbm else a...  10.3 us
    ppermute x1, waiting for transfers between devices, local(): lax.ppermute(tail, 'sp', [(i, (i + 1) % peers) for i in range(peers)])  6.1 us
    unnamed x32, local copies, waits for them, and re-layouts  3.95 us
    ppermute x1, starting transfers between devices, local(): lax.ppermute(tail, 'sp', [(i, (i + 1) % peers) for i in range(peers)])  2.1 us
  transfers between devices with their start and end apart: 2, of which 1 were waited for; matrix products, arithmetic and copies ran while one was open for 0% of the time, Pallas kernels for 3%

profile of v11, /device:TPU:1, one launch (start us, length us, event | category | flops | bytes accessed | tf_op | source)
XLA Modules:
  0.0 92.5 jit_solution(9658657931470804908)
XLA Ops:
  0.0 0.0 copy-start.8
  0.0 0.0 copy-start.7
  0.0 0.0 copy-start.15
  0.0 0.0 copy-start.14
  0.0 0.0 copy-start.13
  0.0 0.0 copy-start.12
  0.0 0.0 copy-start.11
  0.0 0.0 copy-start.10
  0.1 0.0 copy-start.9
  0.1 0.9 shard_map.146
  0.9 2.1 %collective-permute-start = (bf16[32,512]{1,0:T(8,128)(2,1)S(1)}, bf16[32,512]{1,0:T(8,128)(2,1)S(1)}, u32[]{:S(2)}, u32[]{:S(2)}) collective-permute-start(bf16[32,512]{1,0:T(8,128)(2,1)S(1)} %shard_map.146), channel_id=1, source_target_pairs={{0,2},{2,4},{4,6},{6,8},{8,10},{10,12},{12,14},{14,16},{16,18},{18... | collective-permute-start | bytes 98312 | tf_op jit(solution)/shard_map/ppermute | solution.py:310
  3.0 0.0 copy-done.8
  3.0 0.0 copy-done.7
  3.0 0.0 copy-done.15
  3.0 0.0 copy-done.14
  3.0 0.0 copy-done.13
  3.1 0.0 copy-done.12
  3.1 0.0 copy-done.11
  3.1 0.0 copy-done.10
  3.1 0.0 copy-done.9
  3.1 2.3 %shard_map.145 = (bf16[256,512]{1,0:T(8,128)(2,1)S(1)}, f32[4,256,128]{2,1,0:T(8,128)S(1)}, f32[4,32,128]{2,1,0:T(8,128)S(1)}, f32[8,512]{1,0:T(8,128)S(1)}, bf1...) custom-call(bf16[256,512]{1,0:T(8,128)(2,1)S(1)} %copy-done.7, bf16[256,512]{1,0:T(8,128)(2,1)S(1)} %copy-done.8, ...), custom_call_target="tpu_custom_call" | custom-call | flops 6000000000 | tf_op jit(solution)/shard_map/pallas_call | solution.py:42
  5.4 0.0 copy-start.2
  5.4 6.1 %collective-permute-done.halo = bf16[32,512]{1,0:T(8,128)(2,1)S(1)} collective-permute-done((bf16[32,512]{1,0:T(8,128)(2,1)S(1)}, bf16[32,512]{1,0:T(8,128)(2,1)S(1)}, u32[]{:S(2)}, u32[]{:S(2)}) %collective-permute-start) | collective-permute-done | bytes 32800 | tf_op jit(solution)/shard_map/ppermute | solution.py:310
  11.5 0.3 shard_map.147
  11.9 1.3 %collective-permute-start.1 = (bf16[128,512]{1,0:T(8,128)(2,1)S(1)}, bf16[128,512]{1,0:T(8,128)(2,1)S(1)}, u32[]{:S(2)}, u32[]{:S(2)}) collective-permute-start(bf16[128,512]{1,0:T(8,128)(2,1)S(1)} %shard_map.147), channel_id=1, source_target_pairs={{0,1},{1,0},{2,3},{3,2},{4,5},{5,4},{6,7},{7,6},{8,9},{9,8},{10,11... | collective-permute-start | bytes 393224 | tf_op jit(solution)/shard_map/ppermute | solution.py:347
  13.2 0.0 copy-done.2
  13.2 0.0 copy-start
  13.2 2.2 %copy-done = bf16[1024,2048]{1,0:T(8,128)(2,1)S(1)} copy-done((bf16[1024,2048]{1,0:T(8,128)(2,1)S(1)}, bf16[1024,2048]{1,0:T(8,128)(2,1)}, u32[]{:S(2)}) %copy-start) | copy-done | bytes 4194328
  15.4 0.0 copy-start.1
  15.4 0.0 copy-start.3
  15.4 0.5 shard_map.148.partial
  15.8 0.0 collective-permute-done.1.other
  15.9 1.7 %copy-done.1 = bf16[1024,2048]{1,0:T(8,128)(2,1)S(1)} copy-done((bf16[1024,2048]{1,0:T(8,128)(2,1)S(1)}, bf16[1024,2048]{1,0:T(8,128)(2,1)}, u32[]{:S(2)}) %copy-start.1) | copy-done | bytes 4194328
  17.6 0.0 copy-done.3
  17.6 0.0 copy-start.6
  17.6 1.3 %shard_map.149 = (bf16[128,2048]{1,0:T(8,128)(2,1)S(1)}, bf16[1024,1024]{1,0:T(8,128)(2,1)S(1)}) custom-call(s32[1]{0:T(128)} %bitcast.me, bf16[128,512]{1,0:T(8,128)(2,1)S(1)} %collective-permute-done.1.other, bf16[1024,2048]{1,0:T(8,128)(2,1)S(1)} %copy-done.1, f32[128,2048]{1,0:T(8,128)S(1)} %shard_map.148.partial, f32[1,2048]{1,0:T(1,128)S(1)} %bitcast.19, ...), custom_call_target="tpu_custom_call" | custom-call | flops 1000000000 | tf_op jit(solution)/shard_map/pallas_call | solution.py:42
  18.9 0.0 copy-start.4
  18.9 0.0 copy-start.5
  18.9 34.2 %all_to_all.10 = bf16[128,8,1024]{2,1,0:T(8,128)(2,1)S(1)} all-to-all(bf16[128,8,1024]{2,1,0:T(8,128)(2,1)S(1)} %bitcast.15), channel_id=1, replica_groups=mesh['sp'=64,'tp'=2] {'sp','tp'}, dimensions={0} | all-to-all | bytes 4194304 | tf_op jit(solution)/shard_map/all_to_all | solution.py:370
  53.1 0.0 copy-done.6
  53.1 0.0 copy-done.4
  53.1 0.0 copy-done.5
  53.1 3.5 %shard_map.150 = bf16[1024,1024]{1,0:T(8,128)(2,1)S(1)} custom-call(bf16[1024,1024]{1,0:T(8,128)(2,1)S(1)} %bitcast.17, bf16[2048,512]{1,0:T(8,128)(2,1)S(1)} %bitcast.20, bf16[2048,512]{1,0:T(8,128)(2,1)S(1)} %bitcast.21, bf16[512,2048]{1,0:T(8,128)(2,1)S(1)} %bitcast.22), custom_call_target="tpu_custom_call" | custom-call | flops 4000000000 | tf_op jit(solution)/shard_map/pallas_call | solution.py:42
  56.6 34.4 %all_to_all.11 = bf16[128,8,1024]{2,1,0:T(8,128)(2,1)S(1)} all-to-all(bf16[128,8,1024]{2,1,0:T(8,128)(2,1)S(1)} %bitcast.18), channel_id=1, replica_groups=mesh['sp'=64,'tp'=2] {'sp','tp'}, dimensions={0} | all-to-all | bytes 4194304 | tf_op jit(solution)/shard_map/all_to_all | solution.py:370
  91.0 1.5 %shard_map.151 = bf16[128,2048]{1,0:T(8,128)(2,1)} custom-call(bf16[1024,1024]{1,0:T(8,128)(2,1)S(1)} %bitcast.16, bf16[256,1024]{1,0:T(8,128)(2,1)S(1)} %get-tuple-element.19.picked, bf16[128,2048]{1,0:T(8,128)(2,1)S(1)} %get-tuple-element.20.base), custom_call_target="tpu_custom_call" | custom-call | flops 1000000000 | tf_op jit(solution)/shard_map/pallas_call | solution.py:42
Async XLA Ops:
  0.0 3.0 %copy-start.8 = (bf16[256,512]{1,0:T(8,128)(2,1)S(1)}, bf16[256,512]{1,0:T(8,128)(2,1)}, u32[]{:S(2)}) copy-start(bf16[256,512]{1,0:T(8,128)(2,1)} %gate_in.1) | copy-start | bytes 786436
  0.0 3.0 %copy-start.7 = (bf16[256,512]{1,0:T(8,128)(2,1)S(1)}, bf16[256,512]{1,0:T(8,128)(2,1)}, u32[]{:S(2)}) copy-start(bf16[256,512]{1,0:T(8,128)(2,1)} %value_in.1) | copy-start | bytes 786436
  0.0 3.0 %copy-start.15 = (f32[128]{0:T(128)S(1)}, f32[128]{0:T(128)}, u32[]{:S(2)}) copy-start(f32[128]{0:T(128)} %param.26) | copy-start | bytes 1540
  0.0 3.0 %copy-start.14 = (f32[128,2]{0,1:T(2,128)S(1)}, f32[128,2]{0,1:T(2,128)}, u32[]{:S(2)}) copy-start(f32[128,2]{0,1:T(2,128)} %param.25) | copy-start | bytes 3076
  0.0 3.0 %copy-start.13 = (s32[128,2]{0,1:T(2,128)S(1)}, s32[128,2]{0,1:T(2,128)}, u32[]{:S(2)}) copy-start(s32[128,2]{0,1:T(2,128)} %param.24) | copy-start | bytes 3076
  0.0 3.0 %copy-start.12 = (f32[512]{0:T(512)S(1)}, f32[512]{0:T(512)}, u32[]{:S(2)}) copy-start(f32[512]{0:T(512)} %param.20) | copy-start | bytes 6148
  0.0 3.0 %copy-start.11 = (f32[512]{0:T(512)S(1)}, f32[512]{0:T(512)}, u32[]{:S(2)}) copy-start(f32[512]{0:T(512)} %param.19) | copy-start | bytes 6148
  0.0 3.0 %copy-start.10 = (f32[512]{0:T(512)S(1)}, f32[512]{0:T(512)}, u32[]{:S(2)}) copy-start(f32[512]{0:T(512)} %param.18) | copy-start | bytes 6148
  0.1 3.0 %copy-start.9 = (bf16[31,512]{1,0:T(8,128)(2,1)S(1)}, bf16[31,512]{1,0:T(8,128)(2,1)}, u32[]{:S(2)}) copy-start(bf16[31,512]{1,0:T(8,128)(2,1)} %kernel.1) | copy-start | bytes 95236
  0.9 10.6 %collective-permute-start = (bf16[32,512]{1,0:T(8,128)(2,1)S(1)}, bf16[32,512]{1,0:T(8,128)(2,1)S(1)}, u32[]{:S(2)}, u32[]{:S(2)}) collective-permute-start(bf16[32,512]{1,0:T(8,128)(2,1)S(1)} %shard_map.146), channel_id=1, source_target_pairs={{0,2},{2,4},{4,6},{6,8},{8,10},{10,12},{12,14},{14,16},{16,18},{18... | collective-permute-start | bytes 98312 | tf_op jit(solution)/shard_map/ppermute | solution.py:310
  5.4 7.8 %copy-start.2 = (bf16[128,2048]{1,0:T(8,128)(2,1)S(1)}, bf16[128,2048]{1,0:T(8,128)(2,1)}, u32[]{:S(2)}) copy-start(bf16[128,2048]{1,0:T(8,128)(2,1)} %residual.1) | copy-start | bytes 1572868
  11.9 4.0 %collective-permute-start.1 = (bf16[128,512]{1,0:T(8,128)(2,1)S(1)}, bf16[128,512]{1,0:T(8,128)(2,1)S(1)}, u32[]{:S(2)}, u32[]{:S(2)}) collective-permute-start(bf16[128,512]{1,0:T(8,128)(2,1)S(1)} %shard_map.147), channel_id=1, source_target_pairs={{0,1},{1,0},{2,3},{3,2},{4,5},{5,4},{6,7},{7,6},{8,9},{9,8},{10,11... | collective-permute-start | bytes 393224 | tf_op jit(solution)/shard_map/ppermute | solution.py:347
  13.2 2.2 %copy-start = (bf16[1024,2048]{1,0:T(8,128)(2,1)S(1)}, bf16[1024,2048]{1,0:T(8,128)(2,1)}, u32[]{:S(2)}) copy-start(bf16[1024,2048]{1,0:T(8,128)(2,1)} %weight.3) | copy-start | bytes 12582916
  15.4 2.2 %copy-start.1 = (bf16[1024,2048]{1,0:T(8,128)(2,1)S(1)}, bf16[1024,2048]{1,0:T(8,128)(2,1)}, u32[]{:S(2)}) copy-start(bf16[1024,2048]{1,0:T(8,128)(2,1)} %weight.3) | copy-start | bytes 12582916
  15.4 2.2 %copy-start.3 = (f32[2048]{0:T(1024)S(1)}, f32[2048]{0:T(1024)}, u32[]{:S(2)}) copy-start(f32[2048]{0:T(1024)} %param.23) | copy-start | bytes 24580
  17.6 35.6 %copy-start.6 = (bf16[1,512,2048]{2,1,0:T(8,128)(2,1)S(1)}, bf16[1,512,2048]{2,1,0:T(8,128)(2,1)}, u32[]{:S(2)}) copy-start(bf16[1,512,2048]{2,1,0:T(8,128)(2,1)} %param.29) | copy-start | bytes 6291460
  18.9 34.2 %copy-start.4 = (bf16[1,2048,512]{2,1,0:T(8,128)(2,1)S(1)}, bf16[1,2048,512]{2,1,0:T(8,128)(2,1)}, u32[]{:S(2)}) copy-start(bf16[1,2048,512]{2,1,0:T(8,128)(2,1)} %param.27) | copy-start | bytes 6291460
  18.9 34.2 %copy-start.5 = (bf16[1,2048,512]{2,1,0:T(8,128)(2,1)S(1)}, bf16[1,2048,512]{2,1,0:T(8,128)(2,1)}, u32[]{:S(2)}) copy-start(bf16[1,2048,512]{2,1,0:T(8,128)(2,1)} %param.28) | copy-start | bytes 6291460

commit v12 on v11

--- a/solution.py
+++ b/solution.py
@@ -142,19 +142,19 @@
     lax.fori_loop(0, blocks, block, 0)
 
 
-def head(me, cores, halo, front, taps, vecs, ext, out, n_taps):
+def head(halo, front, taps, vecs, ext, out, n_taps):
     for b in range(ext.shape[0]):
         lanes = slice(b * LANE, (b + 1) * LANE)
-        ext[b, 0:HALO, :] = jnp.where(me[0] >= cores, halo[:, lanes].astype(F32), 0.0)
+        ext[b, 0:HALO, :] = jnp.where(lax.axis_index("sp") > 0, halo[:, lanes].astype(F32), 0.0)
         ext[b, HALO : 2 * HALO, :] = front[b, 0:HALO, :]
     for b in range(ext.shape[0]):
         lanes = slice(b * LANE, (b + 1) * LANE)
         out[0:HALO, lanes] = taps_and_norm(ext, taps, vecs, b, 0, HALO, n_taps)
 
 
-def give_body(cores, n_taps, me, mixed, halo, front, taps, vecs, theirs, ext):
+def give_body(n_taps, mixed, halo, front, taps, vecs, theirs, ext):
     half = theirs.shape[0]
-    core = lax.rem(me[0], cores)
+    core = lax.axis_index("tp")
 
     @pl.when(core == 0)
     def _():
@@ -163,18 +163,18 @@
     @pl.when(core != 0)
     def _():
         theirs[...] = mixed[0:half, :]
-        head(me, cores, halo, front, taps, vecs, ext, theirs, n_taps)
-
-
-def own_body(cores, n_taps, me, mixed, halo, front, taps, vecs, weight, residual, partial, ext, mine):
+        head(halo, front, taps, vecs, ext, theirs, n_taps)
+
+
+def own_body(n_taps, mixed, halo, front, taps, vecs, weight, residual, partial, ext, mine):
     half, width = mine.shape
     step = partial.shape[1] // 4
-    core = lax.rem(me[0], cores)
+    core = lax.axis_index("tp")
 
     @pl.when(core == 0)
     def _():
         mine[...] = mixed[0:half, :]
-        head(me, cores, halo, front, taps, vecs, ext, mine, n_taps)
+        head(halo, front, taps, vecs, ext, mine, n_taps)
 
     @pl.when(core != 0)
     def _():
@@ -187,11 +187,11 @@
         partial[:, lanes] = acc + residual[:, lanes].astype(F32)
 
 
-def project_body(cores, me, other, weight, partial, gain, spread, hidden, out, stacked):
+def project_body(other, weight, partial, gain, spread, hidden, out, stacked):
     tokens, half = other.shape
     width = partial.shape[1]
     step = width // 4
-    there = pl.ds(pl.multiple_of((1 - lax.rem(me[0], cores)) * half, half), half)
+    there = pl.ds(pl.multiple_of((1 - lax.axis_index("tp")) * half, half), half)
     total = jnp.zeros((tokens, 1), F32)
     for q in range(4):
         lanes = slice(q * step, (q + 1) * step)
@@ -286,11 +286,9 @@
     tokens, model = residual.shape
     experts = lax.axis_size("sp") * lax.axis_size("tp")
     peers = lax.axis_size("sp")
-    me = lax.axis_index(("sp", "tp")).astype(jnp.int32).reshape(1)
 
     n_taps = conv_kernel.shape[0]
     blocks = width // LANE
-    cores = lax.axis_size("tp")
     step = model // PARTS
     rows = experts * RANKS * PARTS
     message = shape((rows, step), BF16)
@@ -336,33 +334,30 @@
         group_prob.reshape(1, tokens),
     )
     (theirs,) = call(
-        functools.partial(give_body, cores, n_taps),
+        functools.partial(give_body, n_taps),
         (shape((half, width), BF16),),
         scratch=(pltpu.VMEM(ext_shape, F32),),
-        smem=(0,),
-        n_in=6,
+        n_in=5,
         limit=4,
         flops=500_000_000,
-    )(me, mixed, halo, ext, taps, vecs)
+    )(mixed, halo, ext, taps, vecs)
     other = lax.ppermute(theirs, "tp", [(0, 1), (1, 0)])
     (partial,) = call(
-        functools.partial(own_body, cores, n_taps),
+        functools.partial(own_body, n_taps),
         (shape((tokens, model), F32),),
         scratch=(pltpu.VMEM(ext_shape, F32), pltpu.VMEM((half, width), BF16)),
-        smem=(0,),
-        n_in=8,
+        n_in=7,
         limit=4,
         flops=500_000_000,
-    )(me, mixed, halo, ext, taps, vecs, out_weight, residual)
+    )(mixed, halo, ext, taps, vecs, out_weight, residual)
     hidden, send = call(
-        functools.partial(project_body, cores),
+        project_body,
         (shape((tokens, model), BF16), message),
         scratch=(pltpu.VMEM((PARTS * tokens, step), BF16),),
-        smem=(0,),
-        n_in=6,
+        n_in=5,
         limit=16,
         flops=1_000_000_000,
-    )(me, other, out_weight, partial, ffn_gain.reshape(1, model), spread)
+    )(other, out_weight, partial, ffn_gain.reshape(1, model), spread)
     flat = pltpu.VMEM((RANKS * experts, model), BF16)
 
     def exchange(x):

time: 92.6 us -> 89.1 us (0.962)
  local copies, waits for them, and re-layouts: 3.95 us -> 0.07 us
    unnamed x32 -> x30, local copies, waits for them, and re-layouts: 3.95 us -> 0.07 us
  transfers between devices with their start and end apart: 2 -> 2, of which waited for: 1 -> 2; matrix products, arithmetic and copies ran while one was open for 0% -> 0% of each run, Pallas kernels for 3% -> 3%
where the time goes in v12:
time: 89.1 us; the launch traced here: 89 us
  blocking collectives  68.5 us (77%)
  Pallas kernels  10.3 us (12%)
  waiting for transfers between devices  6.57 us (7%)
  starting transfers between devices  3.4 us (4%)
    all_to_all x2, blocking collectives, exchange(): return lax.all_to_all(x, ('sp', 'tp'), 0, 0, tiled=True).reshape(rows, step)  68.5 us
    pallas_call x7, Pallas kernels, call(): run(*(pltpu.with_memory_space_constraint(a, pltpu.HBM) if i in hbm else a...  10.3 us
    ppermute x1, waiting for transfers between devices, local(): lax.ppermute(tail, 'sp', [(i, (i + 1) % peers) for i in range(peers)])  6.06 us
    ppermute x1, starting transfers between devices, local(): lax.ppermute(tail, 'sp', [(i, (i + 1) % peers) for i in range(peers)])  2.1 us
  transfers between devices with their start and end apart: 2, of which 2 were waited for; matrix products, arithmetic and copies ran while one was open for 0% of the time, Pallas kernels for 3%

profile of v12, /device:TPU:1, one launch (start us, length us, event | category | flops | bytes accessed | tf_op | source)
XLA Modules:
  0.0 89.0 jit_solution(8573708665631323526)
XLA Ops:
  0.0 0.0 copy-start.7
  0.0 0.0 copy-start.6
  0.0 0.0 copy-start.14
  0.0 0.0 copy-start.13
  0.0 0.0 copy-start.12
  0.0 0.0 copy-start.11
  0.0 0.0 copy-start.10
  0.0 0.0 copy-start.9
  0.1 0.0 copy-start.8
  0.1 0.9 shard_map.146
  0.9 2.1 %collective-permute-start = (bf16[32,512]{1,0:T(8,128)(2,1)S(1)}, bf16[32,512]{1,0:T(8,128)(2,1)S(1)}, u32[]{:S(2)}, u32[]{:S(2)}) collective-permute-start(bf16[32,512]{1,0:T(8,128)(2,1)S(1)} %shard_map.146), channel_id=1, source_target_pairs={{0,2},{2,4},{4,6},{6,8},{8,10},{10,12},{12,14},{14,16},{16,18},{18... | collective-permute-start | bytes 98312 | tf_op jit(solution)/shard_map/ppermute | solution.py:308
  3.0 0.0 copy-done.7
  3.0 0.0 copy-done.6
  3.0 0.0 copy-done.14
  3.0 0.0 copy-done.13
  3.0 0.0 copy-done.12
  3.1 0.0 copy-done.11
  3.1 0.0 copy-done.10
  3.1 0.0 copy-done.9
  3.1 0.0 copy-done.8
  3.1 0.0 copy-start
  3.1 2.3 %shard_map.145 = (bf16[256,512]{1,0:T(8,128)(2,1)S(1)}, f32[4,256,128]{2,1,0:T(8,128)S(1)}, f32[4,32,128]{2,1,0:T(8,128)S(1)}, f32[8,512]{1,0:T(8,128)S(1)}, bf1...) custom-call(bf16[256,512]{1,0:T(8,128)(2,1)S(1)} %copy-done.6, bf16[256,512]{1,0:T(8,128)(2,1)S(1)} %copy-done.7, ...), custom_call_target="tpu_custom_call" | custom-call | flops 6000000000 | tf_op jit(solution)/shard_map/pallas_call | solution.py:42
  5.5 0.0 copy-start.1
  5.5 6.1 %collective-permute-done.halo = bf16[32,512]{1,0:T(8,128)(2,1)S(1)} collective-permute-done((bf16[32,512]{1,0:T(8,128)(2,1)S(1)}, bf16[32,512]{1,0:T(8,128)(2,1)S(1)}, u32[]{:S(2)}, u32[]{:S(2)}) %collective-permute-start) | collective-permute-done | bytes 32800 | tf_op jit(solution)/shard_map/ppermute | solution.py:308
  11.5 0.3 shard_map.147
  11.9 0.0 copy-start.2
  11.9 1.3 %collective-permute-start.1 = (bf16[128,512]{1,0:T(8,128)(2,1)S(1)}, bf16[128,512]{1,0:T(8,128)(2,1)S(1)}, u32[]{:S(2)}, u32[]{:S(2)}) collective-permute-start(bf16[128,512]{1,0:T(8,128)(2,1)S(1)} %shard_map.147), channel_id=1, source_target_pairs={{0,1},{1,0},{2,3},{3,2},{4,5},{5,4},{6,7},{7,6},{8,9},{9,8},{10,11... | collective-permute-start | bytes 393224 | tf_op jit(solution)/shard_map/ppermute | solution.py:344
  13.2 0.0 copy-done
  13.2 0.0 copy-done.1
  13.2 0.5 shard_map.148.partial
  13.7 0.5 collective-permute-done.1.other
  14.2 0.0 copy-done.2
  14.2 0.0 copy-start.5
  14.2 1.3 %shard_map.149 = (bf16[128,2048]{1,0:T(8,128)(2,1)S(1)}, bf16[1024,1024]{1,0:T(8,128)(2,1)S(1)}) custom-call(bf16[128,512]{1,0:T(8,128)(2,1)S(1)} %collective-permute-done.1.other, bf16[1024,2048]{1,0:T(8,128)(2,1)S(1)} %copy-done, f32[128,2048]{1,0:T(8,128)S(1)} %shard_map.148.partial, f32[1,2048]{1,0:T(1,128)S(1)} %bitcast.18, ...), custom_call_target="tpu_custom_call" | custom-call | flops 1000000000 | tf_op jit(solution)/shard_map/pallas_call | solution.py:42
  15.5 0.0 copy-start.3
  15.5 0.0 copy-start.4
  15.5 34.1 %all_to_all.10 = bf16[128,8,1024]{2,1,0:T(8,128)(2,1)S(1)} all-to-all(bf16[128,8,1024]{2,1,0:T(8,128)(2,1)S(1)} %bitcast.14), channel_id=1, replica_groups=mesh['sp'=64,'tp'=2] {'sp','tp'}, dimensions={0} | all-to-all | bytes 4194304 | tf_op jit(solution)/shard_map/all_to_all | solution.py:365
  49.6 0.0 copy-done.5
  49.6 0.0 copy-done.3
  49.6 0.0 copy-done.4
  49.6 3.5 %shard_map.150 = bf16[1024,1024]{1,0:T(8,128)(2,1)S(1)} custom-call(bf16[1024,1024]{1,0:T(8,128)(2,1)S(1)} %bitcast.16, bf16[2048,512]{1,0:T(8,128)(2,1)S(1)} %bitcast.19, bf16[2048,512]{1,0:T(8,128)(2,1)S(1)} %bitcast.20, bf16[512,2048]{1,0:T(8,128)(2,1)S(1)} %bitcast.21), custom_call_target="tpu_custom_call" | custom-call | flops 4000000000 | tf_op jit(solution)/shard_map/pallas_call | solution.py:42
  53.1 34.4 %all_to_all.11 = bf16[128,8,1024]{2,1,0:T(8,128)(2,1)S(1)} all-to-all(bf16[128,8,1024]{2,1,0:T(8,128)(2,1)S(1)} %bitcast.17), channel_id=1, replica_groups=mesh['sp'=64,'tp'=2] {'sp','tp'}, dimensions={0} | all-to-all | bytes 4194304 | tf_op jit(solution)/shard_map/all_to_all | solution.py:365
  87.5 1.5 %shard_map.151 = bf16[128,2048]{1,0:T(8,128)(2,1)} custom-call(bf16[1024,1024]{1,0:T(8,128)(2,1)S(1)} %bitcast.15, bf16[256,1024]{1,0:T(8,128)(2,1)S(1)} %get-tuple-element.19.picked, bf16[128,2048]{1,0:T(8,128)(2,1)S(1)} %get-tuple-element.20.base), custom_call_target="tpu_custom_call" | custom-call | flops 1000000000 | tf_op jit(solution)/shard_map/pallas_call | solution.py:42
Async XLA Ops:
  0.0 3.0 %copy-start.7 = (bf16[256,512]{1,0:T(8,128)(2,1)S(1)}, bf16[256,512]{1,0:T(8,128)(2,1)}, u32[]{:S(2)}) copy-start(bf16[256,512]{1,0:T(8,128)(2,1)} %gate_in.1) | copy-start | bytes 786436
  0.0 3.0 %copy-start.6 = (bf16[256,512]{1,0:T(8,128)(2,1)S(1)}, bf16[256,512]{1,0:T(8,128)(2,1)}, u32[]{:S(2)}) copy-start(bf16[256,512]{1,0:T(8,128)(2,1)} %value_in.1) | copy-start | bytes 786436
  0.0 3.0 %copy-start.14 = (f32[128]{0:T(128)S(1)}, f32[128]{0:T(128)}, u32[]{:S(2)}) copy-start(f32[128]{0:T(128)} %param.26) | copy-start | bytes 1540
  0.0 3.0 %copy-start.13 = (f32[128,2]{0,1:T(2,128)S(1)}, f32[128,2]{0,1:T(2,128)}, u32[]{:S(2)}) copy-start(f32[128,2]{0,1:T(2,128)} %param.25) | copy-start | bytes 3076
  0.0 3.0 %copy-start.12 = (s32[128,2]{0,1:T(2,128)S(1)}, s32[128,2]{0,1:T(2,128)}, u32[]{:S(2)}) copy-start(s32[128,2]{0,1:T(2,128)} %param.24) | copy-start | bytes 3076
  0.0 3.0 %copy-start.11 = (f32[512]{0:T(512)S(1)}, f32[512]{0:T(512)}, u32[]{:S(2)}) copy-start(f32[512]{0:T(512)} %param.20) | copy-start | bytes 6148
  0.0 3.0 %copy-start.10 = (f32[512]{0:T(512)S(1)}, f32[512]{0:T(512)}, u32[]{:S(2)}) copy-start(f32[512]{0:T(512)} %param.19) | copy-start | bytes 6148
  0.0 3.0 %copy-start.9 = (f32[512]{0:T(512)S(1)}, f32[512]{0:T(512)}, u32[]{:S(2)}) copy-start(f32[512]{0:T(512)} %param.18) | copy-start | bytes 6148
  0.1 3.0 %copy-start.8 = (bf16[31,512]{1,0:T(8,128)(2,1)S(1)}, bf16[31,512]{1,0:T(8,128)(2,1)}, u32[]{:S(2)}) copy-start(bf16[31,512]{1,0:T(8,128)(2,1)} %kernel.1) | copy-start | bytes 95236
  0.9 10.6 %collective-permute-start = (bf16[32,512]{1,0:T(8,128)(2,1)S(1)}, bf16[32,512]{1,0:T(8,128)(2,1)S(1)}, u32[]{:S(2)}, u32[]{:S(2)}) collective-permute-start(bf16[32,512]{1,0:T(8,128)(2,1)S(1)} %shard_map.146), channel_id=1, source_target_pairs={{0,2},{2,4},{4,6},{6,8},{8,10},{10,12},{12,14},{14,16},{16,18},{18... | collective-permute-start | bytes 98312 | tf_op jit(solution)/shard_map/ppermute | solution.py:308
  3.1 10.1 %copy-start = (bf16[1024,2048]{1,0:T(8,128)(2,1)S(1)}, bf16[1024,2048]{1,0:T(8,128)(2,1)}, u32[]{:S(2)}) copy-start(bf16[1024,2048]{1,0:T(8,128)(2,1)} %weight.3) | copy-start | bytes 12582916
  5.5 7.7 %copy-start.1 = (bf16[128,2048]{1,0:T(8,128)(2,1)S(1)}, bf16[128,2048]{1,0:T(8,128)(2,1)}, u32[]{:S(2)}) copy-start(bf16[128,2048]{1,0:T(8,128)(2,1)} %residual.1) | copy-start | bytes 1572868
  11.9 2.3 %copy-start.2 = (f32[2048]{0:T(1024)S(1)}, f32[2048]{0:T(1024)}, u32[]{:S(2)}) copy-start(f32[2048]{0:T(1024)} %param.23) | copy-start | bytes 24580
  11.9 2.3 %collective-permute-start.1 = (bf16[128,512]{1,0:T(8,128)(2,1)S(1)}, bf16[128,512]{1,0:T(8,128)(2,1)S(1)}, u32[]{:S(2)}, u32[]{:S(2)}) collective-permute-start(bf16[128,512]{1,0:T(8,128)(2,1)S(1)} %shard_map.147), channel_id=1, source_target_pairs={{0,1},{1,0},{2,3},{3,2},{4,5},{5,4},{6,7},{7,6},{8,9},{9,8},{10,11... | collective-permute-start | bytes 393224 | tf_op jit(solution)/shard_map/ppermute | solution.py:344
  14.2 35.4 %copy-start.5 = (bf16[1,512,2048]{2,1,0:T(8,128)(2,1)S(1)}, bf16[1,512,2048]{2,1,0:T(8,128)(2,1)}, u32[]{:S(2)}) copy-start(bf16[1,512,2048]{2,1,0:T(8,128)(2,1)} %param.29) | copy-start | bytes 6291460
  15.5 34.1 %copy-start.3 = (bf16[1,2048,512]{2,1,0:T(8,128)(2,1)S(1)}, bf16[1,2048,512]{2,1,0:T(8,128)(2,1)}, u32[]{:S(2)}) copy-start(bf16[1,2048,512]{2,1,0:T(8,128)(2,1)} %param.27) | copy-start | bytes 6291460
  15.5 34.1 %copy-start.4 = (bf16[1,2048,512]{2,1,0:T(8,128)(2,1)S(1)}, bf16[1,2048,512]{2,1,0:T(8,128)(2,1)}, u32[]{:S(2)}) copy-start(bf16[1,2048,512]{2,1,0:T(8,128)(2,1)} %param.28) | copy-start | bytes 6291460

commit v13 on v12

--- a/solution.py
+++ b/solution.py
@@ -218,7 +218,7 @@
     return jnp.where(low, a, pltpu.roll(b, RANKS, 1)), jnp.where(low, pltpu.roll(a, RANKS, 1), b)
 
 
-def expert_body(message, gate, up, down, out, flat):
+def expert_body(message, gate, up, down, out, flat, active):
     rows, step = message.shape
     tile = RANKS * PARTS
     pairs = rows // (2 * tile)
@@ -229,14 +229,16 @@
         wide = message[:, here].astype(F32).reshape(pairs, 2, tile, size)
         for q, half in enumerate(trade(wide[:, 0], wide[:, 1])):
             flat[:, q * step + p * size : q * step + (p + 1) * size] = half.reshape(rows // 2, size).astype(BF16)
-    x = flat[...]
-    g = jnp.dot(x, gate[...], preferred_element_type=F32)
-    u = jnp.dot(x, up[...], preferred_element_type=F32)
-    active = (g / (1.0 + jnp.exp(-g)) * u).astype(BF16)
+    hidden = gate.shape[1]
+    for n in range(2):
+        units = slice(n * hidden // 2, (n + 1) * hidden // 2)
+        g = jnp.dot(flat[...], gate[:, units], preferred_element_type=F32)
+        u = jnp.dot(flat[...], up[:, units], preferred_element_type=F32)
+        active[:, units] = (g / (1.0 + jnp.exp(-g)) * u).astype(BF16)
     for p in range(pieces):
         halves = [
             jnp.dot(
-                active, down[:, q * step + p * size : q * step + (p + 1) * size], preferred_element_type=F32
+                active[...], down[:, q * step + p * size : q * step + (p + 1) * size], preferred_element_type=F32
             ).reshape(pairs, tile, size)
             for q in range(PARTS)
         ]
@@ -366,7 +368,12 @@
 
     got = exchange(send)
     (done,) = call(
-        expert_body, (message,), scratch=(flat,), n_in=4, limit=24, flops=4_000_000_000
+        expert_body,
+        (message,),
+        scratch=(flat, pltpu.VMEM((RANKS * experts, gate_weight.shape[2]), BF16)),
+        n_in=4,
+        limit=24,
+        flops=4_000_000_000,
     )(got, gate_weight[0], up_weight[0], down_weight[0])
     back = exchange(done)
     (result,) = call(

time: 89.1 us -> 89 us (level)
  no operation moved by 1% of the time
where the time goes in v13:
time: 89 us; the launch traced here: 88.9 us
  blocking collectives  68.4 us (77%)
  Pallas kernels  10.2 us (11%)
  waiting for transfers between devices  6.57 us (7%)
  starting transfers between devices  3.4 us (4%)
    all_to_all x2, blocking collectives, exchange(): return lax.all_to_all(x, ('sp', 'tp'), 0, 0, tiled=True).reshape(rows, step)  68.4 us
    pallas_call x7, Pallas kernels, call(): run(*(pltpu.with_memory_space_constraint(a, pltpu.HBM) if i in hbm else a...  10.2 us
    ppermute x1, waiting for transfers between devices, local(): lax.ppermute(tail, 'sp', [(i, (i + 1) % peers) for i in range(peers)])  6.06 us
    ppermute x1, starting transfers between devices, local(): lax.ppermute(tail, 'sp', [(i, (i + 1) % peers) for i in range(peers)])  2.1 us
  transfers between devices with their start and end apart: 2, of which 2 were waited for; matrix products, arithmetic and copies ran while one was open for 0% of the time, Pallas kernels for 3%

profile of v13, /device:TPU:1, one launch (start us, length us, event | category | flops | bytes accessed | tf_op | source)
XLA Modules:
  0.0 88.9 jit_solution(7069371824435845691)
XLA Ops:
  0.0 0.0 copy-start.7
  0.0 0.0 copy-start.6
  0.0 0.0 copy-start.14
  0.0 0.0 copy-start.13
  0.0 0.0 copy-start.12
  0.0 0.0 copy-start.11
  0.0 0.0 copy-start.10
  0.0 0.0 copy-start.9
  0.1 0.0 copy-start.8
  0.1 0.9 shard_map.146
  0.9 2.1 %collective-permute-start = (bf16[32,512]{1,0:T(8,128)(2,1)S(1)}, bf16[32,512]{1,0:T(8,128)(2,1)S(1)}, u32[]{:S(2)}, u32[]{:S(2)}) collective-permute-start(bf16[32,512]{1,0:T(8,128)(2,1)S(1)} %shard_map.146), channel_id=1, source_target_pairs={{0,2},{2,4},{4,6},{6,8},{8,10},{10,12},{12,14},{14,16},{16,18},{18... | collective-permute-start | bytes 98312 | tf_op jit(solution)/shard_map/ppermute | solution.py:310
  3.0 0.0 copy-done.7
  3.0 0.0 copy-done.6
  3.0 0.0 copy-done.14
  3.0 0.0 copy-done.13
  3.0 0.0 copy-done.12
  3.1 0.0 copy-done.11
  3.1 0.0 copy-done.10
  3.1 0.0 copy-done.9
  3.1 0.0 copy-done.8
  3.1 0.0 copy-start
  3.1 2.3 %shard_map.145 = (bf16[256,512]{1,0:T(8,128)(2,1)S(1)}, f32[4,256,128]{2,1,0:T(8,128)S(1)}, f32[4,32,128]{2,1,0:T(8,128)S(1)}, f32[8,512]{1,0:T(8,128)S(1)}, bf1...) custom-call(bf16[256,512]{1,0:T(8,128)(2,1)S(1)} %copy-done.6, bf16[256,512]{1,0:T(8,128)(2,1)S(1)} %copy-done.7, ...), custom_call_target="tpu_custom_call" | custom-call | flops 6000000000 | tf_op jit(solution)/shard_map/pallas_call | solution.py:42
  5.5 0.0 copy-start.1
  5.5 6.1 %collective-permute-done.halo = bf16[32,512]{1,0:T(8,128)(2,1)S(1)} collective-permute-done((bf16[32,512]{1,0:T(8,128)(2,1)S(1)}, bf16[32,512]{1,0:T(8,128)(2,1)S(1)}, u32[]{:S(2)}, u32[]{:S(2)}) %collective-permute-start) | collective-permute-done | bytes 32800 | tf_op jit(solution)/shard_map/ppermute | solution.py:310
  11.5 0.3 shard_map.147
  11.9 0.0 copy-start.2
  11.9 1.3 %collective-permute-start.1 = (bf16[128,512]{1,0:T(8,128)(2,1)S(1)}, bf16[128,512]{1,0:T(8,128)(2,1)S(1)}, u32[]{:S(2)}, u32[]{:S(2)}) collective-permute-start(bf16[128,512]{1,0:T(8,128)(2,1)S(1)} %shard_map.147), channel_id=1, source_target_pairs={{0,1},{1,0},{2,3},{3,2},{4,5},{5,4},{6,7},{7,6},{8,9},{9,8},{10,11... | collective-permute-start | bytes 393224 | tf_op jit(solution)/shard_map/ppermute | solution.py:346
  13.2 0.0 copy-done
  13.2 0.0 copy-done.1
  13.2 0.5 shard_map.148.partial
  13.7 0.5 collective-permute-done.1.other
  14.2 0.0 copy-done.2
  14.2 0.0 copy-start.5
  14.2 1.3 %shard_map.149 = (bf16[128,2048]{1,0:T(8,128)(2,1)S(1)}, bf16[1024,1024]{1,0:T(8,128)(2,1)S(1)}) custom-call(bf16[128,512]{1,0:T(8,128)(2,1)S(1)} %collective-permute-done.1.other, bf16[1024,2048]{1,0:T(8,128)(2,1)S(1)} %copy-done, f32[128,2048]{1,0:T(8,128)S(1)} %shard_map.148.partial, f32[1,2048]{1,0:T(1,128)S(1)} %bitcast.18, ...), custom_call_target="tpu_custom_call" | custom-call | flops 1000000000 | tf_op jit(solution)/shard_map/pallas_call | solution.py:42
  15.5 0.0 copy-start.3
  15.5 0.0 copy-start.4
  15.5 34.1 %all_to_all.10 = bf16[128,8,1024]{2,1,0:T(8,128)(2,1)S(1)} all-to-all(bf16[128,8,1024]{2,1,0:T(8,128)(2,1)S(1)} %bitcast.14), channel_id=1, replica_groups=mesh['sp'=64,'tp'=2] {'sp','tp'}, dimensions={0} | all-to-all | bytes 4194304 | tf_op jit(solution)/shard_map/all_to_all | solution.py:367
  49.6 0.0 copy-done.5
  49.6 0.0 copy-done.3
  49.6 0.0 copy-done.4
  49.6 3.4 %shard_map.150 = bf16[1024,1024]{1,0:T(8,128)(2,1)S(1)} custom-call(bf16[1024,1024]{1,0:T(8,128)(2,1)S(1)} %bitcast.16, bf16[2048,512]{1,0:T(8,128)(2,1)S(1)} %bitcast.19, bf16[2048,512]{1,0:T(8,128)(2,1)S(1)} %bitcast.20, bf16[512,2048]{1,0:T(8,128)(2,1)S(1)} %bitcast.21), custom_call_target="tpu_custom_call" | custom-call | flops 4000000000 | tf_op jit(solution)/shard_map/pallas_call | solution.py:42
  53.1 34.4 %all_to_all.11 = bf16[128,8,1024]{2,1,0:T(8,128)(2,1)S(1)} all-to-all(bf16[128,8,1024]{2,1,0:T(8,128)(2,1)S(1)} %bitcast.17), channel_id=1, replica_groups=mesh['sp'=64,'tp'=2] {'sp','tp'}, dimensions={0} | all-to-all | bytes 4194304 | tf_op jit(solution)/shard_map/all_to_all | solution.py:367
  87.4 1.5 %shard_map.151 = bf16[128,2048]{1,0:T(8,128)(2,1)} custom-call(bf16[1024,1024]{1,0:T(8,128)(2,1)S(1)} %bitcast.15, bf16[256,1024]{1,0:T(8,128)(2,1)S(1)} %get-tuple-element.19.picked, bf16[128,2048]{1,0:T(8,128)(2,1)S(1)} %get-tuple-element.20.base), custom_call_target="tpu_custom_call" | custom-call | flops 1000000000 | tf_op jit(solution)/shard_map/pallas_call | solution.py:42
Async XLA Ops:
  0.0 3.0 %copy-start.7 = (bf16[256,512]{1,0:T(8,128)(2,1)S(1)}, bf16[256,512]{1,0:T(8,128)(2,1)}, u32[]{:S(2)}) copy-start(bf16[256,512]{1,0:T(8,128)(2,1)} %gate_in.1) | copy-start | bytes 786436
  0.0 3.0 %copy-start.6 = (bf16[256,512]{1,0:T(8,128)(2,1)S(1)}, bf16[256,512]{1,0:T(8,128)(2,1)}, u32[]{:S(2)}) copy-start(bf16[256,512]{1,0:T(8,128)(2,1)} %value_in.1) | copy-start | bytes 786436
  0.0 3.0 %copy-start.14 = (f32[128]{0:T(128)S(1)}, f32[128]{0:T(128)}, u32[]{:S(2)}) copy-start(f32[128]{0:T(128)} %param.26) | copy-start | bytes 1540
  0.0 3.0 %copy-start.13 = (f32[128,2]{0,1:T(2,128)S(1)}, f32[128,2]{0,1:T(2,128)}, u32[]{:S(2)}) copy-start(f32[128,2]{0,1:T(2,128)} %param.25) | copy-start | bytes 3076
  0.0 3.0 %copy-start.12 = (s32[128,2]{0,1:T(2,128)S(1)}, s32[128,2]{0,1:T(2,128)}, u32[]{:S(2)}) copy-start(s32[128,2]{0,1:T(2,128)} %param.24) | copy-start | bytes 3076
  0.0 3.0 %copy-start.11 = (f32[512]{0:T(512)S(1)}, f32[512]{0:T(512)}, u32[]{:S(2)}) copy-start(f32[512]{0:T(512)} %param.20) | copy-start | bytes 6148
  0.0 3.0 %copy-start.10 = (f32[512]{0:T(512)S(1)}, f32[512]{0:T(512)}, u32[]{:S(2)}) copy-start(f32[512]{0:T(512)} %param.19) | copy-start | bytes 6148
  0.0 3.0 %copy-start.9 = (f32[512]{0:T(512)S(1)}, f32[512]{0:T(512)}, u32[]{:S(2)}) copy-start(f32[512]{0:T(512)} %param.18) | copy-start | bytes 6148
  0.1 3.0 %copy-start.8 = (bf16[31,512]{1,0:T(8,128)(2,1)S(1)}, bf16[31,512]{1,0:T(8,128)(2,1)}, u32[]{:S(2)}) copy-start(bf16[31,512]{1,0:T(8,128)(2,1)} %kernel.1) | copy-start | bytes 95236
  0.9 10.6 %collective-permute-start = (bf16[32,512]{1,0:T(8,128)(2,1)S(1)}, bf16[32,512]{1,0:T(8,128)(2,1)S(1)}, u32[]{:S(2)}, u32[]{:S(2)}) collective-permute-start(bf16[32,512]{1,0:T(8,128)(2,1)S(1)} %shard_map.146), channel_id=1, source_target_pairs={{0,2},{2,4},{4,6},{6,8},{8,10},{10,12},{12,14},{14,16},{16,18},{18... | collective-permute-start | bytes 98312 | tf_op jit(solution)/shard_map/ppermute | solution.py:310
  3.1 10.1 %copy-start = (bf16[1024,2048]{1,0:T(8,128)(2,1)S(1)}, bf16[1024,2048]{1,0:T(8,128)(2,1)}, u32[]{:S(2)}) copy-start(bf16[1024,2048]{1,0:T(8,128)(2,1)} %weight.3) | copy-start | bytes 12582916
  5.5 7.7 %copy-start.1 = (bf16[128,2048]{1,0:T(8,128)(2,1)S(1)}, bf16[128,2048]{1,0:T(8,128)(2,1)}, u32[]{:S(2)}) copy-start(bf16[128,2048]{1,0:T(8,128)(2,1)} %residual.1) | copy-start | bytes 1572868
  11.9 2.3 %copy-start.2 = (f32[2048]{0:T(1024)S(1)}, f32[2048]{0:T(1024)}, u32[]{:S(2)}) copy-start(f32[2048]{0:T(1024)} %param.23) | copy-start | bytes 24580
  11.9 2.3 %collective-permute-start.1 = (bf16[128,512]{1,0:T(8,128)(2,1)S(1)}, bf16[128,512]{1,0:T(8,128)(2,1)S(1)}, u32[]{:S(2)}, u32[]{:S(2)}) collective-permute-start(bf16[128,512]{1,0:T(8,128)(2,1)S(1)} %shard_map.147), channel_id=1, source_target_pairs={{0,1},{1,0},{2,3},{3,2},{4,5},{5,4},{6,7},{7,6},{8,9},{9,8},{10,11... | collective-permute-start | bytes 393224 | tf_op jit(solution)/shard_map/ppermute | solution.py:346
  14.2 35.4 %copy-start.5 = (bf16[1,512,2048]{2,1,0:T(8,128)(2,1)S(1)}, bf16[1,512,2048]{2,1,0:T(8,128)(2,1)}, u32[]{:S(2)}) copy-start(bf16[1,512,2048]{2,1,0:T(8,128)(2,1)} %param.29) | copy-start | bytes 6291460
  15.5 34.1 %copy-start.3 = (bf16[1,2048,512]{2,1,0:T(8,128)(2,1)S(1)}, bf16[1,2048,512]{2,1,0:T(8,128)(2,1)}, u32[]{:S(2)}) copy-start(bf16[1,2048,512]{2,1,0:T(8,128)(2,1)} %param.27) | copy-start | bytes 6291460
  15.5 34.1 %copy-start.4 = (bf16[1,2048,512]{2,1,0:T(8,128)(2,1)S(1)}, bf16[1,2048,512]{2,1,0:T(8,128)(2,1)}, u32[]{:S(2)}) copy-start(bf16[1,2048,512]{2,1,0:T(8,128)(2,1)} %param.28) | copy-start | bytes 6291460

commit v14 on v12

--- a/solution.py
+++ b/solution.py
@@ -247,17 +247,14 @@
 def combine_body(message, picked, base, out_hbm, out, sems):
     tokens = out.shape[0]
     step = message.shape[1]
-    pieces = 4
-    size = step // pieces
+    cuts = (0, step // 2, step - LANE, step)
     copies = []
-    for p in range(pieces):
-        got = jnp.dot(picked[...], message[:, p * size : (p + 1) * size], preferred_element_type=F32)
+    for start, end in zip(cuts[:-1], cuts[1:], strict=True):
+        got = jnp.dot(picked[...], message[:, start:end], preferred_element_type=F32)
         for q in range(PARTS):
-            lanes = slice(q * step + p * size, q * step + (p + 1) * size)
+            lanes = slice(q * step + start, q * step + end)
             out[:, lanes] = (base[:, lanes].astype(F32) + got[q * tokens : (q + 1) * tokens]).astype(BF16)
-            copy = pltpu.make_async_copy(
-                out.at[:, lanes], out_hbm.at[:, lanes], sems.at[p * PARTS + q]
-            )
+            copy = pltpu.make_async_copy(out.at[:, lanes], out_hbm.at[:, lanes], sems.at[len(copies)])
             copy.start()
             copies.append(copy)
     for copy in copies:

time: 89.1 us -> 89.2 us (level)
  no operation moved by 1% of the time
where the time goes in v14:
time: 89.2 us; the launch traced here: 89 us
  blocking collectives  68.5 us (77%)
  Pallas kernels  10.3 us (12%)
  waiting for transfers between devices  6.57 us (7%)
  starting transfers between devices  3.4 us (4%)
    all_to_all x2, blocking collectives, exchange(): return lax.all_to_all(x, ('sp', 'tp'), 0, 0, tiled=True).reshape(rows, step)  68.5 us
    pallas_call x7, Pallas kernels, call(): run(*(pltpu.with_memory_space_constraint(a, pltpu.HBM) if i in hbm else a...  10.3 us
    ppermute x1, waiting for transfers between devices, local(): lax.ppermute(tail, 'sp', [(i, (i + 1) % peers) for i in range(peers)])  6.06 us
    ppermute x1, starting transfers between devices, local(): lax.ppermute(tail, 'sp', [(i, (i + 1) % peers) for i in range(peers)])  2.1 us
  transfers between devices with their start and end apart: 2, of which 2 were waited for; matrix products, arithmetic and copies ran while one was open for 0% of the time, Pallas kernels for 3%

profile of v14, /device:TPU:1, one launch (start us, length us, event | category | flops | bytes accessed | tf_op | source)
XLA Modules:
  0.0 89.0 jit_solution(1235885712436365749)
XLA Ops:
  0.0 0.0 copy-start.7
  0.0 0.0 copy-start.6
  0.0 0.0 copy-start.14
  0.0 0.0 copy-start.13
  0.0 0.0 copy-start.12
  0.0 0.0 copy-start.11
  0.0 0.0 copy-start.10
  0.0 0.0 copy-start.9
  0.1 0.0 copy-start.8
  0.1 0.9 shard_map.146
  0.9 2.1 %collective-permute-start = (bf16[32,512]{1,0:T(8,128)(2,1)S(1)}, bf16[32,512]{1,0:T(8,128)(2,1)S(1)}, u32[]{:S(2)}, u32[]{:S(2)}) collective-permute-start(bf16[32,512]{1,0:T(8,128)(2,1)S(1)} %shard_map.146), channel_id=1, source_target_pairs={{0,2},{2,4},{4,6},{6,8},{8,10},{10,12},{12,14},{14,16},{16,18},{18... | collective-permute-start | bytes 98312 | tf_op jit(solution)/shard_map/ppermute | solution.py:305
  3.0 0.0 copy-done.7
  3.0 0.0 copy-done.6
  3.0 0.0 copy-done.14
  3.0 0.0 copy-done.13
  3.0 0.0 copy-done.12
  3.1 0.0 copy-done.11
  3.1 0.0 copy-done.10
  3.1 0.0 copy-done.9
  3.1 0.0 copy-done.8
  3.1 0.0 copy-start
  3.1 2.3 %shard_map.145 = (bf16[256,512]{1,0:T(8,128)(2,1)S(1)}, f32[4,256,128]{2,1,0:T(8,128)S(1)}, f32[4,32,128]{2,1,0:T(8,128)S(1)}, f32[8,512]{1,0:T(8,128)S(1)}, bf1...) custom-call(bf16[256,512]{1,0:T(8,128)(2,1)S(1)} %copy-done.6, bf16[256,512]{1,0:T(8,128)(2,1)S(1)} %copy-done.7, ...), custom_call_target="tpu_custom_call" | custom-call | flops 6000000000 | tf_op jit(solution)/shard_map/pallas_call | solution.py:42
  5.5 0.0 copy-start.1
  5.5 6.1 %collective-permute-done.halo = bf16[32,512]{1,0:T(8,128)(2,1)S(1)} collective-permute-done((bf16[32,512]{1,0:T(8,128)(2,1)S(1)}, bf16[32,512]{1,0:T(8,128)(2,1)S(1)}, u32[]{:S(2)}, u32[]{:S(2)}) %collective-permute-start) | collective-permute-done | bytes 32800 | tf_op jit(solution)/shard_map/ppermute | solution.py:305
  11.5 0.3 shard_map.147
  11.9 0.0 copy-start.2
  11.9 1.3 %collective-permute-start.1 = (bf16[128,512]{1,0:T(8,128)(2,1)S(1)}, bf16[128,512]{1,0:T(8,128)(2,1)S(1)}, u32[]{:S(2)}, u32[]{:S(2)}) collective-permute-start(bf16[128,512]{1,0:T(8,128)(2,1)S(1)} %shard_map.147), channel_id=1, source_target_pairs={{0,1},{1,0},{2,3},{3,2},{4,5},{5,4},{6,7},{7,6},{8,9},{9,8},{10,11... | collective-permute-start | bytes 393224 | tf_op jit(solution)/shard_map/ppermute | solution.py:341
  13.2 0.0 copy-done
  13.2 0.0 copy-done.1
  13.2 0.5 shard_map.148.partial
  13.7 0.5 collective-permute-done.1.other
  14.2 0.0 copy-done.2
  14.2 0.0 copy-start.5
  14.2 1.3 %shard_map.149 = (bf16[128,2048]{1,0:T(8,128)(2,1)S(1)}, bf16[1024,1024]{1,0:T(8,128)(2,1)S(1)}) custom-call(bf16[128,512]{1,0:T(8,128)(2,1)S(1)} %collective-permute-done.1.other, bf16[1024,2048]{1,0:T(8,128)(2,1)S(1)} %copy-done, f32[128,2048]{1,0:T(8,128)S(1)} %shard_map.148.partial, f32[1,2048]{1,0:T(1,128)S(1)} %bitcast.18, ...), custom_call_target="tpu_custom_call" | custom-call | flops 1000000000 | tf_op jit(solution)/shard_map/pallas_call | solution.py:42
  15.5 0.0 copy-start.3
  15.5 0.0 copy-start.4
  15.5 34.1 %all_to_all.10 = bf16[128,8,1024]{2,1,0:T(8,128)(2,1)S(1)} all-to-all(bf16[128,8,1024]{2,1,0:T(8,128)(2,1)S(1)} %bitcast.14), channel_id=1, replica_groups=mesh['sp'=64,'tp'=2] {'sp','tp'}, dimensions={0} | all-to-all | bytes 4194304 | tf_op jit(solution)/shard_map/all_to_all | solution.py:362
  49.6 0.0 copy-done.5
  49.6 0.0 copy-done.3
  49.6 0.0 copy-done.4
  49.6 3.5 %shard_map.150 = bf16[1024,1024]{1,0:T(8,128)(2,1)S(1)} custom-call(bf16[1024,1024]{1,0:T(8,128)(2,1)S(1)} %bitcast.16, bf16[2048,512]{1,0:T(8,128)(2,1)S(1)} %bitcast.19, bf16[2048,512]{1,0:T(8,128)(2,1)S(1)} %bitcast.20, bf16[512,2048]{1,0:T(8,128)(2,1)S(1)} %bitcast.21), custom_call_target="tpu_custom_call" | custom-call | flops 4000000000 | tf_op jit(solution)/shard_map/pallas_call | solution.py:42
  53.1 34.4 %all_to_all.11 = bf16[128,8,1024]{2,1,0:T(8,128)(2,1)S(1)} all-to-all(bf16[128,8,1024]{2,1,0:T(8,128)(2,1)S(1)} %bitcast.17), channel_id=1, replica_groups=mesh['sp'=64,'tp'=2] {'sp','tp'}, dimensions={0} | all-to-all | bytes 4194304 | tf_op jit(solution)/shard_map/all_to_all | solution.py:362
  87.5 1.5 %shard_map.151 = bf16[128,2048]{1,0:T(8,128)(2,1)} custom-call(bf16[1024,1024]{1,0:T(8,128)(2,1)S(1)} %bitcast.15, bf16[256,1024]{1,0:T(8,128)(2,1)S(1)} %get-tuple-element.19.picked, bf16[128,2048]{1,0:T(8,128)(2,1)S(1)} %get-tuple-element.20.base), custom_call_target="tpu_custom_call" | custom-call | flops 1000000000 | tf_op jit(solution)/shard_map/pallas_call | solution.py:42
Async XLA Ops:
  0.0 3.0 %copy-start.7 = (bf16[256,512]{1,0:T(8,128)(2,1)S(1)}, bf16[256,512]{1,0:T(8,128)(2,1)}, u32[]{:S(2)}) copy-start(bf16[256,512]{1,0:T(8,128)(2,1)} %gate_in.1) | copy-start | bytes 786436
  0.0 3.0 %copy-start.6 = (bf16[256,512]{1,0:T(8,128)(2,1)S(1)}, bf16[256,512]{1,0:T(8,128)(2,1)}, u32[]{:S(2)}) copy-start(bf16[256,512]{1,0:T(8,128)(2,1)} %value_in.1) | copy-start | bytes 786436
  0.0 3.0 %copy-start.14 = (f32[128]{0:T(128)S(1)}, f32[128]{0:T(128)}, u32[]{:S(2)}) copy-start(f32[128]{0:T(128)} %param.26) | copy-start | bytes 1540
  0.0 3.0 %copy-start.13 = (f32[128,2]{0,1:T(2,128)S(1)}, f32[128,2]{0,1:T(2,128)}, u32[]{:S(2)}) copy-start(f32[128,2]{0,1:T(2,128)} %param.25) | copy-start | bytes 3076
  0.0 3.0 %copy-start.12 = (s32[128,2]{0,1:T(2,128)S(1)}, s32[128,2]{0,1:T(2,128)}, u32[]{:S(2)}) copy-start(s32[128,2]{0,1:T(2,128)} %param.24) | copy-start | bytes 3076
  0.0 3.0 %copy-start.11 = (f32[512]{0:T(512)S(1)}, f32[512]{0:T(512)}, u32[]{:S(2)}) copy-start(f32[512]{0:T(512)} %param.20) | copy-start | bytes 6148
  0.0 3.0 %copy-start.10 = (f32[512]{0:T(512)S(1)}, f32[512]{0:T(512)}, u32[]{:S(2)}) copy-start(f32[512]{0:T(512)} %param.19) | copy-start | bytes 6148
  0.0 3.0 %copy-start.9 = (f32[512]{0:T(512)S(1)}, f32[512]{0:T(512)}, u32[]{:S(2)}) copy-start(f32[512]{0:T(512)} %param.18) | copy-start | bytes 6148
  0.1 3.0 %copy-start.8 = (bf16[31,512]{1,0:T(8,128)(2,1)S(1)}, bf16[31,512]{1,0:T(8,128)(2,1)}, u32[]{:S(2)}) copy-start(bf16[31,512]{1,0:T(8,128)(2,1)} %kernel.1) | copy-start | bytes 95236
  0.9 10.6 %collective-permute-start = (bf16[32,512]{1,0:T(8,128)(2,1)S(1)}, bf16[32,512]{1,0:T(8,128)(2,1)S(1)}, u32[]{:S(2)}, u32[]{:S(2)}) collective-permute-start(bf16[32,512]{1,0:T(8,128)(2,1)S(1)} %shard_map.146), channel_id=1, source_target_pairs={{0,2},{2,4},{4,6},{6,8},{8,10},{10,12},{12,14},{14,16},{16,18},{18... | collective-permute-start | bytes 98312 | tf_op jit(solution)/shard_map/ppermute | solution.py:305
  3.1 10.1 %copy-start = (bf16[1024,2048]{1,0:T(8,128)(2,1)S(1)}, bf16[1024,2048]{1,0:T(8,128)(2,1)}, u32[]{:S(2)}) copy-start(bf16[1024,2048]{1,0:T(8,128)(2,1)} %weight.3) | copy-start | bytes 12582916
  5.5 7.7 %copy-start.1 = (bf16[128,2048]{1,0:T(8,128)(2,1)S(1)}, bf16[128,2048]{1,0:T(8,128)(2,1)}, u32[]{:S(2)}) copy-start(bf16[128,2048]{1,0:T(8,128)(2,1)} %residual.1) | copy-start | bytes 1572868
  11.9 2.3 %copy-start.2 = (f32[2048]{0:T(1024)S(1)}, f32[2048]{0:T(1024)}, u32[]{:S(2)}) copy-start(f32[2048]{0:T(1024)} %param.23) | copy-start | bytes 24580
  11.9 2.3 %collective-permute-start.1 = (bf16[128,512]{1,0:T(8,128)(2,1)S(1)}, bf16[128,512]{1,0:T(8,128)(2,1)S(1)}, u32[]{:S(2)}, u32[]{:S(2)}) collective-permute-start(bf16[128,512]{1,0:T(8,128)(2,1)S(1)} %shard_map.147), channel_id=1, source_target_pairs={{0,1},{1,0},{2,3},{3,2},{4,5},{5,4},{6,7},{7,6},{8,9},{9,8},{10,11... | collective-permute-start | bytes 393224 | tf_op jit(solution)/shard_map/ppermute | solution.py:341
  14.2 35.4 %copy-start.5 = (bf16[1,512,2048]{2,1,0:T(8,128)(2,1)S(1)}, bf16[1,512,2048]{2,1,0:T(8,128)(2,1)}, u32[]{:S(2)}) copy-start(bf16[1,512,2048]{2,1,0:T(8,128)(2,1)} %param.29) | copy-start | bytes 6291460
  15.5 34.1 %copy-start.3 = (bf16[1,2048,512]{2,1,0:T(8,128)(2,1)S(1)}, bf16[1,2048,512]{2,1,0:T(8,128)(2,1)}, u32[]{:S(2)}) copy-start(bf16[1,2048,512]{2,1,0:T(8,128)(2,1)} %param.27) | copy-start | bytes 6291460
  15.5 34.1 %copy-start.4 = (bf16[1,2048,512]{2,1,0:T(8,128)(2,1)S(1)}, bf16[1,2048,512]{2,1,0:T(8,128)(2,1)}, u32[]{:S(2)}) copy-start(bf16[1,2048,512]{2,1,0:T(8,128)(2,1)} %param.28) | copy-start | bytes 6291460
